TPU v7x, 128 devices: a whole 4x4x4 slice. The times are simulated.
128 devices in a mesh: sp: 16 (over z, x), tp: 8 (over y, core).
Axes of the slice: x: 4, y: 4, z: 4, core: 2. Of those that a mesh axis runs over, the one named last changes fastest.
Arguments:
- query_small: bfloat16 [12288, 1024], P('sp', 'tp'), may hold values from -6 to 6
- key_small: bfloat16 [12288, 1024], P('sp', 'tp'), may hold values from -6 to 6
- value_small: bfloat16 [12288, 1024], P('sp', 'tp'), may hold values from -6 to 6
- gates_small: float32 [12288, 16], P('sp', 'tp'), as said below
- query_large: bfloat16 [12288, 1024], P('sp', 'tp'), may hold values from -6 to 6
- key_large: bfloat16 [12288, 1024], P('sp', 'tp'), may hold values from -6 to 6
- value_large: bfloat16 [12288, 1024], P('sp', 'tp'), may hold values from -6 to 6
- gates_large: float32 [12288, 8], P('sp', 'tp'), as said below
- residual: bfloat16 [12288, 2048], P(('sp', 'tp')), may hold values from -6 to 6
- mixer_small: bfloat16 [1024, 2048], P('tp'), may hold values from -1 to 1
- mixer_large: bfloat16 [1024, 2048], P('tp'), may hold values from -1 to 1
- mix_gain: float32 [2048], replicated, may hold values from 0.1 to 1.9
- value_weight: bfloat16 [2048, 5632], P('sp', 'tp'), may hold values from -0.125 to 0.125
- gate_weight: bfloat16 [2048, 5632], P('sp', 'tp'), may hold values from -0.125 to 0.125
- value_taps: float32 [3, 5632], P(None, 'tp'), may hold values from -3 to 3
- gate_taps: float32 [3, 5632], P(None, 'tp'), may hold values from -3 to 3
- down_weight: bfloat16 [5632, 2048], P('tp', 'sp'), may hold values from -0.078125 to 0.078125
- final_gain: float32 [2048], replicated, may hold values from 0.1 to 1.9
Outputs:
- layer_out: bfloat16 [12288, 2048], P(('sp', 'tp'))
Inputs may be any that keep to these rules, and one draw needn't show every extreme that they name: `gates_small`: each column never rises from one position to the next, and its first entry is negative. `gates_large`: each column never rises from one position to the next, and its first entry is negative.
All inputs are finite; a program needn't handle non-finite values.
Results may differ from a plain program's by a relative error of at most 0.018.
Values may be sent and summed in bfloat16 or wider, within the bound.
No kernel may reach another device: no remote copies, remote signals or barrier semaphores. Data moves between devices by JAX's collectives and lax.ppermute only.
A program may use at most 128 MiB of HBM per device.

v0:
```python
import math

import jax
import jax.numpy as jnp
import numpy as np
from jax import lax
from jax.experimental import pallas as pl
from jax.experimental.pallas import tpu as pltpu
from jax.sharding import Mesh
from jax.sharding import PartitionSpec as P


SP = ("sp_z", "sp_x")
TP = ("tp_y", "tp_c")
ALL = SP + TP
bf16 = jnp.bfloat16
f32 = jnp.float32
residual_scale = 2.0**0.5
epsilon = 1e-05


def shifted(value, axis, steps):
    count = lax.axis_size(axis)
    return lax.ppermute(value, axis, [(i, (i + steps) % count) for i in range(count)])


def passed_along(value, axis, steps):
    count = lax.axis_size(axis)
    first, last = (max(0, -steps), min(count, count - steps))
    return lax.ppermute(value, axis, [(source, source + steps) for source in range(first, last)])


LOW = -1e30
CHUNK = 256
EXTRA = 32
STAT_ROWS = 16
RATE = 250e6


def in_pieces(value):
    high = value.astype(bf16).astype(f32)
    middle = (value - high).astype(bf16).astype(f32)
    return high, middle, value - high - middle


def cost_of(us):
    return pl.CostEstimate(flops=int(us * RATE), transcendentals=0, bytes_accessed=0)


def pack(slot, key_small, value_small, key_large, value_large, query_small, query_large, gates):
    rows, width = key_small.shape
    half = rows // 2
    low = width // 2
    tiles = rows // width

    def body(slot_ref, ks, vs, kl, vl, qs, ql, g, kv, *q):
        lane = lax.broadcasted_iota(jnp.int32, (rows, width), 1)
        turn = lambda ref: pltpu.roll(ref[...].astype(f32), low, 1)
        for slot in range(2):
            part = slice(slot * half, (slot + 1) * half)
            kv[slot, :half] = kl[part]
            kv[slot, half:rows] = vl[part]
        kv[2, :rows] = jnp.where(lane < low, ks[...].astype(f32), turn(vs)).astype(bf16)
        kv[3, :rows] = jnp.where(lane < low, turn(ks), vs[...].astype(f32)).astype(bf16)
        for shift in range(4):
            target = lax.rem(slot_ref[0] + shift, 4)

            @pl.when(target < 2)
            def _():
                q[shift][...] = ql[...]

            @pl.when(target == 2)
            def _():
                q[shift][...] = qs[...]

            @pl.when(target == 3)
            def _():
                q[shift][...] = turn(qs).astype(bf16)

        for slot, head in ((0, 2), (1, 2), (2, 0), (3, 1)):
            blocks = []
            for piece in in_pieces(g[head : head + 1, :]):
                blocks += [piece[:, i * width : (i + 1) * width] for i in range(tiles)]
                blocks.append(jnp.zeros((8 - tiles, width), f32))
            blocks.append(jnp.zeros((EXTRA - 24, width), f32))
            kv[slot, rows:] = jnp.concatenate(blocks, axis=0).astype(bf16)

    vm = pl.BlockSpec(memory_space=pltpu.VMEM)
    return pl.pallas_call(
        body,
        in_specs=[pl.BlockSpec(memory_space=pltpu.SMEM)] + [vm] * 7,
        out_specs=[vm] * 5,
        out_shape=[jax.ShapeDtypeStruct((4, rows + EXTRA, width), bf16)]
        + [jax.ShapeDtypeStruct((rows, width), bf16)] * 4,
        cost_estimate=cost_of(2.5),
    )(slot, key_small, value_small, key_large, value_large, query_small, query_large, gates)


def work_tables(calls, depth, turns):
    tables = []
    for here in range(turns):
        row = []
        for shifts in calls:
            steps = []
            for z in range(depth):
                for n, shift in enumerate(shifts):
                    there = (here + shift) % turns
                    for w in range(depth):
                        key, query = w * turns + there, z * turns + here
                        if key < query:
                            steps.append((z, n * depth + w, 0))
                for n, shift in enumerate(shifts):
                    if shift == 0:
                        steps.append((z, n * depth + z, 1))
            row.append(steps)
        tables.append(row)
    longest = [max(len(tables[h][k]) for h in range(turns)) + 1 for k in range(len(calls))]
    out = []
    for k in range(len(calls)):
        table = np.zeros((turns, longest[k] * 3 + 1), np.int32)
        for h in range(turns):
            flat = np.array(tables[h][k] + [(0, 0, 0)] * (longest[k] - len(tables[h][k])), np.int32)
            table[h, :-1] = flat.reshape(-1)
            table[h, -1] = len(tables[h][k])
        out.append(table)
    return out


def attend(where, table, queries, chunks, state, final, tensor_parts, has_diagonal, cost):
    depth = len(queries)
    rows, width = queries[0].shape
    half = rows // 2
    low = width // 2
    tiles = rows // width
    blocks = sum(c.shape[0] for c in chunks)
    columns = rows // CHUNK
    tall = width + 16
    last = table.shape[1] - 1
    own = rows // tensor_parts
    fresh = state is None

    def body(*refs):
        where_ref, table_ref = refs[:2]
        q_refs = refs[2 : 2 + depth]
        chunk_refs = refs[2 + depth : 2 + depth + len(chunks)]
        at = 2 + depth + len(chunks) + (0 if fresh else 2)
        state_in = () if fresh else refs[at - 2 : at]
        if final:
            out_ref = refs[at]
            acc, peak = refs[at + 1 : at + 3]
            scratch = refs[at + 3 :]
        else:
            acc, peak = refs[at : at + 2]
            scratch = refs[at + 2 :]
        qa, ka_small, va_small, ka_large, va_large, first = scratch
        slot = where_ref[0]
        column = where_ref[1]
        count = table_ref[column, last]

        @pl.loop(0, depth)
        def _(z):
            if fresh:
                acc[z] = jnp.zeros(acc.shape[1:], f32)
                peak[z] = jnp.full(peak.shape[1:], LOW, f32)
            else:
                acc[z] = state_in[0][z]
                peak[z] = state_in[1][z]

        def attention(small):
            d = low if small else width
            ext = d + 16
            span = rows if small else half
            tile = CHUNK if small else half
            parts = span // tile
            root = d**0.5
            rate = math.log2(math.e) / root
            ka, va = (ka_small, va_small) if small else (ka_large, va_large)
            deep = width if small else 2 * width
            lane = lax.broadcasted_iota(jnp.int32, (rows, width), 1)

            for shift, q_ref in enumerate(q_refs):
                z = lax.rem(slot + depth - shift, depth)
                q = q_ref[...]
                if small:
                    one = ((lane >= d) & (lane < d + 3)).astype(f32)
                    qa[z, :, :width] = jnp.where(lane < d, q.astype(f32), one).astype(bf16)
                else:
                    qa[z, :, :width] = q
                    qa[z, :, width:] = (lane < 3).astype(f32).astype(bf16)

            def prepare(ref, n, block):
                pieces = ref[n, rows : rows + 24].astype(f32)
                gate = pieces[0:8] + pieces[8:16] + pieces[16:24]
                bias = jnp.concatenate([gate[i : i + 1] for i in range(tiles)], axis=1) * -root
                bias = jnp.broadcast_to(bias, (8, rows))
                if not small:
                    bias = jnp.where(slot == 0, bias[:, :half], bias[:, half:])
                high, middle, rest = in_pieces(bias)
                row = lax.broadcasted_iota(jnp.int32, (8, span), 0)
                zero = jnp.zeros((8, span), f32)
                picked = jnp.where(row == 0, high, jnp.where(row == 1, middle, jnp.where(row == 2, rest, zero)))
                before = d if small else 0
                stack = [picked, jnp.zeros((width - before - 8, span), f32)]
                if before:
                    stack = [jnp.zeros((before, span), f32)] + stack
                gate_columns = jnp.concatenate(stack, axis=0).astype(bf16).T
                if small:
                    kv = ref[n, :rows]
                    ka[block] = jnp.where(lane < d, kv, gate_columns)
                    va[block, :d] = kv.T[d:]
                else:
                    ka[block, :, :width] = ref[n, :half]
                    ka[block, :, width:] = gate_columns
                    va[block, :d] = ref[n, half:rows].T
                va[block, d:] = jnp.ones((16, span), bf16)

            offset = 0
            for ref in chunk_refs:
                base = offset

                @pl.loop(0, ref.shape[0])
                def _(n):
                    prepare(ref, n, base + n)

                offset += ref.shape[0]

            def scores(z, block, c, t):
                return lax.dot_general(
                    ka[block, t * tile : (t + 1) * tile],
                    qa[z, c * CHUNK : (c + 1) * CHUNK, :deep],
                    (((1,), (1,)), ((), ())),
                    preferred_element_type=f32,
                )

            def masked(s, c, t, flag):
                if small and t < c:
                    return s
                key = lax.broadcasted_iota(jnp.int32, (tile, CHUNK), 0) + t * tile
                if not small:
                    key = key + slot * half
                    key = jnp.where(flag == 0, 0, key)
                query = lax.broadcasted_iota(jnp.int32, (tile, CHUNK), 1) + c * CHUNK
                return jnp.where(key <= query, s, LOW)

            def step(n, diagonal):
                z, block = table_ref[column, 3 * n], table_ref[column, 3 * n + 1]
                next_z, next_block = table_ref[column, 3 * n + 3], table_ref[column, 3 * n + 4]
                held_count = lambda c: c + 1 if diagonal and small else parts
                held = [first[t * tile : (t + 1) * tile] for t in range(held_count(0))]
                for c in range(columns):
                    cols = slice(c * CHUNK, (c + 1) * CHUNK)
                    if diagonal:
                        held = [masked(s, c, t, table_ref[column, 3 * n + 2]) for t, s in enumerate(held)]
                    top = held[0]
                    for s in held[1:]:
                        top = jnp.maximum(top, s)
                    old = peak[z, 0:1, cols]
                    new = jnp.maximum(old, jnp.max(top, axis=0, keepdims=True))
                    scaled = new * rate
                    factor = jnp.exp2(old * rate - scaled)
                    peak[z, 0:1, cols] = new
                    coming = []
                    added = None
                    following = c + 1 < columns
                    ahead = held_count(c + 1) if following else parts
                    for t in range(max(len(held), ahead)):
                        if t < ahead:
                            if following:
                                coming.append(scores(z, block, c + 1, t))
                            else:
                                first[t * tile : (t + 1) * tile] = scores(next_z, next_block, 0, t)
                        if t < len(held):
                            w = jnp.exp2(held[t] * rate - scaled).astype(bf16)
                            add = jnp.dot(
                                va[block, :, t * tile : (t + 1) * tile], w, preferred_element_type=f32
                            )
                            added = add if added is None else added + add
                    acc[z, :ext, cols] = acc[z, :ext, cols] * factor + added
                    held = coming

            for t in range(parts):
                first[t * tile : (t + 1) * tile] = scores(table_ref[column, 0], table_ref[column, 1], 0, t)

            @pl.loop(0, count)
            def _(n):
                if not has_diagonal or not small:
                    step(n, has_diagonal)
                    return
                diagonal = table_ref[column, 3 * n + 2]

                @pl.when(diagonal == 0)
                def _():
                    step(n, False)

                @pl.when(diagonal == 1)
                def _():
                    step(n, True)

            if final:

                @pl.loop(0, depth)
                def _(z):
                    total = acc[z, d : d + 1]
                    out = acc[z, :d] / total
                    if small:
                        out = jnp.concatenate([out, jnp.zeros((width - d, rows), f32)], axis=0)
                    out = out.T.astype(bf16)
                    level = peak[z, 0:1] * rate + jnp.log2(total)
                    stat = jnp.concatenate([*in_pieces(level), jnp.zeros((STAT_ROWS - 3, rows), f32)], axis=0)
                    for r in range(tensor_parts):
                        out_ref[z * tensor_parts + r, :own] = out[r * own : (r + 1) * own]
                        if not small:
                            mine = stat[:, r * own : (r + 1) * own]
                            mine = jnp.concatenate([mine, jnp.zeros((STAT_ROWS, width - own), f32)], axis=1)
                            out_ref[z * tensor_parts + r, own:] = mine.astype(bf16)
                        else:
                            out_ref[z * tensor_parts + r, own:] = jnp.zeros((STAT_ROWS, width), bf16)

        @pl.when(slot < 2)
        def _():
            attention(False)

        @pl.when(slot >= 2)
        def _():
            attention(True)

    vm = pl.BlockSpec(memory_space=pltpu.VMEM)
    sm = pl.BlockSpec(memory_space=pltpu.SMEM)
    state_shapes = [((depth, tall, rows), f32), ((depth, 8, rows), f32)]
    scratch = [pltpu.VMEM(s, t) for s, t in state_shapes] if final else []
    scratch += [
        pltpu.VMEM((depth, rows, 2 * width), bf16),
        pltpu.VMEM((blocks, rows, width), bf16),
        pltpu.VMEM((blocks, low + 16, rows), bf16),
        pltpu.VMEM((blocks, half, 2 * width), bf16),
        pltpu.VMEM((blocks, tall, half), bf16),
        pltpu.VMEM((rows, CHUNK), f32),
    ]
    if final:
        out_shape = jax.ShapeDtypeStruct((depth * tensor_parts, own + STAT_ROWS, width), bf16)
        out_specs = vm
    else:
        out_shape = [jax.ShapeDtypeStruct(s, t) for s, t in state_shapes]
        out_specs = [vm, vm]
    args = [where, table, *queries, *chunks] + ([] if fresh else list(state))
    return pl.pallas_call(
        body,
        in_specs=[sm, sm] + [vm] * (len(args) - 2),
        out_specs=out_specs,
        scratch_shapes=scratch,
        out_shape=out_shape,
        compiler_params=pltpu.CompilerParams(vmem_limit_bytes=58 * 2**20),
        cost_estimate=cost_of(cost),
    )(*args)


def mix_rows(place, arrived, mixers, residual, gain):
    own, wide = residual.shape
    width = arrived.shape[2]
    cores = 2
    turns = arrived.shape[0] // 4 // cores
    parts = turns * cores

    def body(place_ref, arrived_ref, *refs):
        mixer_refs = refs[: len(mixers)]
        residual_ref, gain_ref, out_ref, acc = refs[len(mixers) :]
        lane = lax.broadcasted_iota(jnp.int32, (own, width), 1)

        def level(index):
            pieces = arrived_ref[index, own:].astype(f32)
            line = pieces[0:1] + pieces[1:2] + pieces[2:3]
            return jnp.broadcast_to(line, (8, width)).T[:own, 0:1]

        def rows_of(part):
            second = pltpu.roll(arrived_ref[3 * parts + part, :own].astype(f32), width // 2, 1)
            small = jnp.where(lane < width // 2, arrived_ref[2 * parts + part, :own].astype(f32), second)
            share = 1.0 / (1.0 + jnp.exp2(level(part) - level(parts + part)))
            large = arrived_ref[part, :own].astype(f32) * (1.0 - share) + arrived_ref[
                parts + part, :own
            ].astype(f32) * share
            return small.astype(bf16), large.astype(bf16)

        acc[...] = residual_ref[...].astype(f32) * residual_scale
        for ref, (_, shift, other) in zip(mixer_refs, mixers):
            y = lax.rem(place_ref[0] + shift + turns, turns)
            core = place_ref[1] if other == 0 else 1 - place_ref[1]
            both = rows_of(y * cores + core)
            acc[...] += jnp.dot(jnp.concatenate(both, axis=1), ref[...], preferred_element_type=f32)
        values = acc[...]
        center = jnp.mean(values, axis=-1, keepdims=True)
        values = values - center
        spread = jnp.mean(jnp.square(values), axis=-1, keepdims=True)
        out_ref[...] = (values * lax.rsqrt(spread + epsilon) * gain_ref[...]).astype(bf16)

    vm = pl.BlockSpec(memory_space=pltpu.VMEM)
    return pl.pallas_call(
        body,
        in_specs=[pl.BlockSpec(memory_space=pltpu.SMEM)] + [vm] * (len(mixers) + 3),
        out_specs=vm,
        scratch_shapes=[pltpu.VMEM((own, wide), f32)],
        out_shape=jax.ShapeDtypeStruct((own, wide), bf16),
        compiler_params=pltpu.CompilerParams(vmem_limit_bytes=40 * 2**20),
        cost_estimate=cost_of(5.0),
    )(place, arrived, *[m[0] for m in mixers], residual, gain.reshape(1, wide))


BLOCK = 768
LEAD = 16


def pack_weights(value_weight, gate_weight, down_weight):
    rows, width = value_weight.shape

    def body(v, g, d, out):
        for k, part in enumerate((v[...], g[...], d[...].T)):
            out[:, k * BLOCK : k * BLOCK + width] = part
            out[:, k * BLOCK + width : (k + 1) * BLOCK] = jnp.zeros((rows, BLOCK - width), bf16)

    vm = pl.BlockSpec(memory_space=pltpu.VMEM)
    return pl.pallas_call(
        body,
        in_specs=[vm] * 3,
        out_specs=vm,
        out_shape=jax.ShapeDtypeStruct((rows, 3 * BLOCK), bf16),
        cost_estimate=cost_of(1.5),
    )(value_weight, gate_weight, down_weight)


def window(array, k):
    return pl.BlockSpec((array.shape[0], BLOCK), lambda i: (0, k))


def whole(array):
    return pl.BlockSpec(array.shape, lambda i: (0,) * array.ndim)


def ups(chunks, weights, width, cost):
    rows = sum(c.shape[0] for c in chunks)

    def body(*refs):
        value_ref, gate_ref, out_value, out_gate = refs[len(chunks) :]
        x = jnp.concatenate([r[...] for r in refs[: len(chunks)]], axis=0)
        for ref, out in ((value_ref, out_value), (gate_ref, out_gate)):
            out[...] = jnp.dot(x, ref[:, :width], preferred_element_type=f32).astype(bf16)

    shape = jax.ShapeDtypeStruct((rows, width), bf16)
    return pl.pallas_call(
        body,
        grid=(1,),
        in_specs=[whole(c) for c in chunks] + [window(weights, 0), window(weights, 1)],
        out_specs=[whole(shape)] * 2,
        out_shape=[shape] * 2,
        compiler_params=pltpu.CompilerParams(vmem_limit_bytes=40 * 2**20),
        cost_estimate=cost_of(cost),
    )(*chunks, weights, weights)


def ends(place, pieces, spots, own, turns, cores):
    width = pieces[0][0].shape[1]

    def body(place_ref, *refs):
        outs, leaving = refs[-3:-1], refs[-1]
        spot = 0
        for k in range(0, len(refs) - 3, 2):
            for i in range(refs[k].shape[0] // own):
                shift, other = spots[spot]
                spot += 1
                y = lax.rem(place_ref[0] + shift + turns, turns)
                core = place_ref[1] if other == 0 else 1 - place_ref[1]
                for side in range(2):
                    outs[side][y * cores + core] = refs[k + side][(i + 1) * own - LEAD : (i + 1) * own]
        for side in range(2):
            leaving[side * LEAD : (side + 1) * LEAD] = outs[side][turns * cores - 1]

    vm = pl.BlockSpec(memory_space=pltpu.VMEM)
    flat = [a for pair in pieces for a in pair]
    return pl.pallas_call(
        body,
        in_specs=[pl.BlockSpec(memory_space=pltpu.SMEM)] + [vm] * len(flat),
        out_specs=[vm] * 3,
        out_shape=[jax.ShapeDtypeStruct((turns * cores, LEAD, width), bf16)] * 2
        + [jax.ShapeDtypeStruct((2 * LEAD, width), bf16)],
        cost_estimate=cost_of(1.5),
    )(place, *flat)


def downs(place, pieces, groups, tails, halo, value_taps, gate_taps, weights, own, turns, cores, cost):
    width = pieces[0][0].shape[1]
    wide = weights.shape[0]
    count = len(groups)

    def body(place_ref, *refs):
        vt_ref, gt_ref, down_ref, halo_ref = refs[:4]
        tail_refs = refs[4:6]
        up_refs = refs[6 : 6 + 2 * len(pieces)]
        theirs, mine, hidden, terms = refs[6 + 2 * len(pieces) :]

        def filtered(ref, taps, tail, side, at, part):
            halo_rows = halo_ref[side * LEAD : (side + 1) * LEAD].astype(f32)
            before = tail[jnp.maximum(part - 1, 0)].astype(f32)
            before = jnp.where(part == 0, halo_rows, before)
            here = ref[pl.ds(pl.multiple_of(at * own, LEAD), own)].astype(f32)
            rows = jnp.concatenate([before, here], axis=0)
            two = pltpu.roll(rows, 2, 0)[LEAD:]
            one = pltpu.roll(rows, 1, 0)[LEAD:]
            return taps[0:1] * two + taps[1:2] * one + taps[2:3] * rows[LEAD:]

        @pl.loop(0, 2)
        def _(turn):
            core = jnp.where(turn == 0, 1 - place_ref[1], place_ref[1])
            for i, (piece, at_own, at_other, shift) in enumerate(groups):
                at = jnp.where(turn == 0, at_other, at_own)
                part = lax.rem(place_ref[0] + shift + turns, turns) * cores + core
                value = filtered(up_refs[2 * piece], vt_ref, tail_refs[0], 0, at, part)
                gate = filtered(up_refs[2 * piece + 1], gt_ref, tail_refs[1], 1, at, part)
                hidden[i * own : (i + 1) * own] = (gate / (1.0 + jnp.exp(-gate)) * value).astype(bf16)
            terms[...] = lax.dot_general(
                hidden[...],
                down_ref[:, :width],
                (((1,), (1,)), ((), ())),
                preferred_element_type=f32,
            )
            for own_turn, out in enumerate((theirs, mine)):

                @pl.when(turn == own_turn)
                def _():
                    @pl.loop(0, count)
                    def _(i):
                        out[i] = terms[pl.ds(pl.multiple_of(i * own, LEAD), own)].astype(out.dtype)

    shapes = [jax.ShapeDtypeStruct((count, own, wide), t) for t in (bf16, f32)]
    flat = [a for pair in pieces for a in pair]
    return pl.pallas_call(
        body,
        grid=(1,),
        in_specs=[pl.BlockSpec(memory_space=pltpu.SMEM), whole(value_taps), whole(gate_taps)]
        + [window(weights, 2), whole(halo), whole(tails[0]), whole(tails[1])]
        + [whole(a) for a in flat],
        out_specs=[whole(x) for x in shapes],
        out_shape=shapes,
        scratch_shapes=[
            pltpu.VMEM((count * own, width), bf16),
            pltpu.VMEM((count * own, wide), f32),
        ],
        compiler_params=pltpu.CompilerParams(vmem_limit_bytes=50 * 2**20),
        cost_estimate=cost_of(cost),
    )(place, value_taps, gate_taps, weights, halo, *tails, *flat)


def paired(mine, theirs, kinds):
    count, own, wide = mine.shape

    def body(mine_ref, their_ref, *outs):
        for i, out in enumerate(outs):
            out[...] = (mine_ref[i] + their_ref[i].astype(f32)).astype(out.dtype)

    vm = pl.BlockSpec(memory_space=pltpu.VMEM)
    return pl.pallas_call(
        body,
        in_specs=[vm] * 2,
        out_specs=[vm] * count,
        out_shape=[jax.ShapeDtypeStruct((own, wide), kind) for kind in kinds],
        cost_estimate=cost_of(0.7 * count),
    )(mine, theirs)


def finish(mixed, own, shares, gain):
    rows, wide = mixed.shape

    def body(*refs):
        mixed_ref, own_ref = refs[:2]
        gain_ref, out_ref = refs[-2:]
        total = own_ref[...]
        for r in refs[2:-2]:
            total = total + r[...].astype(f32)
        values = residual_scale * mixed_ref[...].astype(f32) + total
        center = jnp.mean(values, axis=-1, keepdims=True)
        values = values - center
        spread = jnp.mean(jnp.square(values), axis=-1, keepdims=True)
        out_ref[...] = (values * lax.rsqrt(spread + epsilon) * gain_ref[...]).astype(bf16)

    vm = pl.BlockSpec(memory_space=pltpu.VMEM)
    return pl.pallas_call(
        body,
        in_specs=[vm] * (3 + len(shares)),
        out_specs=vm,
        out_shape=jax.ShapeDtypeStruct((rows, wide), bf16),
        cost_estimate=cost_of(2.0),
    )(mixed, own, *shares, gain.reshape(1, wide))


def per_device(
    query_small,
    key_small,
    value_small,
    gates_small,
    query_large,
    key_large,
    value_large,
    gates_large,
    residual,
    mixer_small,
    mixer_large,
    mix_gain,
    value_weight,
    gate_weight,
    value_taps,
    gate_taps,
    down_weight,
    final_gain,
):
    shard_rows = query_small.shape[0]
    slot = lax.axis_index("sp_z").astype(jnp.int32)
    column = lax.axis_index("sp_x").astype(jnp.int32)
    depth, turns = lax.axis_size("sp_z"), lax.axis_size("sp_x")
    heads_small = gates_small.shape[1]
    heads_large = gates_large.shape[1]
    blank = jnp.zeros((8 - heads_small - heads_large, shard_rows), f32)
    own_gates = jnp.concatenate([gates_small.T, gates_large.T, blank], axis=0)
    packed, *asked = pack(
        slot.reshape(1),
        key_small,
        value_small,
        key_large,
        value_large,
        query_small,
        query_large,
        own_gates,
    )
    shards = pack_weights(value_weight, gate_weight, down_weight)
    packed, shards = lax.optimization_barrier((packed, shards))
    weights = lax.all_gather(shards, SP, axis=0, tiled=True)
    pairs = lax.all_to_all(packed, "sp_z", split_axis=0, concat_axis=0, tiled=True)
    queries = [asked[0]] + [shifted(asked[k], "sp_z", k) for k in range(1, depth)]
    pairs, *queries = lax.optimization_barrier((pairs, *queries))
    before = shifted(pairs, "sp_x", 1)
    after = shifted(pairs, "sp_x", -1)
    mixer = jnp.concatenate([mixer_small, mixer_large], axis=0)
    mixers = [mixer, shifted(mixer, "tp_y", 1), shifted(mixer, "tp_y", -1)]
    calls = ((0,), (-1, 1), (2,))
    tables = work_tables(calls, depth, turns)
    place_here = jnp.stack([slot, column])
    call = lambda k, chunks, state: attend(
        place_here,
        jnp.asarray(tables[k]),
        queries,
        chunks,
        state,
        k + 1 == len(calls),
        lax.axis_size(TP),
        0 in calls[k],
        12.0 * len(calls[k]),
    )
    state = call(0, [pairs], None)
    before, after, state, mixers = lax.optimization_barrier((before, after, state, mixers))
    far = [
        shifted(before[: depth // 2], "sp_x", 1),
        shifted(after[depth // 2 :], "sp_x", -1),
    ]
    mixers.append(shifted(mixers[1], "tp_y", 1))
    state = call(1, [before, after], state)
    state = call(2, far, state)
    state, mixers, weights = lax.optimization_barrier((state, mixers, weights))
    arrived = lax.all_to_all(state, ("sp_z",) + TP, split_axis=0, concat_axis=0, tiled=True)
    shifts = (0, -1, 1, 2)
    mixers = [(a, shift, 0) for a, shift in zip(mixers, shifts)] + [
        (shifted(a, "tp_c", 1), shift, 1) for a, shift in zip(mixers, shifts)
    ]
    place = jnp.stack([lax.axis_index("tp_y"), lax.axis_index("tp_c")]).astype(jnp.int32)
    mixed = mix_rows(place, arrived, mixers, residual, mix_gain)
    turns_y, cores = lax.axis_size("tp_y"), lax.axis_size("tp_c")
    own_rows = mixed.shape[0]
    half = own_rows // 2
    width = value_weight.shape[1]
    spots = [(0, 0), (0, 1), (-1, 0), (1, 0), (-1, 1), (1, 1), (2, 0), (2, 1)]
    last_one, next_one = shifted(mixed, "tp_y", 1), shifted(mixed, "tp_y", -1)
    near = ups([mixed, shifted(mixed, "tp_c", 1)], weights, width, 3.0)
    near, last_one, next_one = lax.optimization_barrier((near, last_one, next_one))
    opposite = [shifted(last_one[:half], "tp_y", 1), shifted(next_one[half:], "tp_y", -1)]
    beside = [last_one, next_one] + [shifted(a, "tp_c", 1) for a in (last_one, next_one)]
    beside = ups(beside, weights, width, 4.0)
    beside, opposite = lax.optimization_barrier((beside, opposite))
    opposite = ups(opposite + [shifted(a, "tp_c", 1) for a in opposite], weights, width, 3.0)
    pieces = [near, beside, opposite]
    *tails, leaving = ends(place, pieces, spots, own_rows, turns_y, cores)
    halo = passed_along(leaving, SP, 1)
    down = lambda chosen, groups, cost: downs(
        place,
        chosen,
        groups,
        tails,
        halo,
        value_taps,
        gate_taps,
        weights,
        own_rows,
        turns_y,
        cores,
        cost,
    )
    theirs, mine = down([opposite], [(0, 0, 1, 2)], 4.0)
    (distant,) = paired(mine, shifted(theirs, "tp_c", 1), [bf16])
    near, beside, distant = lax.optimization_barrier((near, beside, distant))
    shares = [shifted(distant, "tp_y", 2)]
    theirs, mine = down([near, beside], [(0, 0, 1, 0), (1, 0, 2, -1), (1, 1, 3, 1)], 8.0)
    own, before, after = paired(mine, shifted(theirs, "tp_c", 1), [f32, bf16, bf16])
    shares += [shifted(before, "tp_y", -1), shifted(after, "tp_y", 1)]
    return finish(mixed, own, shares, final_gain)


def solution(mesh):
    split = Mesh(mesh.devices.reshape(4, 4, 4, 2), ALL)
    placed = (P(SP, TP),) * 8 + (
        P(ALL, None),
        P(TP, None),
        P(TP, None),
        P(),
        P(SP, TP),
        P(SP, TP),
        P(None, TP),
        P(None, TP),
        P(TP, SP),
        P(),
    )

    return jax.shard_map(per_device, mesh=split, in_specs=placed, out_specs=P(ALL, None), check_vma=False)
```

profile of v0, /device:TPU:33, one launch (start us, length us, event | category | flops | bytes accessed | tf_op | source)
XLA Modules:
  0.0 247.3 jit_solution(13279802603681400687)
XLA Ops:
  6.5 1.7 copy.22.v
  8.3 1.7 copy.23.g
  10.1 1.4 maximum_maximum_fusion.g
  11.5 2.0 shard_map.200
  13.5 3.0 %shard_map.199 = (bf16[4,800,128]{2,1,0:T(8,128)(2,1)}, bf16[768,128]{1,0:T(8,128)(2,1)}, bf16[768,128]{1,0:T(8,128)(2,1)}, bf16[768,128]{1,0:T(8,128)(2,1)}, bf16[768,128]{1,0:T(8,128)(2,1)}) custom-call(s32[1]{0:T(128)} %bitcast.2.slot_ref, bf16[768,128]{1,0:T(8,128)(2,1)} %ks.1, bf16[768,128]{1,0:T(8,128)(2,1)} %vs.1, bf16[768,128]{1,0:T(8,128)(2,1)} %kl.1, ...), custom_call_target="tpu_custom_call" | custom-call | flops 625000000 | tf_op jit(solution)/shard_map/pallas_call | solution.py:89
  16.5 5.0 %all-to-all-start = ((bf16[4,800,128]{2,1,0:T(8,128)(2,1)}), bf16[4,800,128]{2,1,0:T(8,128)(2,1)S(1)}, u32[]{:S(2)}, u32[]{:S(2)}) async-start(bf16[4,800,128]{2,1,0:T(8,128)(2,1)} %get-tuple-element.64), calls=%async_computation | async-start | bytes 1638400 | tf_op jit(solution)/shard_map/all_to_all | solution.py:633
  21.6 2.8 %collective-permute-start.6 = (bf16[256,2048]{1,0:T(8,128)(2,1)S(1)}, bf16[256,2048]{1,0:T(8,128)(2,1)S(1)}, u32[]{:S(2)}, u32[]{:S(2)}) collective-permute-start(bf16[256,2048]{1,0:T(8,128)(2,1)S(1)} %constant_dynamic-update-slice_fusion.refs_0_), channel_id=1, source_target_pairs={{0,6},{2,0},{4,2},{6,4},{1,7},{3,1},{5,3},{7,5},{8,14},{10,8},{12,... | collective-permute-start | bytes 3145736 | tf_op jit(solution)/shard_map/ppermute | solution.py:24
  24.4 1.2 collective-permute-start
  26.2 2.1 collective-permute-start.2
  28.3 10.4 %collective-permute-done.refs_3_ = bf16[768,128]{1,0:T(8,128)(2,1)S(1)} collective-permute-done((bf16[768,128]{1,0:T(8,128)(2,1)}, bf16[768,128]{1,0:T(8,128)(2,1)S(1)}, u32[]{:S(2)}, u32[]{:S(2)}) %collective-permute-start) | collective-permute-done | bytes 196640 | tf_op jit(solution)/shard_map/ppermute | solution.py:24
  38.7 1.2 collective-permute-done.1.refs_4_
  39.9 3.3 %collective-permute-done.2.refs_5_ = bf16[768,128]{1,0:T(8,128)(2,1)S(1)} collective-permute-done((bf16[768,128]{1,0:T(8,128)(2,1)S(1)}, bf16[768,128]{1,0:T(8,128)(2,1)S(1)}, u32[]{:S(2)}, u32[]{:S(2)}) %collective-permute-start.2) | collective-permute-done | bytes 196640 | tf_op jit(solution)/shard_map/ppermute | solution.py:24
  43.2 2.5 %collective-permute-start.4 = (bf16[4,800,128]{2,1,0:T(8,128)(2,1)S(1)}, bf16[4,800,128]{2,1,0:T(8,128)(2,1)}, u32[]{:S(2)}, u32[]{:S(2)}) collective-permute-start(bf16[4,800,128]{2,1,0:T(8,128)(2,1)S(1)} %all-to-all-done.refs_6_), channel_id=1, source_target_pairs={{0,24},{8,0},{16,8},{24,16},{1,25},{9,1},{17,9},{25,17},{2,26},{10... | collective-permute-start | bytes 2457608 | tf_op jit(solution)/shard_map/ppermute | solution.py:24
  45.7 0.7 pad_add_fusion.1.refs_0_
  46.4 11.7 %shard_map.201 = (f32[4,144,768]{2,1,0:T(8,128)}, f32[4,8,768]{2,1,0:T(8,128)}) custom-call(s32[2]{0:T(128)} %pad_add_fusion.1.refs_0_, s32[4,34]{1,0:T(4,128)} %constant.23.clone.refs_1_, bf16[768,128]{1,0:T(8,128)(2,1)} %get-tuple-element.69.refs_2_, bf16[768,128]{1,0:T(8,128)(2,1)} %copy-done.36, bf16[768,128]{1,0:T(8,128)(2,1)} %copy-done.37, ...), custom_call_target="tpu_custom_call" | custom-call | flops 3000000000 | tf_op jit(solution)/shard_map/pallas_call | solution.py:346
  58.1 9.9 %collective-permute-done.4.refs_7_ = bf16[4,800,128]{2,1,0:T(8,128)(2,1)} collective-permute-done((bf16[4,800,128]{2,1,0:T(8,128)(2,1)S(1)}, bf16[4,800,128]{2,1,0:T(8,128)(2,1)}, u32[]{:S(2)}, u32[]{:S(2)}) %collective-permute-start.4) | collective-permute-done | bytes 819232 | tf_op jit(solution)/shard_map/ppermute | solution.py:24
  68.0 2.7 %collective-permute-done.3.refs_6_ = bf16[4,800,128]{2,1,0:T(8,128)(2,1)} collective-permute-done((bf16[4,800,128]{2,1,0:T(8,128)(2,1)S(1)}, bf16[4,800,128]{2,1,0:T(8,128)(2,1)}, u32[]{:S(2)}, u32[]{:S(2)}) %collective-permute-start.3) | collective-permute-done | bytes 819232 | tf_op jit(solution)/shard_map/ppermute | solution.py:24
  71.4 1.0 slice.13
  72.4 1.0 slice.12
  73.5 2.7 %collective-permute-start.8 = (bf16[2,800,128]{2,1,0:T(8,128)(2,1)S(1)}, bf16[2,800,128]{2,1,0:T(8,128)(2,1)S(1)}, u32[]{:S(2)}, u32[]{:S(2)}) collective-permute-start(bf16[2,800,128]{2,1,0:T(8,128)(2,1)S(1)} %slice.13), channel_id=1, source_target_pairs={{0,24},{8,0},{16,8},{24,16},{1,25},{9,1},{17,9},{25,17},{2,26},{10... | collective-permute-start | bytes 1228808 | tf_op jit(solution)/shard_map/ppermute | solution.py:24
  76.2 14.1 %shard_map.202 = (f32[4,144,768]{2,1,0:T(8,128)}, f32[4,8,768]{2,1,0:T(8,128)}) custom-call(s32[2]{0:T(128)} %pad_add_fusion.1.refs_0_, s32[4,64]{1,0:T(4,128)} %constant.24.clone.refs_1_, bf16[768,128]{1,0:T(8,128)(2,1)} %get-tuple-element.69.refs_2_, bf16[768,128]{1,0:T(8,128)(2,1)} %copy-done.36, bf16[768,128]{1,0:T(8,128)(2,1)} %copy-done.37, ...), custom_call_target="tpu_custom_call" | custom-call | flops 6000000000 | tf_op jit(solution)/shard_map/pallas_call | solution.py:346
  90.3 2.7 %collective-permute-done.7.refs_6_ = bf16[2,800,128]{2,1,0:T(8,128)(2,1)S(1)} collective-permute-done((bf16[2,800,128]{2,1,0:T(8,128)(2,1)S(1)}, bf16[2,800,128]{2,1,0:T(8,128)(2,1)S(1)}, u32[]{:S(2)}, u32[]{:S(2)}) %collective-permute-start.7) | collective-permute-done | bytes 409632 | tf_op jit(solution)/shard_map/ppermute | solution.py:24
  93.0 0.7 copy-done.34
  93.9 9.3 %shard_map.203 = bf16[32,112,128]{2,1,0:T(8,128)(2,1)} custom-call(s32[2]{0:T(128)} %pad_add_fusion.1.refs_0_, s32[4,34]{1,0:T(4,128)} %constant.25.clone.refs_1_, bf16[768,128]{1,0:T(8,128)(2,1)} %get-tuple-element.69.refs_2_, bf16[768,128]{1,0:T(8,128)(2,1)} %copy-done.36, bf16[768,128]{1,0:T(8,128)(2,1)} %copy-done.37, bf16[768,128]{1,0:T(8,128)(2,1)} %copy-done.38, ...), custom_call_target="tpu_custom_call" | custom-call | flops 3000000000 | tf_op jit(solution)/shard_map/pallas_call | solution.py:346
  103.2 12.9 %all-gather.2.cloned.1.call-done.refs_2_.refs_3_.refs_4_.refs_5_ = bf16[2048,2304]{1,0:T(8,128)(2,1)} async-done(((bf16[128,2304]{1,0:T(8,128)(2,1)}), bf16[2048,2304]{1,0:T(8,128)(2,1)}) %all-gather.2.cloned.1.call-update) | async-done | bytes 9437200 | tf_op jit(solution)/shard_map/all_gather | solution.py:632
  117.2 11.7 %all-to-all-start.1 = ((bf16[32,112,128]{2,1,0:T(8,128)(2,1)}), bf16[32,112,128]{2,1,0:T(8,128)(2,1)S(1)}, u32[]{:S(2)}, u32[]{:S(2)}) async-start(bf16[32,112,128]{2,1,0:T(8,128)(2,1)} %shard_map.203), calls=%async_computation.1 | async-start | bytes 1835008 | tf_op jit(solution)/shard_map/all_to_all | solution.py:664
  128.9 14.1 %all-to-all-done.1.arrived_ref = bf16[32,112,128]{2,1,0:T(8,128)(2,1)S(1)} async-done(((bf16[32,112,128]{2,1,0:T(8,128)(2,1)}), bf16[32,112,128]{2,1,0:T(8,128)(2,1)S(1)}, u32[]{:S(2)}, u32[]{:S(2)}) %all-to-all-start.1) | async-done | bytes 917536 | tf_op jit(solution)/shard_map/all_to_all | solution.py:664
  143.1 1.0 copy-done.19
  144.1 4.9 %shard_map.204.refs_0_ = bf16[96,2048]{1,0:T(8,128)(2,1)S(1)} custom-call(s32[2]{0:T(128)S(1)} %pad_add_fusion.place_ref, bf16[32,112,128]{2,1,0:T(8,128)(2,1)S(1)} %all-to-all-done.1.arrived_ref, bf16[256,2048]{1,0:T(8,128)(2,1)S(1)} %constant_dynamic-update-slice_fusion.refs_0_, bf16[256,2048]{1,0:T(8,128)(2,1)} %collective-permute-done.5.refs_1_, ...), custom_call_target="tpu_custom_call" | custom-call | flops 1250000000 | tf_op jit(solution)/shard_map/pallas_call | solution.py:396
  149.1 1.9 collective-permute-start.16
  151.0 1.4 shard_map.205
  152.4 7.0 %collective-permute-done.16.refs_1_ = bf16[96,2048]{1,0:T(8,128)(2,1)S(1)} collective-permute-done((bf16[96,2048]{1,0:T(8,128)(2,1)S(1)}, bf16[96,2048]{1,0:T(8,128)(2,1)S(1)}, u32[]{:S(2)}, u32[]{:S(2)}) %collective-permute-start.16) | collective-permute-done | bytes 393248 | tf_op jit(solution)/shard_map/ppermute | solution.py:24
  159.4 2.8 %collective-permute-done.15.refs_0_ = bf16[96,2048]{1,0:T(8,128)(2,1)S(1)} collective-permute-done((bf16[96,2048]{1,0:T(8,128)(2,1)S(1)}, bf16[96,2048]{1,0:T(8,128)(2,1)S(1)}, u32[]{:S(2)}, u32[]{:S(2)}) %collective-permute-start.15) | collective-permute-done | bytes 393248 | tf_op jit(solution)/shard_map/ppermute | solution.py:24
  162.2 1.6 collective-permute-start.17
  163.9 1.5 collective-permute-start.19
  165.7 2.6 %shard_map.206 = (bf16[384,704]{1,0:T(8,128)(2,1)S(1)}, bf16[384,704]{1,0:T(8,128)(2,1)S(1)}) custom-call(bf16[96,2048]{1,0:T(8,128)(2,1)S(1)} %collective-permute-done.15.refs_0_, bf16[96,2048]{1,0:T(8,128)(2,1)S(1)} %collective-permute-done.16.refs_1_, bf16[96,2048]{1,0:T(8,128)(2,1)S(1)} %collective-permute-done.17.refs_2_, ...), custom_call_target="tpu_custom_call" | custom-call | flops 1000000000 | tf_op jit(solution)/shard_map/pallas_call | solution.py:447
  168.3 1.5 collective-permute-done.20.refs_1_
  169.8 1.1 collective-permute-done.19.refs_0_
  170.9 1.6 collective-permute-start.21
  172.5 1.1 collective-permute-done.21.refs_2_
  173.9 1.4 shard_map.207
  175.3 0.7 copy-done.10
  176.0 0.8 copy-done.12
  176.8 2.5 shard_map.208
  179.3 4.8 %collective-permute-start.23 = (bf16[32,704]{1,0:T(8,128)(2,1)}, bf16[32,704]{1,0:T(8,128)(2,1)S(1)}, u32[]{:S(2)}, u32[]{:S(2)}) collective-permute-start(bf16[32,704]{1,0:T(8,128)(2,1)} %get-tuple-element.106), channel_id=1, source_target_pairs={{0,8},{8,16},{16,24},{24,32},{32,40},{40,48},{48,56},{56,64},{64,7... | collective-permute-start | bytes 135176 | tf_op jit(solution)/shard_map/ppermute | solution.py:30
  184.1 12.1 %collective-permute-done.23.refs_3_ = bf16[32,704]{1,0:T(8,128)(2,1)S(1)} collective-permute-done((bf16[32,704]{1,0:T(8,128)(2,1)}, bf16[32,704]{1,0:T(8,128)(2,1)S(1)}, u32[]{:S(2)}, u32[]{:S(2)}) %collective-permute-start.23) | collective-permute-done | bytes 45088 | tf_op jit(solution)/shard_map/ppermute | solution.py:30
  196.3 0.9 copy-done.15
  197.2 0.9 copy-done.17
  198.1 4.3 %shard_map.209 = (bf16[1,96,2048]{2,1,0:T(8,128)(2,1)S(1)}, f32[1,96,2048]{2,1,0:T(8,128)S(1)}) custom-call(s32[2]{0:T(128)S(1)} %copy-done.23, f32[3,704]{1,0:T(4,128)S(1)} %copy-done.20, f32[3,704]{1,0:T(4,128)S(1)} %copy-done.21, bf16[2048,2304]{1,0:T(8,128)(2,1)} %all-gather.2.cloned.1.call-done.refs_2_.refs_3_.refs_4_.refs_5_, ...), custom_call_target="tpu_custom_call" | custom-call | flops 1000000000 | tf_op jit(solution)/shard_map/pallas_call | solution.py:533
  202.4 0.9 copy-done.14
  203.3 0.9 collective-permute-start.24
  204.2 1.3 collective-permute-done.24.their_ref
  205.5 0.7 copy-done.30
  206.3 2.1 shard_map.210
  208.4 7.1 %shard_map.211 = (bf16[3,96,2048]{2,1,0:T(8,128)(2,1)S(1)}, f32[3,96,2048]{2,1,0:T(8,128)}) custom-call(s32[2]{0:T(128)S(1)} %copy-done.23, f32[3,704]{1,0:T(4,128)S(1)} %copy-done.20, f32[3,704]{1,0:T(4,128)S(1)} %copy-done.21, bf16[2048,2304]{1,0:T(8,128)(2,1)} %all-gather.2.cloned.1.call-done.refs_2_.refs_3_.refs_4_.refs_5_, ...), custom_call_target="tpu_custom_call" | custom-call | flops 2000000000 | tf_op jit(solution)/shard_map/pallas_call | solution.py:533
  216.5 2.0 collective-permute-done.25.their_ref
  218.4 1.0 copy-done.25
  219.5 3.2 %shard_map.212 = (f32[96,2048]{1,0:T(8,128)}, bf16[96,2048]{1,0:T(8,128)(2,1)}, bf16[96,2048]{1,0:T(8,128)(2,1)}) custom-call(f32[3,96,2048]{2,1,0:T(8,128)} %get-tuple-element.115.mine_ref, bf16[3,96,2048]{2,1,0:T(8,128)(2,1)} %copy-done.25), custom_call_target="tpu_custom_call" | custom-call | flops 525000000 | tf_op jit(solution)/shard_map/pallas_call | solution.py:558
  222.8 1.4 collective-permute-start.28
  224.1 3.9 %collective-permute-done.26.refs_2_ = bf16[96,2048]{1,0:T(8,128)(2,1)S(1)} collective-permute-done((bf16[96,2048]{1,0:T(8,128)(2,1)S(1)}, bf16[96,2048]{1,0:T(8,128)(2,1)S(1)}, u32[]{:S(2)}, u32[]{:S(2)}) %collective-permute-start.26) | collective-permute-done | bytes 393248 | tf_op jit(solution)/shard_map/ppermute | solution.py:24
  228.0 6.0 %collective-permute-done.27.refs_3_ = bf16[96,2048]{1,0:T(8,128)(2,1)S(1)} collective-permute-done((bf16[96,2048]{1,0:T(8,128)(2,1)}, bf16[96,2048]{1,0:T(8,128)(2,1)S(1)}, u32[]{:S(2)}, u32[]{:S(2)}) %collective-permute-start.27) | collective-permute-done | bytes 393248 | tf_op jit(solution)/shard_map/ppermute | solution.py:24
  234.0 2.9 %collective-permute-done.28.refs_4_ = bf16[96,2048]{1,0:T(8,128)(2,1)S(1)} collective-permute-done((bf16[96,2048]{1,0:T(8,128)(2,1)}, bf16[96,2048]{1,0:T(8,128)(2,1)S(1)}, u32[]{:S(2)}, u32[]{:S(2)}) %collective-permute-start.28) | collective-permute-done | bytes 393248 | tf_op jit(solution)/shard_map/ppermute | solution.py:24
  236.9 0.8 copy-done.33
  237.7 2.8 %shard_map.213 = bf16[96,2048]{1,0:T(8,128)(2,1)} custom-call(bf16[96,2048]{1,0:T(8,128)(2,1)} %copy-done.1, f32[96,2048]{1,0:T(8,128)} %get-tuple-element.117.refs_1_, bf16[96,2048]{1,0:T(8,128)(2,1)} %copy-done.31, bf16[96,2048]{1,0:T(8,128)(2,1)} %copy-done.32, bf16[96,2048]{1,0:T(8,128)(2,1)} %copy-done.33, f32[1,2048]{1,0:T(1,128)} %bitcast.9), custom_call_target="tpu_custom_call" | custom-call | flops 500000000 | tf_op jit(solution)/shard_map/pallas_call | solution.py:583
  (109 shorter events, 4.8 us)
Async XLA Ops:
  6.5 109.6 %all-gather.2.cloned.1.call-start = ((), (), s32[]{:S(2)}) async-start(), calls=%async_computation.2 | async-start | bytes 10027008 | tf_op jit(solution)/shard_map/all_gather | solution.py:632
  13.5 8.0 %copy-start.27 = (bf16[128,2048]{1,0:T(8,128)(2,1)S(1)}, bf16[128,2048]{1,0:T(8,128)(2,1)}, u32[]{:S(2)}) copy-start(bf16[128,2048]{1,0:T(8,128)(2,1)} %param.30) | copy-start | bytes 1572868
  16.5 5.1 %copy-start.28 = (bf16[128,2048]{1,0:T(8,128)(2,1)S(1)}, bf16[128,2048]{1,0:T(8,128)(2,1)}, u32[]{:S(2)}) copy-start(bf16[128,2048]{1,0:T(8,128)(2,1)} %param.31) | copy-start | bytes 1572868
  16.5 26.6 %all-to-all-start = ((bf16[4,800,128]{2,1,0:T(8,128)(2,1)}), bf16[4,800,128]{2,1,0:T(8,128)(2,1)S(1)}, u32[]{:S(2)}, u32[]{:S(2)}) async-start(bf16[4,800,128]{2,1,0:T(8,128)(2,1)} %get-tuple-element.64), calls=%async_computation | async-start | bytes 1638400 | tf_op jit(solution)/shard_map/all_to_all | solution.py:633
  21.5 4.7 %copy-start.39 = (bf16[768,128]{1,0:T(8,128)(2,1)S(1)}, bf16[768,128]{1,0:T(8,128)(2,1)}, u32[]{:S(2)}) copy-start(bf16[768,128]{1,0:T(8,128)(2,1)} %get-tuple-element.68) | copy-start | bytes 589828
  21.6 36.5 %collective-permute-start.6 = (bf16[256,2048]{1,0:T(8,128)(2,1)S(1)}, bf16[256,2048]{1,0:T(8,128)(2,1)S(1)}, u32[]{:S(2)}, u32[]{:S(2)}) collective-permute-start(bf16[256,2048]{1,0:T(8,128)(2,1)S(1)} %constant_dynamic-update-slice_fusion.refs_0_), channel_id=1, source_target_pairs={{0,6},{2,0},{4,2},{6,4},{1,7},{3,1},{5,3},{7,5},{8,14},{10,8},{12,... | collective-permute-start | bytes 3145736 | tf_op jit(solution)/shard_map/ppermute | solution.py:24
  24.4 33.7 %collective-permute-start.5 = (bf16[256,2048]{1,0:T(8,128)(2,1)S(1)}, bf16[256,2048]{1,0:T(8,128)(2,1)}, u32[]{:S(2)}, u32[]{:S(2)}) collective-permute-start(bf16[256,2048]{1,0:T(8,128)(2,1)S(1)} %constant_dynamic-update-slice_fusion.refs_0_), channel_id=1, source_target_pairs={{0,2},{2,4},{4,6},{6,0},{1,3},{3,5},{5,7},{7,1},{8,10},{10,12},{12... | collective-permute-start | bytes 3145736 | tf_op jit(solution)/shard_map/ppermute | solution.py:24
  24.4 14.2 %collective-permute-start = (bf16[768,128]{1,0:T(8,128)(2,1)}, bf16[768,128]{1,0:T(8,128)(2,1)S(1)}, u32[]{:S(2)}, u32[]{:S(2)}) collective-permute-start(bf16[768,128]{1,0:T(8,128)(2,1)} %get-tuple-element.66), channel_id=1, source_target_pairs={{0,32},{32,64},{64,96},{96,0},{1,33},{33,65},{65,97},{97,1},{2,34}... | collective-permute-start | bytes 589832 | tf_op jit(solution)/shard_map/ppermute | solution.py:24
  25.6 14.3 %collective-permute-start.1 = (bf16[768,128]{1,0:T(8,128)(2,1)}, bf16[768,128]{1,0:T(8,128)(2,1)S(1)}, u32[]{:S(2)}, u32[]{:S(2)}) collective-permute-start(bf16[768,128]{1,0:T(8,128)(2,1)} %get-tuple-element.67), channel_id=1, source_target_pairs={{0,64},{32,96},{64,0},{96,32},{1,65},{33,97},{65,1},{97,33},{2,66}... | collective-permute-start | bytes 589832 | tf_op jit(solution)/shard_map/ppermute | solution.py:24
  26.2 16.9 %collective-permute-start.2 = (bf16[768,128]{1,0:T(8,128)(2,1)S(1)}, bf16[768,128]{1,0:T(8,128)(2,1)S(1)}, u32[]{:S(2)}, u32[]{:S(2)}) collective-permute-start(bf16[768,128]{1,0:T(8,128)(2,1)S(1)} %copy-done.39), channel_id=1, source_target_pairs={{0,96},{32,0},{64,32},{96,64},{1,97},{33,1},{65,33},{97,65},{2,98}... | collective-permute-start | bytes 589832 | tf_op jit(solution)/shard_map/ppermute | solution.py:24
  38.7 7.7 %copy-start.36 = (bf16[768,128]{1,0:T(8,128)(2,1)}, bf16[768,128]{1,0:T(8,128)(2,1)S(1)}, u32[]{:S(2)}) copy-start(bf16[768,128]{1,0:T(8,128)(2,1)S(1)} %collective-permute-done.refs_3_) | copy-start | bytes 589828
  39.9 6.5 %copy-start.37 = (bf16[768,128]{1,0:T(8,128)(2,1)}, bf16[768,128]{1,0:T(8,128)(2,1)S(1)}, u32[]{:S(2)}) copy-start(bf16[768,128]{1,0:T(8,128)(2,1)S(1)} %collective-permute-done.1.refs_4_) | copy-start | bytes 589828
  43.1 3.2 %copy-start.38 = (bf16[768,128]{1,0:T(8,128)(2,1)}, bf16[768,128]{1,0:T(8,128)(2,1)S(1)}, u32[]{:S(2)}) copy-start(bf16[768,128]{1,0:T(8,128)(2,1)S(1)} %collective-permute-done.2.refs_5_) | copy-start | bytes 589828
  43.2 3.2 %copy-start.26 = (bf16[4,800,128]{2,1,0:T(8,128)(2,1)}, bf16[4,800,128]{2,1,0:T(8,128)(2,1)S(1)}, u32[]{:S(2)}) copy-start(bf16[4,800,128]{2,1,0:T(8,128)(2,1)S(1)} %all-to-all-done.refs_6_) | copy-start | bytes 2457604
  43.2 24.9 %collective-permute-start.4 = (bf16[4,800,128]{2,1,0:T(8,128)(2,1)S(1)}, bf16[4,800,128]{2,1,0:T(8,128)(2,1)}, u32[]{:S(2)}, u32[]{:S(2)}) collective-permute-start(bf16[4,800,128]{2,1,0:T(8,128)(2,1)S(1)} %all-to-all-done.refs_6_), channel_id=1, source_target_pairs={{0,24},{8,0},{16,8},{24,16},{1,25},{9,1},{17,9},{25,17},{2,26},{10... | collective-permute-start | bytes 2457608 | tf_op jit(solution)/shard_map/ppermute | solution.py:24
  45.7 25.0 %collective-permute-start.3 = (bf16[4,800,128]{2,1,0:T(8,128)(2,1)S(1)}, bf16[4,800,128]{2,1,0:T(8,128)(2,1)}, u32[]{:S(2)}, u32[]{:S(2)}) collective-permute-start(bf16[4,800,128]{2,1,0:T(8,128)(2,1)S(1)} %all-to-all-done.refs_6_), channel_id=1, source_target_pairs={{0,8},{8,16},{16,24},{24,0},{1,9},{9,17},{17,25},{25,1},{2,10},{10... | collective-permute-start | bytes 2457608 | tf_op jit(solution)/shard_map/ppermute | solution.py:24
  70.7 32.5 %collective-permute-start.9 = (bf16[256,2048]{1,0:T(8,128)(2,1)}, bf16[256,2048]{1,0:T(8,128)(2,1)}, u32[]{:S(2)}, u32[]{:S(2)}) collective-permute-start(bf16[256,2048]{1,0:T(8,128)(2,1)} %collective-permute-done.5.refs_1_), channel_id=1, source_target_pairs={{0,2},{2,4},{4,6},{6,0},{1,3},{3,5},{5,7},{7,1},{8,10},{10,12},{12... | collective-permute-start | bytes 3145736 | tf_op jit(solution)/shard_map/ppermute | solution.py:24
  73.5 19.6 %collective-permute-start.7 = (bf16[2,800,128]{2,1,0:T(8,128)(2,1)S(1)}, bf16[2,800,128]{2,1,0:T(8,128)(2,1)S(1)}, u32[]{:S(2)}, u32[]{:S(2)}) collective-permute-start(bf16[2,800,128]{2,1,0:T(8,128)(2,1)S(1)} %slice.12), channel_id=1, source_target_pairs={{0,8},{8,16},{16,24},{24,0},{1,9},{9,17},{17,25},{25,1},{2,10},{10... | collective-permute-start | bytes 1228808 | tf_op jit(solution)/shard_map/ppermute | solution.py:24
  73.5 19.5 %collective-permute-start.8 = (bf16[2,800,128]{2,1,0:T(8,128)(2,1)S(1)}, bf16[2,800,128]{2,1,0:T(8,128)(2,1)S(1)}, u32[]{:S(2)}, u32[]{:S(2)}) collective-permute-start(bf16[2,800,128]{2,1,0:T(8,128)(2,1)S(1)} %slice.13), channel_id=1, source_target_pairs={{0,24},{8,0},{16,8},{24,16},{1,25},{9,1},{17,9},{25,17},{2,26},{10... | collective-permute-start | bytes 1228808 | tf_op jit(solution)/shard_map/ppermute | solution.py:24
  103.2 39.9 %copy-start.24 = (f32[2048]{0:T(1024)S(1)}, f32[2048]{0:T(1024)}, u32[]{:S(2)}) copy-start(f32[2048]{0:T(1024)} %param.32) | copy-start | bytes 24580
  116.1 26.9 %collective-permute-start.10 = (bf16[256,2048]{1,0:T(8,128)(2,1)S(1)}, bf16[256,2048]{1,0:T(8,128)(2,1)}, u32[]{:S(2)}, u32[]{:S(2)}) collective-permute-start(bf16[256,2048]{1,0:T(8,128)(2,1)S(1)} %constant_dynamic-update-slice_fusion.refs_0_), channel_id=1, source_target_pairs={{0,1},{1,0},{2,3},{3,2},{4,5},{5,4},{6,7},{7,6},{8,9},{9,8},{10,11... | collective-permute-start | bytes 3145736 | tf_op jit(solution)/shard_map/ppermute | solution.py:24
  116.7 26.4 %collective-permute-start.11 = (bf16[256,2048]{1,0:T(8,128)(2,1)}, bf16[256,2048]{1,0:T(8,128)(2,1)}, u32[]{:S(2)}, u32[]{:S(2)}) collective-permute-start(bf16[256,2048]{1,0:T(8,128)(2,1)} %collective-permute-done.5.refs_1_), channel_id=1, source_target_pairs={{0,1},{1,0},{2,3},{3,2},{4,5},{5,4},{6,7},{7,6},{8,9},{9,8},{10,11... | collective-permute-start | bytes 3145736 | tf_op jit(solution)/shard_map/ppermute | solution.py:24
  116.7 26.4 %collective-permute-start.12 = (bf16[256,2048]{1,0:T(8,128)(2,1)S(1)}, bf16[256,2048]{1,0:T(8,128)(2,1)}, u32[]{:S(2)}, u32[]{:S(2)}) collective-permute-start(bf16[256,2048]{1,0:T(8,128)(2,1)S(1)} %collective-permute-done.6.refs_2_), channel_id=1, source_target_pairs={{0,1},{1,0},{2,3},{3,2},{4,5},{5,4},{6,7},{7,6},{8,9},{9,8},{10,11... | collective-permute-start | bytes 3145736 | tf_op jit(solution)/shard_map/ppermute | solution.py:24
  117.2 25.9 %collective-permute-start.13 = (bf16[256,2048]{1,0:T(8,128)(2,1)}, bf16[256,2048]{1,0:T(8,128)(2,1)}, u32[]{:S(2)}, u32[]{:S(2)}) collective-permute-start(bf16[256,2048]{1,0:T(8,128)(2,1)} %collective-permute-done.9.refs_3_), channel_id=1, source_target_pairs={{0,1},{1,0},{2,3},{3,2},{4,5},{5,4},{6,7},{7,6},{8,9},{9,8},{10,11... | collective-permute-start | bytes 3145736 | tf_op jit(solution)/shard_map/ppermute | solution.py:24
  117.2 25.8 %all-to-all-start.1 = ((bf16[32,112,128]{2,1,0:T(8,128)(2,1)}), bf16[32,112,128]{2,1,0:T(8,128)(2,1)S(1)}, u32[]{:S(2)}, u32[]{:S(2)}) async-start(bf16[32,112,128]{2,1,0:T(8,128)(2,1)} %shard_map.203), calls=%async_computation.1 | async-start | bytes 1835008 | tf_op jit(solution)/shard_map/all_to_all | solution.py:664
  128.9 20.0 %copy-start.22 = (s32[2]{0:T(128)}, s32[2]{0:T(128)S(1)}, u32[]{:S(2)}) copy-start(s32[2]{0:T(128)S(1)} %pad_add_fusion.place_ref) | copy-start | bytes 28
  143.1 1.0 copy-start.19
  144.1 6.9 %copy-start = (bf16[2048,2304]{1,0:T(8,128)(2,1)S(1)}, bf16[2048,2304]{1,0:T(8,128)(2,1)}, u32[]{:S(2)}) copy-start(bf16[2048,2304]{1,0:T(8,128)(2,1)} %all-gather.2.cloned.1.call-done.refs_2_.refs_3_.refs_4_.refs_5_) | copy-start | bytes 28311556
  149.0 3.4 %copy-start.1 = (bf16[96,2048]{1,0:T(8,128)(2,1)}, bf16[96,2048]{1,0:T(8,128)(2,1)S(1)}, u32[]{:S(2)}) copy-start(bf16[96,2048]{1,0:T(8,128)(2,1)S(1)} %shard_map.204.refs_0_) | copy-start | bytes 1179652
  149.0 2.0 collective-permute-start.14
  149.1 10.3 %collective-permute-start.16 = (bf16[96,2048]{1,0:T(8,128)(2,1)S(1)}, bf16[96,2048]{1,0:T(8,128)(2,1)S(1)}, u32[]{:S(2)}, u32[]{:S(2)}) collective-permute-start(bf16[96,2048]{1,0:T(8,128)(2,1)S(1)} %shard_map.204.refs_0_), channel_id=1, source_target_pairs={{0,6},{2,0},{4,2},{6,4},{1,7},{3,1},{5,3},{7,5},{8,14},{10,8},{12,... | collective-permute-start | bytes 1179656 | tf_op jit(solution)/shard_map/ppermute | solution.py:24
  151.0 11.2 %collective-permute-start.15 = (bf16[96,2048]{1,0:T(8,128)(2,1)S(1)}, bf16[96,2048]{1,0:T(8,128)(2,1)S(1)}, u32[]{:S(2)}, u32[]{:S(2)}) collective-permute-start(bf16[96,2048]{1,0:T(8,128)(2,1)S(1)} %shard_map.204.refs_0_), channel_id=1, source_target_pairs={{0,2},{2,4},{4,6},{6,0},{1,3},{3,5},{5,7},{7,1},{8,10},{10,12},{12... | collective-permute-start | bytes 1179656 | tf_op jit(solution)/shard_map/ppermute | solution.py:24
  152.4 15.8 %copy-start.6 = (bf16[192,704]{1,0:T(8,128)(2,1)}, bf16[192,704]{1,0:T(8,128)(2,1)S(1)}, u32[]{:S(2)}) copy-start(bf16[192,704]{1,0:T(8,128)(2,1)S(1)} %get-tuple-element.111.refs_0_.refs_6_) | copy-start | bytes 811012
  152.4 15.8 %copy-start.8 = (bf16[192,704]{1,0:T(8,128)(2,1)}, bf16[192,704]{1,0:T(8,128)(2,1)S(1)}, u32[]{:S(2)}) copy-start(bf16[192,704]{1,0:T(8,128)(2,1)S(1)} %get-tuple-element.112.refs_1_.refs_7_) | copy-start | bytes 811012
  162.2 3.1 %collective-permute-start.17 = (bf16[96,2048]{1,0:T(8,128)(2,1)S(1)}, bf16[96,2048]{1,0:T(8,128)(2,1)S(1)}, u32[]{:S(2)}, u32[]{:S(2)}) collective-permute-start(bf16[96,2048]{1,0:T(8,128)(2,1)S(1)} %collective-permute-done.15.refs_0_), channel_id=1, source_target_pairs={{0,1},{1,0},{2,3},{3,2},{4,5},{5,4},{6,7},{7,6},{8,9},{9,8},{10,11... | collective-permute-start | bytes 1179656 | tf_op jit(solution)/shard_map/ppermute | solution.py:24
  163.7 1.9 collective-permute-start.18
  163.8 6.0 %collective-permute-start.20 = (bf16[48,2048]{1,0:T(8,128)(2,1)S(1)}, bf16[48,2048]{1,0:T(8,128)(2,1)S(1)}, u32[]{:S(2)}, u32[]{:S(2)}) collective-permute-start(bf16[48,2048]{1,0:T(8,128)(2,1)S(1)} %slice.15), channel_id=1, source_target_pairs={{0,6},{2,0},{4,2},{6,4},{1,7},{3,1},{5,3},{7,5},{8,14},{10,8},{12,... | collective-permute-start | bytes 589832 | tf_op jit(solution)/shard_map/ppermute | solution.py:24
  163.9 7.0 %collective-permute-start.19 = (bf16[48,2048]{1,0:T(8,128)(2,1)S(1)}, bf16[48,2048]{1,0:T(8,128)(2,1)S(1)}, u32[]{:S(2)}, u32[]{:S(2)}) collective-permute-start(bf16[48,2048]{1,0:T(8,128)(2,1)S(1)} %slice.14), channel_id=1, source_target_pairs={{0,2},{2,4},{4,6},{6,0},{1,3},{3,5},{5,7},{7,1},{8,10},{10,12},{12... | collective-permute-start | bytes 589832 | tf_op jit(solution)/shard_map/ppermute | solution.py:24
  168.3 7.0 %copy-start.2 = (bf16[384,704]{1,0:T(8,128)(2,1)}, bf16[384,704]{1,0:T(8,128)(2,1)S(1)}, u32[]{:S(2)}) copy-start(bf16[384,704]{1,0:T(8,128)(2,1)S(1)} %get-tuple-element.113.refs_2_.refs_8_) | copy-start | bytes 1622020
  168.3 7.0 %copy-start.4 = (bf16[384,704]{1,0:T(8,128)(2,1)}, bf16[384,704]{1,0:T(8,128)(2,1)S(1)}, u32[]{:S(2)}) copy-start(bf16[384,704]{1,0:T(8,128)(2,1)S(1)} %get-tuple-element.114.refs_3_.refs_9_) | copy-start | bytes 1622020
  170.9 2.6 %collective-permute-start.21 = (bf16[48,2048]{1,0:T(8,128)(2,1)S(1)}, bf16[48,2048]{1,0:T(8,128)(2,1)S(1)}, u32[]{:S(2)}, u32[]{:S(2)}) collective-permute-start(bf16[48,2048]{1,0:T(8,128)(2,1)S(1)} %collective-permute-done.19.refs_0_), channel_id=1, source_target_pairs={{0,1},{1,0},{2,3},{3,2},{4,5},{5,4},{6,7},{7,6},{8,9},{9,8},{10,11... | collective-permute-start | bytes 589832 | tf_op jit(solution)/shard_map/ppermute | solution.py:24
  172.5 1.4 collective-permute-start.22
  176.8 19.5 %copy-start.20 = (f32[3,704]{1,0:T(4,128)S(1)}, f32[3,704]{1,0:T(4,128)}, u32[]{:S(2)}) copy-start(f32[3,704]{1,0:T(4,128)} %refs_0_.3) | copy-start | bytes 25348
  176.8 19.5 %copy-start.21 = (f32[3,704]{1,0:T(4,128)S(1)}, f32[3,704]{1,0:T(4,128)}, u32[]{:S(2)}) copy-start(f32[3,704]{1,0:T(4,128)} %refs_1_.6) | copy-start | bytes 25348
  176.8 19.5 %copy-start.23 = (s32[2]{0:T(128)S(1)}, s32[2]{0:T(128)}, u32[]{:S(2)}) copy-start(s32[2]{0:T(128)} %copy-done.22) | copy-start | bytes 28
  176.8 19.5 %copy-start.11 = (bf16[192,704]{1,0:T(8,128)(2,1)S(1)}, bf16[192,704]{1,0:T(8,128)(2,1)}, u32[]{:S(2)}) copy-start(bf16[192,704]{1,0:T(8,128)(2,1)} %copy-done.10) | copy-start | bytes 811012
  176.8 19.5 %copy-start.13 = (bf16[192,704]{1,0:T(8,128)(2,1)S(1)}, bf16[192,704]{1,0:T(8,128)(2,1)}, u32[]{:S(2)}) copy-start(bf16[192,704]{1,0:T(8,128)(2,1)} %copy-done.12) | copy-start | bytes 811012
  179.3 17.0 %collective-permute-start.23 = (bf16[32,704]{1,0:T(8,128)(2,1)}, bf16[32,704]{1,0:T(8,128)(2,1)S(1)}, u32[]{:S(2)}, u32[]{:S(2)}) collective-permute-start(bf16[32,704]{1,0:T(8,128)(2,1)} %get-tuple-element.106), channel_id=1, source_target_pairs={{0,8},{8,16},{16,24},{24,32},{32,40},{40,48},{48,56},{56,64},{64,7... | collective-permute-start | bytes 135176 | tf_op jit(solution)/shard_map/ppermute | solution.py:30
  196.3 0.9 copy-start.15
  198.1 10.3 %copy-start.9 = (bf16[192,704]{1,0:T(8,128)(2,1)S(1)}, bf16[192,704]{1,0:T(8,128)(2,1)}, u32[]{:S(2)}) copy-start(bf16[192,704]{1,0:T(8,128)(2,1)} %copy-done.8) | copy-start | bytes 811012
  198.1 10.3 %copy-start.16 = (bf16[8,16,704]{2,1,0:T(8,128)(2,1)S(1)}, bf16[8,16,704]{2,1,0:T(8,128)(2,1)}, u32[]{:S(2)}) copy-start(bf16[8,16,704]{2,1,0:T(8,128)(2,1)} %get-tuple-element.107.refs_4_) | copy-start | bytes 540676
  198.1 10.3 %copy-start.18 = (bf16[8,16,704]{2,1,0:T(8,128)(2,1)S(1)}, bf16[8,16,704]{2,1,0:T(8,128)(2,1)}, u32[]{:S(2)}) copy-start(bf16[8,16,704]{2,1,0:T(8,128)(2,1)} %get-tuple-element.108.refs_5_) | copy-start | bytes 540676
  203.3 5.1 %copy-start.3 = (bf16[384,704]{1,0:T(8,128)(2,1)S(1)}, bf16[384,704]{1,0:T(8,128)(2,1)}, u32[]{:S(2)}) copy-start(bf16[384,704]{1,0:T(8,128)(2,1)} %copy-done.2) | copy-start | bytes 1622020
  203.3 5.1 %copy-start.5 = (bf16[384,704]{1,0:T(8,128)(2,1)S(1)}, bf16[384,704]{1,0:T(8,128)(2,1)}, u32[]{:S(2)}) copy-start(bf16[384,704]{1,0:T(8,128)(2,1)} %copy-done.4) | copy-start | bytes 1622020
  203.3 5.1 %copy-start.7 = (bf16[192,704]{1,0:T(8,128)(2,1)S(1)}, bf16[192,704]{1,0:T(8,128)(2,1)}, u32[]{:S(2)}) copy-start(bf16[192,704]{1,0:T(8,128)(2,1)} %copy-done.6) | copy-start | bytes 811012
  203.3 2.2 collective-permute-start.24
  208.4 7.5 %copy-start.29 = (bf16[96,2048]{1,0:T(8,128)(2,1)S(1)}, bf16[96,2048]{1,0:T(8,128)(2,1)}, u32[]{:S(2)}) copy-start(bf16[96,2048]{1,0:T(8,128)(2,1)} %shard_map.210) | copy-start | bytes 1179652
  215.6 2.9 %collective-permute-start.25 = (bf16[3,96,2048]{2,1,0:T(8,128)(2,1)S(1)}, bf16[3,96,2048]{2,1,0:T(8,128)(2,1)S(1)}, u32[]{:S(2)}, u32[]{:S(2)}) collective-permute-start(bf16[3,96,2048]{2,1,0:T(8,128)(2,1)S(1)} %get-tuple-element.116), channel_id=1, source_target_pairs={{0,1},{1,0},{2,3},{3,2},{4,5},{5,4},{6,7},{7,6},{8,9},{9,8},{10,11... | collective-permute-start | bytes 3538952 | tf_op jit(solution)/shard_map/ppermute | solution.py:24
  216.0 12.0 %collective-permute-start.26 = (bf16[96,2048]{1,0:T(8,128)(2,1)S(1)}, bf16[96,2048]{1,0:T(8,128)(2,1)S(1)}, u32[]{:S(2)}, u32[]{:S(2)}) collective-permute-start(bf16[96,2048]{1,0:T(8,128)(2,1)S(1)} %copy-done.29), channel_id=1, source_target_pairs={{0,4},{2,6},{4,0},{6,2},{1,5},{3,7},{5,1},{7,3},{8,12},{10,14},{12... | collective-permute-start | bytes 1179656 | tf_op jit(solution)/shard_map/ppermute | solution.py:24
  218.4 1.0 copy-start.25
  222.7 11.3 %collective-permute-start.27 = (bf16[96,2048]{1,0:T(8,128)(2,1)}, bf16[96,2048]{1,0:T(8,128)(2,1)S(1)}, u32[]{:S(2)}, u32[]{:S(2)}) collective-permute-start(bf16[96,2048]{1,0:T(8,128)(2,1)} %get-tuple-element.119), channel_id=1, source_target_pairs={{0,6},{2,0},{4,2},{6,4},{1,7},{3,1},{5,3},{7,5},{8,14},{10,8},{12,... | collective-permute-start | bytes 1179656 | tf_op jit(solution)/shard_map/ppermute | solution.py:24
  222.8 14.2 %collective-permute-start.28 = (bf16[96,2048]{1,0:T(8,128)(2,1)}, bf16[96,2048]{1,0:T(8,128)(2,1)S(1)}, u32[]{:S(2)}, u32[]{:S(2)}) collective-permute-start(bf16[96,2048]{1,0:T(8,128)(2,1)} %get-tuple-element.120), channel_id=1, source_target_pairs={{0,2},{2,4},{4,6},{6,0},{1,3},{3,5},{5,7},{7,1},{8,10},{10,12},{12... | collective-permute-start | bytes 1179656 | tf_op jit(solution)/shard_map/ppermute | solution.py:24
  228.0 8.9 %copy-start.31 = (bf16[96,2048]{1,0:T(8,128)(2,1)}, bf16[96,2048]{1,0:T(8,128)(2,1)S(1)}, u32[]{:S(2)}) copy-start(bf16[96,2048]{1,0:T(8,128)(2,1)S(1)} %collective-permute-done.26.refs_2_) | copy-start | bytes 1179652
  234.0 2.9 %copy-start.32 = (bf16[96,2048]{1,0:T(8,128)(2,1)}, bf16[96,2048]{1,0:T(8,128)(2,1)S(1)}, u32[]{:S(2)}) copy-start(bf16[96,2048]{1,0:T(8,128)(2,1)S(1)} %collective-permute-done.27.refs_3_) | copy-start | bytes 1179652
  (8 other events, 6.4 us)
Sparse Core Ops, SparseCore 0:
  16.6 99.4 all-gather.1
where the time goes:
time: 248 us; the launch traced here: 247 us
  waiting for transfers between devices  99.6 us (40%)
  Pallas kernels  72.4 us (29%)
  starting transfers between devices  45 us (18%)
  local copies, waits for them, and re-layouts  14.5 us (6%)
  between operations  13.8 us (6%)
    ppermute x28, waiting for transfers between devices, shifted(): lax.ppermute(value, axis, [(i, (i + steps) % count) for i in range(count)])  60.4 us
    pallas_call x3, Pallas kernels, attend(): pl.pallas_call(body, in_specs=[sm, sm] + [vm] * (len(args) - 2), out_spec...  35.1 us
    ppermute x28, starting transfers between devices, shifted(): lax.ppermute(value, axis, [(i, (i + steps) % count) for i in range(count)])  23.5 us
    all_to_all x1, waiting for transfers between devices, per_device(): lax.all_to_all(state, ('sp_z',) + TP, split_axis=0, concat_axis=0, tiled=...  14.1 us
    all_gather x1, waiting for transfers between devices, per_device(): weights = lax.all_gather(shards, SP, axis=0, tiled=True)  12.9 us
    unnamed x83, local copies, waits for them, and re-layouts  12.2 us
    ppermute x1, waiting for transfers between devices, passed_along(): lax.ppermute(value, axis, [(source, source + steps) for source in range(f...  12.1 us
    all_to_all x1, starting transfers between devices, per_device(): lax.all_to_all(state, ('sp_z',) + TP, split_axis=0, concat_axis=0, tiled=...  11.7 us
  transfers between devices with their start and end apart: 32, of which 21 were waited for; matrix products, arithmetic and copies ran while one was open for 1% of the time, Pallas kernels for 17%

commit v1 on v0

--- a/solution.py
+++ b/solution.py
@@ -47,13 +47,13 @@
     return pl.CostEstimate(flops=int(us * RATE), transcendentals=0, bytes_accessed=0)
 
 
-def pack(slot, key_small, value_small, key_large, value_large, query_small, query_large, gates):
+def pack(slot, key_small, value_small, key_large, value_large, query_small, query_large, gates_small, gates_large):
     rows, width = key_small.shape
     half = rows // 2
     low = width // 2
     tiles = rows // width
 
-    def body(slot_ref, ks, vs, kl, vl, qs, ql, g, kv, *q):
+    def body(slot_ref, ks, vs, kl, vl, qs, ql, gs, gl, kv, *q):
         lane = lax.broadcasted_iota(jnp.int32, (rows, width), 1)
         turn = lambda ref: pltpu.roll(ref[...].astype(f32), low, 1)
         for slot in range(2):
@@ -77,9 +77,9 @@
             def _():
                 q[shift][...] = turn(qs).astype(bf16)
 
-        for slot, head in ((0, 2), (1, 2), (2, 0), (3, 1)):
+        for slot, gate in ((0, gl[0:1]), (1, gl[0:1]), (2, gs[0:1]), (3, gs[1:2])):
             blocks = []
-            for piece in in_pieces(g[head : head + 1, :]):
+            for piece in in_pieces(gate):
                 blocks += [piece[:, i * width : (i + 1) * width] for i in range(tiles)]
                 blocks.append(jnp.zeros((8 - tiles, width), f32))
             blocks.append(jnp.zeros((EXTRA - 24, width), f32))
@@ -88,12 +88,12 @@
     vm = pl.BlockSpec(memory_space=pltpu.VMEM)
     return pl.pallas_call(
         body,
-        in_specs=[pl.BlockSpec(memory_space=pltpu.SMEM)] + [vm] * 7,
+        in_specs=[pl.BlockSpec(memory_space=pltpu.SMEM)] + [vm] * 8,
         out_specs=[vm] * 5,
         out_shape=[jax.ShapeDtypeStruct((4, rows + EXTRA, width), bf16)]
         + [jax.ShapeDtypeStruct((rows, width), bf16)] * 4,
         cost_estimate=cost_of(2.5),
-    )(slot, key_small, value_small, key_large, value_large, query_small, query_large, gates)
+    )(slot, key_small, value_small, key_large, value_large, query_small, query_large, gates_small, gates_large)
 
 
 def work_tables(calls, depth, turns):
@@ -409,11 +409,11 @@
 
 
 def pack_weights(value_weight, gate_weight, down_weight):
-    rows, width = value_weight.shape
+    width, rows = value_weight.shape
 
     def body(v, g, d, out):
-        for k, part in enumerate((v[...], g[...], d[...].T)):
-            out[:, k * BLOCK : k * BLOCK + width] = part
+        for k, part in enumerate((v, g, d)):
+            out[:, k * BLOCK : k * BLOCK + width] = part[...].T
             out[:, k * BLOCK + width : (k + 1) * BLOCK] = jnp.zeros((rows, BLOCK - width), bf16)
 
     vm = pl.BlockSpec(memory_space=pltpu.VMEM)
@@ -609,14 +609,9 @@
     down_weight,
     final_gain,
 ):
-    shard_rows = query_small.shape[0]
     slot = lax.axis_index("sp_z").astype(jnp.int32)
     column = lax.axis_index("sp_x").astype(jnp.int32)
     depth, turns = lax.axis_size("sp_z"), lax.axis_size("sp_x")
-    heads_small = gates_small.shape[1]
-    heads_large = gates_large.shape[1]
-    blank = jnp.zeros((8 - heads_small - heads_large, shard_rows), f32)
-    own_gates = jnp.concatenate([gates_small.T, gates_large.T, blank], axis=0)
     packed, *asked = pack(
         slot.reshape(1),
         key_small,
@@ -625,16 +620,19 @@
         value_large,
         query_small,
         query_large,
-        own_gates,
+        gates_small.T,
+        gates_large.T,
     )
-    shards = pack_weights(value_weight, gate_weight, down_weight)
-    packed, shards = lax.optimization_barrier((packed, shards))
+    packed, value_turned, gate_turned, down_turned = lax.optimization_barrier(
+        (packed, value_weight.T, gate_weight.T, down_weight)
+    )
+    pairs = lax.all_to_all(packed, "sp_z", split_axis=0, concat_axis=0, tiled=True)
+    shards = pack_weights(value_turned, gate_turned, down_turned)
+    pairs, shards, asked = lax.optimization_barrier((pairs, shards, asked))
     weights = lax.all_gather(shards, SP, axis=0, tiled=True)
-    pairs = lax.all_to_all(packed, "sp_z", split_axis=0, concat_axis=0, tiled=True)
-    queries = [asked[0]] + [shifted(asked[k], "sp_z", k) for k in range(1, depth)]
-    pairs, *queries = lax.optimization_barrier((pairs, *queries))
     before = shifted(pairs, "sp_x", 1)
     after = shifted(pairs, "sp_x", -1)
+    queries = [asked[0]] + [shifted(asked[k], "sp_z", k) for k in range(1, depth)]
     mixer = jnp.concatenate([mixer_small, mixer_large], axis=0)
     mixers = [mixer, shifted(mixer, "tp_y", 1), shifted(mixer, "tp_y", -1)]
     calls = ((0,), (-1, 1), (2,))
@@ -659,13 +657,13 @@
     ]
     mixers.append(shifted(mixers[1], "tp_y", 1))
     state = call(1, [before, after], state)
-    state = call(2, far, state)
-    state, mixers, weights = lax.optimization_barrier((state, mixers, weights))
-    arrived = lax.all_to_all(state, ("sp_z",) + TP, split_axis=0, concat_axis=0, tiled=True)
+    far, state, mixers = lax.optimization_barrier((far, state, mixers))
     shifts = (0, -1, 1, 2)
     mixers = [(a, shift, 0) for a, shift in zip(mixers, shifts)] + [
         (shifted(a, "tp_c", 1), shift, 1) for a, shift in zip(mixers, shifts)
     ]
+    state = call(2, far, state)
+    arrived = lax.all_to_all(state, ("sp_z",) + TP, split_axis=0, concat_axis=0, tiled=True)
     place = jnp.stack([lax.axis_index("tp_y"), lax.axis_index("tp_c")]).astype(jnp.int32)
     mixed = mix_rows(place, arrived, mixers, residual, mix_gain)
     turns_y, cores = lax.axis_size("tp_y"), lax.axis_size("tp_c")

time: 248 us -> 234 us (0.944)
  the two profiles are of different devices: /device:TPU:33 before, /device:TPU:32 now
where the time goes in v1:
time: 234 us; the launch traced here: 233 us
  waiting for transfers between devices  80.3 us (34%)
  Pallas kernels  71.9 us (31%)
  starting transfers between devices  52 us (22%)
  local copies, waits for them, and re-layouts  14.4 us (6%)
  between operations  13.8 us (6%)
    ppermute x28, waiting for transfers between devices, shifted(): lax.ppermute(value, axis, [(i, (i + steps) % count) for i in range(count)])  43.7 us
    pallas_call x3, Pallas kernels, attend(): pl.pallas_call(body, in_specs=[sm, sm] + [vm] * (len(args) - 2), out_spec...  34.7 us
    ppermute x28, starting transfers between devices, shifted(): lax.ppermute(value, axis, [(i, (i + steps) % count) for i in range(count)])  28.2 us
    ppermute x1, waiting for transfers between devices, passed_along(): lax.ppermute(value, axis, [(source, source + steps) for source in range(f...  14.4 us
    all_to_all x1, waiting for transfers between devices, per_device(): lax.all_to_all(state, ('sp_z',) + TP, split_axis=0, concat_axis=0, tiled=...  13.2 us
    unnamed x85, local copies, waits for them, and re-layouts  12.2 us
    all_to_all x1, starting transfers between devices, per_device(): lax.all_to_all(state, ('sp_z',) + TP, split_axis=0, concat_axis=0, tiled=...  12.2 us
    pallas_call x2, Pallas kernels, downs(): pl.pallas_call(body, grid=(1,), in_specs=[pl.BlockSpec(memory_space=pltpu...  11.4 us
  transfers between devices with their start and end apart: 32, of which 16 were waited for; matrix products, arithmetic and copies ran while one was open for 1% of the time, Pallas kernels for 21%

profile of v1, /device:TPU:32, one launch (start us, length us, event | category | flops | bytes accessed | tf_op | source)
XLA Modules:
  0.0 233.1 jit_solution(11992528120253739700)
XLA Ops:
  6.5 2.9 %shard_map.199 = (bf16[4,800,128]{2,1,0:T(8,128)(2,1)}, bf16[768,128]{1,0:T(8,128)(2,1)}, bf16[768,128]{1,0:T(8,128)(2,1)}, bf16[768,128]{1,0:T(8,128)(2,1)}, bf16[768,128]{1,0:T(8,128)(2,1)}) custom-call(s32[1]{0:T(128)} %bitcast.2.slot_ref, bf16[768,128]{1,0:T(8,128)(2,1)} %ks.1, bf16[768,128]{1,0:T(8,128)(2,1)} %vs.1, bf16[768,128]{1,0:T(8,128)(2,1)} %kl.1, ...), custom_call_target="tpu_custom_call" | custom-call | flops 625000000 | tf_op jit(solution)/shard_map/pallas_call | solution.py:89
  9.5 5.6 %all-to-all-start = ((bf16[4,800,128]{2,1,0:T(8,128)(2,1)}), bf16[4,800,128]{2,1,0:T(8,128)(2,1)S(1)}, u32[]{:S(2)}, u32[]{:S(2)}) async-start(bf16[4,800,128]{2,1,0:T(8,128)(2,1)} %get-tuple-element.69), calls=%async_computation | async-start | bytes 1638400 | tf_op jit(solution)/shard_map/all_to_all | solution.py:629
  15.1 2.2 shard_map.200
  17.3 8.9 %all-to-all-done.refs_6_ = bf16[4,800,128]{2,1,0:T(8,128)(2,1)S(1)} async-done(((bf16[4,800,128]{2,1,0:T(8,128)(2,1)}), bf16[4,800,128]{2,1,0:T(8,128)(2,1)S(1)}, u32[]{:S(2)}, u32[]{:S(2)}) %all-to-all-start) | async-done | bytes 819232 | tf_op jit(solution)/shard_map/all_to_all | solution.py:629
  26.4 1.6 collective-permute-start.5
  28.0 1.7 collective-permute-start.6
  29.7 1.5 collective-permute-start.3
  31.2 1.7 collective-permute-start.4
  32.9 2.4 %collective-permute-done.refs_3_ = bf16[768,128]{1,0:T(8,128)(2,1)S(1)} collective-permute-done((bf16[768,128]{1,0:T(8,128)(2,1)S(1)}, bf16[768,128]{1,0:T(8,128)(2,1)S(1)}, u32[]{:S(2)}, u32[]{:S(2)}) %collective-permute-start) | collective-permute-done | bytes 196640 | tf_op jit(solution)/shard_map/ppermute | solution.py:24
  35.3 1.5 collective-permute-start.1
  36.8 10.0 %collective-permute-done.1.refs_4_ = bf16[768,128]{1,0:T(8,128)(2,1)S(1)} collective-permute-done((bf16[768,128]{1,0:T(8,128)(2,1)S(1)}, bf16[768,128]{1,0:T(8,128)(2,1)S(1)}, u32[]{:S(2)}, u32[]{:S(2)}) %collective-permute-start.1) | collective-permute-done | bytes 196640 | tf_op jit(solution)/shard_map/ppermute | solution.py:24
  46.9 0.6 collective-permute-start.2
  47.4 0.6 pad_add_fusion.1.refs_0_
  48.0 6.7 %collective-permute-done.2.refs_5_ = bf16[768,128]{1,0:T(8,128)(2,1)S(1)} collective-permute-done((bf16[768,128]{1,0:T(8,128)(2,1)}, bf16[768,128]{1,0:T(8,128)(2,1)S(1)}, u32[]{:S(2)}, u32[]{:S(2)}) %collective-permute-start.2) | collective-permute-done | bytes 196640 | tf_op jit(solution)/shard_map/ppermute | solution.py:24
  54.8 0.7 copy-done.39
  55.4 11.6 %shard_map.201 = (f32[4,144,768]{2,1,0:T(8,128)}, f32[4,8,768]{2,1,0:T(8,128)}) custom-call(s32[2]{0:T(128)} %pad_add_fusion.1.refs_0_, s32[4,34]{1,0:T(4,128)} %constant.21.clone.refs_1_, bf16[768,128]{1,0:T(8,128)(2,1)} %get-tuple-element.77.refs_2_, bf16[768,128]{1,0:T(8,128)(2,1)} %copy-done.37, bf16[768,128]{1,0:T(8,128)(2,1)} %copy-done.38, ...), custom_call_target="tpu_custom_call" | custom-call | flops 3000000000 | tf_op jit(solution)/shard_map/pallas_call | solution.py:346
  67.1 1.1 slice.12
  68.2 2.3 collective-permute-start.7
  70.6 1.0 slice.13
  71.6 1.7 collective-permute-start.8
  73.2 14.0 %shard_map.202 = (f32[4,144,768]{2,1,0:T(8,128)}, f32[4,8,768]{2,1,0:T(8,128)}) custom-call(s32[2]{0:T(128)} %pad_add_fusion.1.refs_0_, s32[4,64]{1,0:T(4,128)} %constant.22.clone.refs_1_, bf16[768,128]{1,0:T(8,128)(2,1)} %get-tuple-element.77.refs_2_, bf16[768,128]{1,0:T(8,128)(2,1)} %copy-done.37, bf16[768,128]{1,0:T(8,128)(2,1)} %copy-done.38, ...), custom_call_target="tpu_custom_call" | custom-call | flops 6000000000 | tf_op jit(solution)/shard_map/pallas_call | solution.py:346
  87.7 2.7 %collective-permute-done.8.refs_7_ = bf16[2,800,128]{2,1,0:T(8,128)(2,1)S(1)} collective-permute-done((bf16[2,800,128]{2,1,0:T(8,128)(2,1)S(1)}, bf16[2,800,128]{2,1,0:T(8,128)(2,1)S(1)}, u32[]{:S(2)}, u32[]{:S(2)}) %collective-permute-start.8) | collective-permute-done | bytes 409632 | tf_op jit(solution)/shard_map/ppermute | solution.py:24
  90.4 0.5 collective-permute-start.11
  91.4 9.1 %shard_map.203 = bf16[32,112,128]{2,1,0:T(8,128)(2,1)} custom-call(s32[2]{0:T(128)} %pad_add_fusion.1.refs_0_, s32[4,34]{1,0:T(4,128)} %constant.23.clone.refs_1_, bf16[768,128]{1,0:T(8,128)(2,1)} %get-tuple-element.77.refs_2_, bf16[768,128]{1,0:T(8,128)(2,1)} %copy-done.37, bf16[768,128]{1,0:T(8,128)(2,1)} %copy-done.38, bf16[768,128]{1,0:T(8,128)(2,1)} %copy-done.39, ...), custom_call_target="tpu_custom_call" | custom-call | flops 3000000000 | tf_op jit(solution)/shard_map/pallas_call | solution.py:346
  100.6 12.2 %all-to-all-start.1 = ((bf16[32,112,128]{2,1,0:T(8,128)(2,1)}), bf16[32,112,128]{2,1,0:T(8,128)(2,1)S(1)}, u32[]{:S(2)}, u32[]{:S(2)}) async-start(bf16[32,112,128]{2,1,0:T(8,128)(2,1)} %shard_map.203), calls=%async_computation.1 | async-start | bytes 1835008 | tf_op jit(solution)/shard_map/all_to_all | solution.py:666
  112.9 13.2 %all-to-all-done.1.arrived_ref = bf16[32,112,128]{2,1,0:T(8,128)(2,1)S(1)} async-done(((bf16[32,112,128]{2,1,0:T(8,128)(2,1)}), bf16[32,112,128]{2,1,0:T(8,128)(2,1)S(1)}, u32[]{:S(2)}, u32[]{:S(2)}) %all-to-all-start.1) | async-done | bytes 917536 | tf_op jit(solution)/shard_map/all_to_all | solution.py:666
  126.1 1.0 copy-done.20
  127.1 4.7 %shard_map.204.refs_0_ = bf16[96,2048]{1,0:T(8,128)(2,1)S(1)} custom-call(s32[2]{0:T(128)S(1)} %pad_add_fusion.place_ref, bf16[32,112,128]{2,1,0:T(8,128)(2,1)S(1)} %all-to-all-done.1.arrived_ref, bf16[256,2048]{1,0:T(8,128)(2,1)S(1)} %constant_dynamic-update-slice_fusion.refs_0_, bf16[256,2048]{1,0:T(8,128)(2,1)S(1)} %collective-permute-done.5.refs_1_, ...), custom_call_target="tpu_custom_call" | custom-call | flops 1250000000 | tf_op jit(solution)/shard_map/pallas_call | solution.py:396
  131.9 1.1 collective-permute-start.14
  132.9 1.2 collective-permute-start.15
  134.2 2.0 collective-permute-start.16
  136.2 3.7 %copy-done = bf16[2048,2304]{1,0:T(8,128)(2,1)S(1)} copy-done((bf16[2048,2304]{1,0:T(8,128)(2,1)S(1)}, bf16[2048,2304]{1,0:T(8,128)(2,1)}, u32[]{:S(2)}) %copy-start) | copy-done | bytes 9437208
  139.9 1.4 shard_map.205
  141.3 3.9 %collective-permute-done.15.refs_0_ = bf16[96,2048]{1,0:T(8,128)(2,1)S(1)} collective-permute-done((bf16[96,2048]{1,0:T(8,128)(2,1)S(1)}, bf16[96,2048]{1,0:T(8,128)(2,1)S(1)}, u32[]{:S(2)}, u32[]{:S(2)}) %collective-permute-start.15) | collective-permute-done | bytes 393248 | tf_op jit(solution)/shard_map/ppermute | solution.py:24
  145.3 0.5 collective-permute-start.18
  145.8 0.7 collective-permute-start.19
  146.5 2.6 %collective-permute-start.20 = (bf16[48,2048]{1,0:T(8,128)(2,1)S(1)}, bf16[48,2048]{1,0:T(8,128)(2,1)S(1)}, u32[]{:S(2)}, u32[]{:S(2)}) collective-permute-start(bf16[48,2048]{1,0:T(8,128)(2,1)S(1)} %slice.15), channel_id=1, source_target_pairs={{0,6},{2,0},{4,2},{6,4},{1,7},{3,1},{5,3},{7,5},{8,14},{10,8},{12,... | collective-permute-start | bytes 589832 | tf_op jit(solution)/shard_map/ppermute | solution.py:24
  149.1 2.6 %shard_map.206 = (bf16[384,704]{1,0:T(8,128)(2,1)S(1)}, bf16[384,704]{1,0:T(8,128)(2,1)S(1)}) custom-call(bf16[96,2048]{1,0:T(8,128)(2,1)S(1)} %collective-permute-done.15.refs_0_, bf16[96,2048]{1,0:T(8,128)(2,1)S(1)} %collective-permute-done.16.refs_1_, bf16[96,2048]{1,0:T(8,128)(2,1)S(1)} %collective-permute-done.17.refs_2_, ...), custom_call_target="tpu_custom_call" | custom-call | flops 1000000000 | tf_op jit(solution)/shard_map/pallas_call | solution.py:447
  151.8 2.1 collective-permute-done.19.refs_0_
  153.9 0.5 collective-permute-start.22
  154.4 0.9 collective-permute-done.21.refs_2_
  155.6 1.4 shard_map.207
  157.1 0.7 copy-done.11
  157.8 0.7 copy-done.13
  158.5 2.5 %shard_map.208 = (bf16[8,16,704]{2,1,0:T(8,128)(2,1)}, bf16[8,16,704]{2,1,0:T(8,128)(2,1)}, bf16[32,704]{1,0:T(8,128)(2,1)}) custom-call(s32[2]{0:T(128)} %copy-done.23, bf16[192,704]{1,0:T(8,128)(2,1)} %copy-done.7, bf16[192,704]{1,0:T(8,128)(2,1)} %copy-done.9, bf16[384,704]{1,0:T(8,128)(2,1)} %copy-done.3, bf16[384,704]{1,0:T(8,128)(2,1)} %copy-done.5, ...), custom_call_target="tpu_custom_call" | custom-call | flops 375000000 | tf_op jit(solution)/shard_map/pallas_call | solution.py:477
  161.0 6.0 %collective-permute-start.23 = (bf16[32,704]{1,0:T(8,128)(2,1)}, bf16[32,704]{1,0:T(8,128)(2,1)S(1)}, u32[]{:S(2)}, u32[]{:S(2)}) collective-permute-start(bf16[32,704]{1,0:T(8,128)(2,1)} %get-tuple-element.116), channel_id=1, source_target_pairs={{0,8},{8,16},{16,24},{24,32},{32,40},{40,48},{48,56},{56,64},{64,7... | collective-permute-start | bytes 135176 | tf_op jit(solution)/shard_map/ppermute | solution.py:30
  167.0 14.4 %collective-permute-done.23.refs_3_ = bf16[32,704]{1,0:T(8,128)(2,1)S(1)} collective-permute-done((bf16[32,704]{1,0:T(8,128)(2,1)}, bf16[32,704]{1,0:T(8,128)(2,1)S(1)}, u32[]{:S(2)}, u32[]{:S(2)}) %collective-permute-start.23) | collective-permute-done | bytes 45088 | tf_op jit(solution)/shard_map/ppermute | solution.py:30
  181.5 0.9 copy-done.16
  182.4 0.9 copy-done.18
  183.3 4.3 %shard_map.209 = (bf16[1,96,2048]{2,1,0:T(8,128)(2,1)S(1)}, f32[1,96,2048]{2,1,0:T(8,128)S(1)}) custom-call(s32[2]{0:T(128)S(1)} %copy-done.24, f32[3,704]{1,0:T(4,128)S(1)} %copy-done.21, f32[3,704]{1,0:T(4,128)S(1)} %copy-done.22, bf16[2048,2304]{1,0:T(8,128)(2,1)} %all-gather.2.cloned.1.call-done.refs_2_.refs_3_.refs_4_.refs_5_, ...), custom_call_target="tpu_custom_call" | custom-call | flops 1000000000 | tf_op jit(solution)/shard_map/pallas_call | solution.py:533
  187.7 0.9 copy-done.15
  188.5 1.7 collective-permute-done.24.their_ref
  190.3 0.7 copy-done.31
  191.0 2.1 shard_map.210
  193.1 7.1 %shard_map.211 = (bf16[3,96,2048]{2,1,0:T(8,128)(2,1)S(1)}, f32[3,96,2048]{2,1,0:T(8,128)}) custom-call(s32[2]{0:T(128)S(1)} %copy-done.24, f32[3,704]{1,0:T(4,128)S(1)} %copy-done.21, f32[3,704]{1,0:T(4,128)S(1)} %copy-done.22, bf16[2048,2304]{1,0:T(8,128)(2,1)} %all-gather.2.cloned.1.call-done.refs_2_.refs_3_.refs_4_.refs_5_, ...), custom_call_target="tpu_custom_call" | custom-call | flops 2000000000 | tf_op jit(solution)/shard_map/pallas_call | solution.py:533
  200.4 2.9 %collective-permute-start.26 = (bf16[96,2048]{1,0:T(8,128)(2,1)S(1)}, bf16[96,2048]{1,0:T(8,128)(2,1)S(1)}, u32[]{:S(2)}, u32[]{:S(2)}) collective-permute-start(bf16[96,2048]{1,0:T(8,128)(2,1)S(1)} %copy-done.30), channel_id=1, source_target_pairs={{0,4},{2,6},{4,0},{6,2},{1,5},{3,7},{5,1},{7,3},{8,12},{10,14},{12... | collective-permute-start | bytes 1179656 | tf_op jit(solution)/shard_map/ppermute | solution.py:24
  203.3 1.1 copy-done.26
  204.4 3.2 %shard_map.212 = (f32[96,2048]{1,0:T(8,128)}, bf16[96,2048]{1,0:T(8,128)(2,1)}, bf16[96,2048]{1,0:T(8,128)(2,1)}) custom-call(f32[3,96,2048]{2,1,0:T(8,128)} %get-tuple-element.125.mine_ref, bf16[3,96,2048]{2,1,0:T(8,128)(2,1)} %copy-done.26), custom_call_target="tpu_custom_call" | custom-call | flops 525000000 | tf_op jit(solution)/shard_map/pallas_call | solution.py:558
  207.6 2.8 %collective-permute-start.27 = (bf16[96,2048]{1,0:T(8,128)(2,1)}, bf16[96,2048]{1,0:T(8,128)(2,1)S(1)}, u32[]{:S(2)}, u32[]{:S(2)}) collective-permute-start(bf16[96,2048]{1,0:T(8,128)(2,1)} %get-tuple-element.129), channel_id=1, source_target_pairs={{0,6},{2,0},{4,2},{6,4},{1,7},{3,1},{5,3},{7,5},{8,14},{10,8},{12,... | collective-permute-start | bytes 1179656 | tf_op jit(solution)/shard_map/ppermute | solution.py:24
  210.4 3.2 %collective-permute-done.26.refs_2_ = bf16[96,2048]{1,0:T(8,128)(2,1)S(1)} collective-permute-done((bf16[96,2048]{1,0:T(8,128)(2,1)S(1)}, bf16[96,2048]{1,0:T(8,128)(2,1)S(1)}, u32[]{:S(2)}, u32[]{:S(2)}) %collective-permute-start.26) | collective-permute-done | bytes 393248 | tf_op jit(solution)/shard_map/ppermute | solution.py:24
  213.6 8.4 %collective-permute-done.27.refs_3_ = bf16[96,2048]{1,0:T(8,128)(2,1)S(1)} collective-permute-done((bf16[96,2048]{1,0:T(8,128)(2,1)}, bf16[96,2048]{1,0:T(8,128)(2,1)S(1)}, u32[]{:S(2)}, u32[]{:S(2)}) %collective-permute-start.27) | collective-permute-done | bytes 393248 | tf_op jit(solution)/shard_map/ppermute | solution.py:24
  222.1 0.6 collective-permute-done.28.refs_4_
  222.8 0.7 copy-done.34
  223.5 2.8 %shard_map.213 = bf16[96,2048]{1,0:T(8,128)(2,1)} custom-call(bf16[96,2048]{1,0:T(8,128)(2,1)} %copy-done.2, f32[96,2048]{1,0:T(8,128)} %get-tuple-element.127.refs_1_, bf16[96,2048]{1,0:T(8,128)(2,1)} %copy-done.32, bf16[96,2048]{1,0:T(8,128)(2,1)} %copy-done.33, bf16[96,2048]{1,0:T(8,128)(2,1)} %copy-done.34, f32[1,2048]{1,0:T(1,128)} %bitcast.11), custom_call_target="tpu_custom_call" | custom-call | flops 500000000 | tf_op jit(solution)/shard_map/pallas_call | solution.py:583
  (108 shorter events, 2.0 us)
Async XLA Ops:
  9.5 16.8 %copy-start.28 = (bf16[128,2048]{1,0:T(8,128)(2,1)S(1)}, bf16[128,2048]{1,0:T(8,128)(2,1)}, u32[]{:S(2)}) copy-start(bf16[128,2048]{1,0:T(8,128)(2,1)} %param.30) | copy-start | bytes 1572868
  9.5 16.7 %all-to-all-start = ((bf16[4,800,128]{2,1,0:T(8,128)(2,1)}), bf16[4,800,128]{2,1,0:T(8,128)(2,1)S(1)}, u32[]{:S(2)}, u32[]{:S(2)}) async-start(bf16[4,800,128]{2,1,0:T(8,128)(2,1)} %get-tuple-element.69), calls=%async_computation | async-start | bytes 1638400 | tf_op jit(solution)/shard_map/all_to_all | solution.py:629
  15.0 11.3 %copy-start.29 = (bf16[128,2048]{1,0:T(8,128)(2,1)S(1)}, bf16[128,2048]{1,0:T(8,128)(2,1)}, u32[]{:S(2)}) copy-start(bf16[128,2048]{1,0:T(8,128)(2,1)} %param.31) | copy-start | bytes 1572868
  15.0 14.6 %copy-start.41 = (bf16[768,128]{1,0:T(8,128)(2,1)S(1)}, bf16[768,128]{1,0:T(8,128)(2,1)}, u32[]{:S(2)}) copy-start(bf16[768,128]{1,0:T(8,128)(2,1)} %get-tuple-element.78) | copy-start | bytes 589828
  15.0 20.3 %copy-start.40 = (bf16[768,128]{1,0:T(8,128)(2,1)S(1)}, bf16[768,128]{1,0:T(8,128)(2,1)}, u32[]{:S(2)}) copy-start(bf16[768,128]{1,0:T(8,128)(2,1)} %get-tuple-element.79) | copy-start | bytes 589828
  15.0 121.1 %all-gather.2.cloned.1.call-start = ((), (), s32[]{:S(2)}) async-start(), calls=%async_computation.2 | async-start | bytes 10027008 | tf_op jit(solution)/shard_map/all_gather | solution.py:632
  26.2 28.5 %copy-start.27 = (bf16[4,800,128]{2,1,0:T(8,128)(2,1)}, bf16[4,800,128]{2,1,0:T(8,128)(2,1)S(1)}, u32[]{:S(2)}) copy-start(bf16[4,800,128]{2,1,0:T(8,128)(2,1)S(1)} %all-to-all-done.refs_6_) | copy-start | bytes 2457604
  26.4 40.7 %collective-permute-start.5 = (bf16[256,2048]{1,0:T(8,128)(2,1)S(1)}, bf16[256,2048]{1,0:T(8,128)(2,1)S(1)}, u32[]{:S(2)}, u32[]{:S(2)}) collective-permute-start(bf16[256,2048]{1,0:T(8,128)(2,1)S(1)} %constant_dynamic-update-slice_fusion.refs_0_), channel_id=1, source_target_pairs={{0,2},{2,4},{4,6},{6,0},{1,3},{3,5},{5,7},{7,1},{8,10},{10,12},{12... | collective-permute-start | bytes 3145736 | tf_op jit(solution)/shard_map/ppermute | solution.py:24
  28.0 39.0 %collective-permute-start.6 = (bf16[256,2048]{1,0:T(8,128)(2,1)S(1)}, bf16[256,2048]{1,0:T(8,128)(2,1)}, u32[]{:S(2)}, u32[]{:S(2)}) collective-permute-start(bf16[256,2048]{1,0:T(8,128)(2,1)S(1)} %constant_dynamic-update-slice_fusion.refs_0_), channel_id=1, source_target_pairs={{0,6},{2,0},{4,2},{6,4},{1,7},{3,1},{5,3},{7,5},{8,14},{10,8},{12,... | collective-permute-start | bytes 3145736 | tf_op jit(solution)/shard_map/ppermute | solution.py:24
  29.7 5.7 %collective-permute-start = (bf16[768,128]{1,0:T(8,128)(2,1)S(1)}, bf16[768,128]{1,0:T(8,128)(2,1)S(1)}, u32[]{:S(2)}, u32[]{:S(2)}) collective-permute-start(bf16[768,128]{1,0:T(8,128)(2,1)S(1)} %copy-done.41), channel_id=1, source_target_pairs={{0,32},{32,64},{64,96},{96,0},{1,33},{33,65},{65,97},{97,1},{2,34}... | collective-permute-start | bytes 589832 | tf_op jit(solution)/shard_map/ppermute | solution.py:24
  29.7 37.4 %collective-permute-start.3 = (bf16[4,800,128]{2,1,0:T(8,128)(2,1)S(1)}, bf16[4,800,128]{2,1,0:T(8,128)(2,1)}, u32[]{:S(2)}, u32[]{:S(2)}) collective-permute-start(bf16[4,800,128]{2,1,0:T(8,128)(2,1)S(1)} %all-to-all-done.refs_6_), channel_id=1, source_target_pairs={{0,8},{8,16},{16,24},{24,0},{1,9},{9,17},{17,25},{25,1},{2,10},{10... | collective-permute-start | bytes 2457608 | tf_op jit(solution)/shard_map/ppermute | solution.py:24
  31.2 35.9 %collective-permute-start.4 = (bf16[4,800,128]{2,1,0:T(8,128)(2,1)S(1)}, bf16[4,800,128]{2,1,0:T(8,128)(2,1)}, u32[]{:S(2)}, u32[]{:S(2)}) collective-permute-start(bf16[4,800,128]{2,1,0:T(8,128)(2,1)S(1)} %all-to-all-done.refs_6_), channel_id=1, source_target_pairs={{0,24},{8,0},{16,8},{24,16},{1,25},{9,1},{17,9},{25,17},{2,26},{10... | collective-permute-start | bytes 2457608 | tf_op jit(solution)/shard_map/ppermute | solution.py:24
  35.3 19.4 %copy-start.37 = (bf16[768,128]{1,0:T(8,128)(2,1)}, bf16[768,128]{1,0:T(8,128)(2,1)S(1)}, u32[]{:S(2)}) copy-start(bf16[768,128]{1,0:T(8,128)(2,1)S(1)} %collective-permute-done.refs_3_) | copy-start | bytes 589828
  35.3 11.5 %collective-permute-start.1 = (bf16[768,128]{1,0:T(8,128)(2,1)S(1)}, bf16[768,128]{1,0:T(8,128)(2,1)S(1)}, u32[]{:S(2)}, u32[]{:S(2)}) collective-permute-start(bf16[768,128]{1,0:T(8,128)(2,1)S(1)} %copy-done.40), channel_id=1, source_target_pairs={{0,64},{32,96},{64,0},{96,32},{1,65},{33,97},{65,1},{97,33},{2,66}... | collective-permute-start | bytes 589832 | tf_op jit(solution)/shard_map/ppermute | solution.py:24
  46.8 7.9 %copy-start.38 = (bf16[768,128]{1,0:T(8,128)(2,1)}, bf16[768,128]{1,0:T(8,128)(2,1)S(1)}, u32[]{:S(2)}) copy-start(bf16[768,128]{1,0:T(8,128)(2,1)S(1)} %collective-permute-done.1.refs_4_) | copy-start | bytes 589828
  46.9 7.9 %collective-permute-start.2 = (bf16[768,128]{1,0:T(8,128)(2,1)}, bf16[768,128]{1,0:T(8,128)(2,1)S(1)}, u32[]{:S(2)}, u32[]{:S(2)}) collective-permute-start(bf16[768,128]{1,0:T(8,128)(2,1)} %get-tuple-element.80), channel_id=1, source_target_pairs={{0,96},{32,0},{64,32},{96,64},{1,97},{33,1},{65,33},{97,65},{2,98}... | collective-permute-start | bytes 589832 | tf_op jit(solution)/shard_map/ppermute | solution.py:24
  67.1 23.4 %collective-permute-start.9 = (bf16[256,2048]{1,0:T(8,128)(2,1)S(1)}, bf16[256,2048]{1,0:T(8,128)(2,1)}, u32[]{:S(2)}, u32[]{:S(2)}) collective-permute-start(bf16[256,2048]{1,0:T(8,128)(2,1)S(1)} %collective-permute-done.5.refs_1_), channel_id=1, source_target_pairs={{0,2},{2,4},{4,6},{6,0},{1,3},{3,5},{5,7},{7,1},{8,10},{10,12},{12... | collective-permute-start | bytes 3145736 | tf_op jit(solution)/shard_map/ppermute | solution.py:24
  68.2 19.4 %collective-permute-start.7 = (bf16[2,800,128]{2,1,0:T(8,128)(2,1)S(1)}, bf16[2,800,128]{2,1,0:T(8,128)(2,1)S(1)}, u32[]{:S(2)}, u32[]{:S(2)}) collective-permute-start(bf16[2,800,128]{2,1,0:T(8,128)(2,1)S(1)} %slice.12), channel_id=1, source_target_pairs={{0,8},{8,16},{16,24},{24,0},{1,9},{9,17},{17,25},{25,1},{2,10},{10... | collective-permute-start | bytes 1228808 | tf_op jit(solution)/shard_map/ppermute | solution.py:24
  71.6 18.8 %collective-permute-start.8 = (bf16[2,800,128]{2,1,0:T(8,128)(2,1)S(1)}, bf16[2,800,128]{2,1,0:T(8,128)(2,1)S(1)}, u32[]{:S(2)}, u32[]{:S(2)}) collective-permute-start(bf16[2,800,128]{2,1,0:T(8,128)(2,1)S(1)} %slice.13), channel_id=1, source_target_pairs={{0,24},{8,0},{16,8},{24,16},{1,25},{9,1},{17,9},{25,17},{2,26},{10... | collective-permute-start | bytes 1228808 | tf_op jit(solution)/shard_map/ppermute | solution.py:24
  87.7 3.8 %copy-start.35 = (bf16[2,800,128]{2,1,0:T(8,128)(2,1)}, bf16[2,800,128]{2,1,0:T(8,128)(2,1)S(1)}, u32[]{:S(2)}) copy-start(bf16[2,800,128]{2,1,0:T(8,128)(2,1)S(1)} %collective-permute-done.7.refs_6_) | copy-start | bytes 1228804
  90.4 1.0 copy-start.36
  90.4 35.6 %collective-permute-start.10 = (bf16[256,2048]{1,0:T(8,128)(2,1)S(1)}, bf16[256,2048]{1,0:T(8,128)(2,1)}, u32[]{:S(2)}, u32[]{:S(2)}) collective-permute-start(bf16[256,2048]{1,0:T(8,128)(2,1)S(1)} %constant_dynamic-update-slice_fusion.refs_0_), channel_id=1, source_target_pairs={{0,1},{1,0},{2,3},{3,2},{4,5},{5,4},{6,7},{7,6},{8,9},{9,8},{10,11... | collective-permute-start | bytes 3145736 | tf_op jit(solution)/shard_map/ppermute | solution.py:24
  90.4 35.6 %collective-permute-start.11 = (bf16[256,2048]{1,0:T(8,128)(2,1)S(1)}, bf16[256,2048]{1,0:T(8,128)(2,1)}, u32[]{:S(2)}, u32[]{:S(2)}) collective-permute-start(bf16[256,2048]{1,0:T(8,128)(2,1)S(1)} %collective-permute-done.5.refs_1_), channel_id=1, source_target_pairs={{0,1},{1,0},{2,3},{3,2},{4,5},{5,4},{6,7},{7,6},{8,9},{9,8},{10,11... | collective-permute-start | bytes 3145736 | tf_op jit(solution)/shard_map/ppermute | solution.py:24
  90.9 35.1 %collective-permute-start.12 = (bf16[256,2048]{1,0:T(8,128)(2,1)}, bf16[256,2048]{1,0:T(8,128)(2,1)}, u32[]{:S(2)}, u32[]{:S(2)}) collective-permute-start(bf16[256,2048]{1,0:T(8,128)(2,1)} %collective-permute-done.6.refs_2_), channel_id=1, source_target_pairs={{0,1},{1,0},{2,3},{3,2},{4,5},{5,4},{6,7},{7,6},{8,9},{9,8},{10,11... | collective-permute-start | bytes 3145736 | tf_op jit(solution)/shard_map/ppermute | solution.py:24
  91.0 35.0 %collective-permute-start.13 = (bf16[256,2048]{1,0:T(8,128)(2,1)}, bf16[256,2048]{1,0:T(8,128)(2,1)}, u32[]{:S(2)}, u32[]{:S(2)}) collective-permute-start(bf16[256,2048]{1,0:T(8,128)(2,1)} %collective-permute-done.9.refs_3_), channel_id=1, source_target_pairs={{0,1},{1,0},{2,3},{3,2},{4,5},{5,4},{6,7},{7,6},{8,9},{9,8},{10,11... | collective-permute-start | bytes 3145736 | tf_op jit(solution)/shard_map/ppermute | solution.py:24
  100.6 25.5 %copy-start.25 = (f32[2048]{0:T(1024)S(1)}, f32[2048]{0:T(1024)}, u32[]{:S(2)}) copy-start(f32[2048]{0:T(1024)} %param.32) | copy-start | bytes 24580
  100.6 25.5 %all-to-all-start.1 = ((bf16[32,112,128]{2,1,0:T(8,128)(2,1)}), bf16[32,112,128]{2,1,0:T(8,128)(2,1)S(1)}, u32[]{:S(2)}, u32[]{:S(2)}) async-start(bf16[32,112,128]{2,1,0:T(8,128)(2,1)} %shard_map.203), calls=%async_computation.1 | async-start | bytes 1835008 | tf_op jit(solution)/shard_map/all_to_all | solution.py:666
  112.8 19.0 %copy-start.23 = (s32[2]{0:T(128)}, s32[2]{0:T(128)S(1)}, u32[]{:S(2)}) copy-start(s32[2]{0:T(128)S(1)} %pad_add_fusion.place_ref) | copy-start | bytes 28
  131.8 9.4 %copy-start.2 = (bf16[96,2048]{1,0:T(8,128)(2,1)}, bf16[96,2048]{1,0:T(8,128)(2,1)S(1)}, u32[]{:S(2)}) copy-start(bf16[96,2048]{1,0:T(8,128)(2,1)S(1)} %shard_map.204.refs_0_) | copy-start | bytes 1179652
  131.9 4.3 %collective-permute-start.14 = (bf16[96,2048]{1,0:T(8,128)(2,1)S(1)}, bf16[96,2048]{1,0:T(8,128)(2,1)S(1)}, u32[]{:S(2)}, u32[]{:S(2)}) collective-permute-start(bf16[96,2048]{1,0:T(8,128)(2,1)S(1)} %shard_map.204.refs_0_), channel_id=1, source_target_pairs={{0,1},{1,0},{2,3},{3,2},{4,5},{5,4},{6,7},{7,6},{8,9},{9,8},{10,11... | collective-permute-start | bytes 1179656 | tf_op jit(solution)/shard_map/ppermute | solution.py:24
  132.9 12.3 %collective-permute-start.15 = (bf16[96,2048]{1,0:T(8,128)(2,1)S(1)}, bf16[96,2048]{1,0:T(8,128)(2,1)S(1)}, u32[]{:S(2)}, u32[]{:S(2)}) collective-permute-start(bf16[96,2048]{1,0:T(8,128)(2,1)S(1)} %shard_map.204.refs_0_), channel_id=1, source_target_pairs={{0,2},{2,4},{4,6},{6,0},{1,3},{3,5},{5,7},{7,1},{8,10},{10,12},{12... | collective-permute-start | bytes 1179656 | tf_op jit(solution)/shard_map/ppermute | solution.py:24
  134.2 11.1 %collective-permute-start.16 = (bf16[96,2048]{1,0:T(8,128)(2,1)S(1)}, bf16[96,2048]{1,0:T(8,128)(2,1)S(1)}, u32[]{:S(2)}, u32[]{:S(2)}) collective-permute-start(bf16[96,2048]{1,0:T(8,128)(2,1)S(1)} %shard_map.204.refs_0_), channel_id=1, source_target_pairs={{0,6},{2,0},{4,2},{6,4},{1,7},{3,1},{5,3},{7,5},{8,14},{10,8},{12,... | collective-permute-start | bytes 1179656 | tf_op jit(solution)/shard_map/ppermute | solution.py:24
  136.2 3.7 %copy-start = (bf16[2048,2304]{1,0:T(8,128)(2,1)S(1)}, bf16[2048,2304]{1,0:T(8,128)(2,1)}, u32[]{:S(2)}) copy-start(bf16[2048,2304]{1,0:T(8,128)(2,1)} %all-gather.2.cloned.1.call-done.refs_2_.refs_3_.refs_4_.refs_5_) | copy-start | bytes 28311556
  139.9 9.3 %copy-start.1 = (bf16[2048,2304]{1,0:T(8,128)(2,1)S(1)}, bf16[2048,2304]{1,0:T(8,128)(2,1)}, u32[]{:S(2)}) copy-start(bf16[2048,2304]{1,0:T(8,128)(2,1)} %all-gather.2.cloned.1.call-done.refs_2_.refs_3_.refs_4_.refs_5_) | copy-start | bytes 28311556
  141.3 7.8 %copy-start.7 = (bf16[192,704]{1,0:T(8,128)(2,1)}, bf16[192,704]{1,0:T(8,128)(2,1)S(1)}, u32[]{:S(2)}) copy-start(bf16[192,704]{1,0:T(8,128)(2,1)S(1)} %get-tuple-element.121.refs_0_.refs_6_) | copy-start | bytes 811012
  141.3 10.4 %copy-start.9 = (bf16[192,704]{1,0:T(8,128)(2,1)}, bf16[192,704]{1,0:T(8,128)(2,1)S(1)}, u32[]{:S(2)}) copy-start(bf16[192,704]{1,0:T(8,128)(2,1)S(1)} %get-tuple-element.122.refs_1_.refs_7_) | copy-start | bytes 811012
  145.3 3.9 %collective-permute-start.17 = (bf16[96,2048]{1,0:T(8,128)(2,1)S(1)}, bf16[96,2048]{1,0:T(8,128)(2,1)S(1)}, u32[]{:S(2)}, u32[]{:S(2)}) collective-permute-start(bf16[96,2048]{1,0:T(8,128)(2,1)S(1)} %collective-permute-done.15.refs_0_), channel_id=1, source_target_pairs={{0,1},{1,0},{2,3},{3,2},{4,5},{5,4},{6,7},{7,6},{8,9},{9,8},{10,11... | collective-permute-start | bytes 1179656 | tf_op jit(solution)/shard_map/ppermute | solution.py:24
  145.3 3.9 %collective-permute-start.18 = (bf16[96,2048]{1,0:T(8,128)(2,1)S(1)}, bf16[96,2048]{1,0:T(8,128)(2,1)S(1)}, u32[]{:S(2)}, u32[]{:S(2)}) collective-permute-start(bf16[96,2048]{1,0:T(8,128)(2,1)S(1)} %collective-permute-done.16.refs_1_), channel_id=1, source_target_pairs={{0,1},{1,0},{2,3},{3,2},{4,5},{5,4},{6,7},{7,6},{8,9},{9,8},{10,11... | collective-permute-start | bytes 1179656 | tf_op jit(solution)/shard_map/ppermute | solution.py:24
  145.8 8.1 %collective-permute-start.19 = (bf16[48,2048]{1,0:T(8,128)(2,1)S(1)}, bf16[48,2048]{1,0:T(8,128)(2,1)S(1)}, u32[]{:S(2)}, u32[]{:S(2)}) collective-permute-start(bf16[48,2048]{1,0:T(8,128)(2,1)S(1)} %slice.14), channel_id=1, source_target_pairs={{0,2},{2,4},{4,6},{6,0},{1,3},{3,5},{5,7},{7,1},{8,10},{10,12},{12... | collective-permute-start | bytes 589832 | tf_op jit(solution)/shard_map/ppermute | solution.py:24
  146.5 7.4 %collective-permute-start.20 = (bf16[48,2048]{1,0:T(8,128)(2,1)S(1)}, bf16[48,2048]{1,0:T(8,128)(2,1)S(1)}, u32[]{:S(2)}, u32[]{:S(2)}) collective-permute-start(bf16[48,2048]{1,0:T(8,128)(2,1)S(1)} %slice.15), channel_id=1, source_target_pairs={{0,6},{2,0},{4,2},{6,4},{1,7},{3,1},{5,3},{7,5},{8,14},{10,8},{12,... | collective-permute-start | bytes 589832 | tf_op jit(solution)/shard_map/ppermute | solution.py:24
  151.8 5.3 %copy-start.3 = (bf16[384,704]{1,0:T(8,128)(2,1)}, bf16[384,704]{1,0:T(8,128)(2,1)S(1)}, u32[]{:S(2)}) copy-start(bf16[384,704]{1,0:T(8,128)(2,1)S(1)} %get-tuple-element.123.refs_2_.refs_8_) | copy-start | bytes 1622020
  151.8 5.3 %copy-start.5 = (bf16[384,704]{1,0:T(8,128)(2,1)}, bf16[384,704]{1,0:T(8,128)(2,1)S(1)}, u32[]{:S(2)}) copy-start(bf16[384,704]{1,0:T(8,128)(2,1)S(1)} %get-tuple-element.124.refs_3_.refs_9_) | copy-start | bytes 1622020
  153.9 1.4 collective-permute-start.21
  153.9 1.7 collective-permute-start.22
  158.5 22.9 %copy-start.21 = (f32[3,704]{1,0:T(4,128)S(1)}, f32[3,704]{1,0:T(4,128)}, u32[]{:S(2)}) copy-start(f32[3,704]{1,0:T(4,128)} %refs_0_.3) | copy-start | bytes 25348
  158.5 22.9 %copy-start.22 = (f32[3,704]{1,0:T(4,128)S(1)}, f32[3,704]{1,0:T(4,128)}, u32[]{:S(2)}) copy-start(f32[3,704]{1,0:T(4,128)} %refs_1_.6) | copy-start | bytes 25348
  158.5 22.9 %copy-start.24 = (s32[2]{0:T(128)S(1)}, s32[2]{0:T(128)}, u32[]{:S(2)}) copy-start(s32[2]{0:T(128)} %copy-done.23) | copy-start | bytes 28
  158.5 22.9 %copy-start.12 = (bf16[192,704]{1,0:T(8,128)(2,1)S(1)}, bf16[192,704]{1,0:T(8,128)(2,1)}, u32[]{:S(2)}) copy-start(bf16[192,704]{1,0:T(8,128)(2,1)} %copy-done.11) | copy-start | bytes 811012
  158.5 23.0 %copy-start.14 = (bf16[192,704]{1,0:T(8,128)(2,1)S(1)}, bf16[192,704]{1,0:T(8,128)(2,1)}, u32[]{:S(2)}) copy-start(bf16[192,704]{1,0:T(8,128)(2,1)} %copy-done.13) | copy-start | bytes 811012
  161.0 20.5 %collective-permute-start.23 = (bf16[32,704]{1,0:T(8,128)(2,1)}, bf16[32,704]{1,0:T(8,128)(2,1)S(1)}, u32[]{:S(2)}, u32[]{:S(2)}) collective-permute-start(bf16[32,704]{1,0:T(8,128)(2,1)} %get-tuple-element.116), channel_id=1, source_target_pairs={{0,8},{8,16},{16,24},{24,32},{32,40},{40,48},{48,56},{56,64},{64,7... | collective-permute-start | bytes 135176 | tf_op jit(solution)/shard_map/ppermute | solution.py:30
  183.3 9.8 %copy-start.10 = (bf16[192,704]{1,0:T(8,128)(2,1)S(1)}, bf16[192,704]{1,0:T(8,128)(2,1)}, u32[]{:S(2)}) copy-start(bf16[192,704]{1,0:T(8,128)(2,1)} %copy-done.9) | copy-start | bytes 811012
  183.3 9.8 %copy-start.17 = (bf16[8,16,704]{2,1,0:T(8,128)(2,1)S(1)}, bf16[8,16,704]{2,1,0:T(8,128)(2,1)}, u32[]{:S(2)}) copy-start(bf16[8,16,704]{2,1,0:T(8,128)(2,1)} %get-tuple-element.117.refs_4_) | copy-start | bytes 540676
  183.3 9.8 %copy-start.19 = (bf16[8,16,704]{2,1,0:T(8,128)(2,1)S(1)}, bf16[8,16,704]{2,1,0:T(8,128)(2,1)}, u32[]{:S(2)}) copy-start(bf16[8,16,704]{2,1,0:T(8,128)(2,1)} %get-tuple-element.118.refs_5_) | copy-start | bytes 540676
  188.5 4.6 %copy-start.4 = (bf16[384,704]{1,0:T(8,128)(2,1)S(1)}, bf16[384,704]{1,0:T(8,128)(2,1)}, u32[]{:S(2)}) copy-start(bf16[384,704]{1,0:T(8,128)(2,1)} %copy-done.3) | copy-start | bytes 1622020
  188.5 4.6 %copy-start.6 = (bf16[384,704]{1,0:T(8,128)(2,1)S(1)}, bf16[384,704]{1,0:T(8,128)(2,1)}, u32[]{:S(2)}) copy-start(bf16[384,704]{1,0:T(8,128)(2,1)} %copy-done.5) | copy-start | bytes 1622020
  188.5 4.6 %copy-start.8 = (bf16[192,704]{1,0:T(8,128)(2,1)S(1)}, bf16[192,704]{1,0:T(8,128)(2,1)}, u32[]{:S(2)}) copy-start(bf16[192,704]{1,0:T(8,128)(2,1)} %copy-done.7) | copy-start | bytes 811012
  188.5 1.7 collective-permute-start.24
  193.1 7.3 %copy-start.30 = (bf16[96,2048]{1,0:T(8,128)(2,1)S(1)}, bf16[96,2048]{1,0:T(8,128)(2,1)}, u32[]{:S(2)}) copy-start(bf16[96,2048]{1,0:T(8,128)(2,1)} %shard_map.210) | copy-start | bytes 1179652
  200.3 3.1 %collective-permute-start.25 = (bf16[3,96,2048]{2,1,0:T(8,128)(2,1)S(1)}, bf16[3,96,2048]{2,1,0:T(8,128)(2,1)S(1)}, u32[]{:S(2)}, u32[]{:S(2)}) collective-permute-start(bf16[3,96,2048]{2,1,0:T(8,128)(2,1)S(1)} %get-tuple-element.126), channel_id=1, source_target_pairs={{0,1},{1,0},{2,3},{3,2},{4,5},{5,4},{6,7},{7,6},{8,9},{9,8},{10,11... | collective-permute-start | bytes 3538952 | tf_op jit(solution)/shard_map/ppermute | solution.py:24
  200.4 13.2 %collective-permute-start.26 = (bf16[96,2048]{1,0:T(8,128)(2,1)S(1)}, bf16[96,2048]{1,0:T(8,128)(2,1)S(1)}, u32[]{:S(2)}, u32[]{:S(2)}) collective-permute-start(bf16[96,2048]{1,0:T(8,128)(2,1)S(1)} %copy-done.30), channel_id=1, source_target_pairs={{0,4},{2,6},{4,0},{6,2},{1,5},{3,7},{5,1},{7,3},{8,12},{10,14},{12... | collective-permute-start | bytes 1179656 | tf_op jit(solution)/shard_map/ppermute | solution.py:24
  203.3 1.1 copy-start.26
  207.6 14.5 %collective-permute-start.27 = (bf16[96,2048]{1,0:T(8,128)(2,1)}, bf16[96,2048]{1,0:T(8,128)(2,1)S(1)}, u32[]{:S(2)}, u32[]{:S(2)}) collective-permute-start(bf16[96,2048]{1,0:T(8,128)(2,1)} %get-tuple-element.129), channel_id=1, source_target_pairs={{0,6},{2,0},{4,2},{6,4},{1,7},{3,1},{5,3},{7,5},{8,14},{10,8},{12,... | collective-permute-start | bytes 1179656 | tf_op jit(solution)/shard_map/ppermute | solution.py:24
  210.4 12.3 %collective-permute-start.28 = (bf16[96,2048]{1,0:T(8,128)(2,1)}, bf16[96,2048]{1,0:T(8,128)(2,1)S(1)}, u32[]{:S(2)}, u32[]{:S(2)}) collective-permute-start(bf16[96,2048]{1,0:T(8,128)(2,1)} %get-tuple-element.130), channel_id=1, source_target_pairs={{0,2},{2,4},{4,6},{6,0},{1,3},{3,5},{5,7},{7,1},{8,10},{10,12},{12... | collective-permute-start | bytes 1179656 | tf_op jit(solution)/shard_map/ppermute | solution.py:24
  213.6 9.1 %copy-start.32 = (bf16[96,2048]{1,0:T(8,128)(2,1)}, bf16[96,2048]{1,0:T(8,128)(2,1)S(1)}, u32[]{:S(2)}) copy-start(bf16[96,2048]{1,0:T(8,128)(2,1)S(1)} %collective-permute-done.26.refs_2_) | copy-start | bytes 1179652
  (10 other events, 8.1 us)
Sparse Core Ops, SparseCore 0:
  26.4 88.8 all-gather.1

commit v2 on v1

--- a/solution.py
+++ b/solution.py
@@ -349,7 +349,7 @@
         out_specs=out_specs,
         scratch_shapes=scratch,
         out_shape=out_shape,
-        compiler_params=pltpu.CompilerParams(vmem_limit_bytes=58 * 2**20),
+        compiler_params=pltpu.CompilerParams(vmem_limit_bytes=30 * 2**20),
         cost_estimate=cost_of(cost),
     )(*args)
 
@@ -399,7 +399,7 @@
         out_specs=vm,
         scratch_shapes=[pltpu.VMEM((own, wide), f32)],
         out_shape=jax.ShapeDtypeStruct((own, wide), bf16),
-        compiler_params=pltpu.CompilerParams(vmem_limit_bytes=40 * 2**20),
+        compiler_params=pltpu.CompilerParams(vmem_limit_bytes=24 * 2**20),
         cost_estimate=cost_of(5.0),
     )(place, arrived, *[m[0] for m in mixers], residual, gain.reshape(1, wide))
 
@@ -434,54 +434,51 @@
     return pl.BlockSpec(array.shape, lambda i: (0,) * array.ndim)
 
 
-def ups(chunks, weights, width, cost):
+def ups(chunks, weights, width, cost, earlier=(), place=None, spots=(), turns=0, cores=0):
     rows = sum(c.shape[0] for c in chunks)
+    own = chunks[0].shape[0] * len(chunks) // 2 if earlier else 0
+    flat = [a for pair in earlier for a in pair]
 
     def body(*refs):
-        value_ref, gate_ref, out_value, out_gate = refs[len(chunks) :]
-        x = jnp.concatenate([r[...] for r in refs[: len(chunks)]], axis=0)
-        for ref, out in ((value_ref, out_value), (gate_ref, out_gate)):
+        place_ref, chunk_refs = refs[0], refs[1 : 1 + len(chunks)]
+        value_ref, gate_ref = refs[1 + len(chunks) : 3 + len(chunks)]
+        done = refs[3 + len(chunks) : 3 + len(chunks) + len(flat)]
+        outs = refs[3 + len(chunks) + len(flat) :]
+        x = jnp.concatenate([r[...] for r in chunk_refs], axis=0)
+        for ref, out in ((value_ref, outs[0]), (gate_ref, outs[1])):
             out[...] = jnp.dot(x, ref[:, :width], preferred_element_type=f32).astype(bf16)
-
-    shape = jax.ShapeDtypeStruct((rows, width), bf16)
-    return pl.pallas_call(
-        body,
-        grid=(1,),
-        in_specs=[whole(c) for c in chunks] + [window(weights, 0), window(weights, 1)],
-        out_specs=[whole(shape)] * 2,
-        out_shape=[shape] * 2,
-        compiler_params=pltpu.CompilerParams(vmem_limit_bytes=40 * 2**20),
-        cost_estimate=cost_of(cost),
-    )(*chunks, weights, weights)
-
-
-def ends(place, pieces, spots, own, turns, cores):
-    width = pieces[0][0].shape[1]
-
-    def body(place_ref, *refs):
-        outs, leaving = refs[-3:-1], refs[-1]
+        if not earlier:
+            return
+        tails, leaving = outs[2:4], outs[4]
+        pieces = (*done, *outs[:2])
         spot = 0
-        for k in range(0, len(refs) - 3, 2):
-            for i in range(refs[k].shape[0] // own):
+        for k in range(0, len(pieces), 2):
+            for i in range(pieces[k].shape[0] // own):
                 shift, other = spots[spot]
                 spot += 1
                 y = lax.rem(place_ref[0] + shift + turns, turns)
                 core = place_ref[1] if other == 0 else 1 - place_ref[1]
                 for side in range(2):
-                    outs[side][y * cores + core] = refs[k + side][(i + 1) * own - LEAD : (i + 1) * own]
+                    tails[side][y * cores + core] = pieces[k + side][(i + 1) * own - LEAD : (i + 1) * own]
         for side in range(2):
-            leaving[side * LEAD : (side + 1) * LEAD] = outs[side][turns * cores - 1]
-
-    vm = pl.BlockSpec(memory_space=pltpu.VMEM)
-    flat = [a for pair in pieces for a in pair]
+            leaving[side * LEAD : (side + 1) * LEAD] = tails[side][turns * cores - 1]
+
+    shapes = [jax.ShapeDtypeStruct((rows, width), bf16)] * 2
+    if earlier:
+        shapes += [jax.ShapeDtypeStruct((turns * cores, LEAD, width), bf16)] * 2
+        shapes.append(jax.ShapeDtypeStruct((2 * LEAD, width), bf16))
     return pl.pallas_call(
         body,
-        in_specs=[pl.BlockSpec(memory_space=pltpu.SMEM)] + [vm] * len(flat),
-        out_specs=[vm] * 3,
-        out_shape=[jax.ShapeDtypeStruct((turns * cores, LEAD, width), bf16)] * 2
-        + [jax.ShapeDtypeStruct((2 * LEAD, width), bf16)],
-        cost_estimate=cost_of(1.5),
-    )(place, *flat)
+        grid=(1,),
+        in_specs=[pl.BlockSpec(memory_space=pltpu.SMEM)]
+        + [whole(c) for c in chunks]
+        + [window(weights, 0), window(weights, 1)]
+        + [whole(a) for a in flat],
+        out_specs=[whole(x) for x in shapes],
+        out_shape=shapes,
+        compiler_params=pltpu.CompilerParams(vmem_limit_bytes=24 * 2**20),
+        cost_estimate=cost_of(cost),
+    )(place, *chunks, weights, weights, *flat)
 
 
 def downs(place, pieces, groups, tails, halo, value_taps, gate_taps, weights, own, turns, cores, cost):
@@ -542,7 +539,7 @@
             pltpu.VMEM((count * own, width), bf16),
             pltpu.VMEM((count * own, wide), f32),
         ],
-        compiler_params=pltpu.CompilerParams(vmem_limit_bytes=50 * 2**20),
+        compiler_params=pltpu.CompilerParams(vmem_limit_bytes=24 * 2**20),
         cost_estimate=cost_of(cost),
     )(place, value_taps, gate_taps, weights, halo, *tails, *flat)
 
@@ -634,7 +631,7 @@
     after = shifted(pairs, "sp_x", -1)
     queries = [asked[0]] + [shifted(asked[k], "sp_z", k) for k in range(1, depth)]
     mixer = jnp.concatenate([mixer_small, mixer_large], axis=0)
-    mixers = [mixer, shifted(mixer, "tp_y", 1), shifted(mixer, "tp_y", -1)]
+    mixers = [mixer] + [shifted(mixer, "tp_y", k) for k in (1, -1, 2)]
     calls = ((0,), (-1, 1), (2,))
     tables = work_tables(calls, depth, turns)
     place_here = jnp.stack([slot, column])
@@ -650,21 +647,18 @@
         12.0 * len(calls[k]),
     )
     state = call(0, [pairs], None)
-    before, after, state, mixers = lax.optimization_barrier((before, after, state, mixers))
-    far = [
-        shifted(before[: depth // 2], "sp_x", 1),
-        shifted(after[depth // 2 :], "sp_x", -1),
-    ]
-    mixers.append(shifted(mixers[1], "tp_y", 1))
+    pairs, before, after, state = lax.optimization_barrier((pairs, before, after, state))
+    far = shifted(pairs, "sp_x", 2)
     state = call(1, [before, after], state)
     far, state, mixers = lax.optimization_barrier((far, state, mixers))
     shifts = (0, -1, 1, 2)
     mixers = [(a, shift, 0) for a, shift in zip(mixers, shifts)] + [
         (shifted(a, "tp_c", 1), shift, 1) for a, shift in zip(mixers, shifts)
     ]
-    state = call(2, far, state)
+    state = call(2, [far], state)
     arrived = lax.all_to_all(state, ("sp_z",) + TP, split_axis=0, concat_axis=0, tiled=True)
     place = jnp.stack([lax.axis_index("tp_y"), lax.axis_index("tp_c")]).astype(jnp.int32)
+    arrived, weights = lax.optimization_barrier((arrived, weights))
     mixed = mix_rows(place, arrived, mixers, residual, mix_gain)
     turns_y, cores = lax.axis_size("tp_y"), lax.axis_size("tp_c")
     own_rows = mixed.shape[0]
@@ -672,15 +666,17 @@
     width = value_weight.shape[1]
     spots = [(0, 0), (0, 1), (-1, 0), (1, 0), (-1, 1), (1, 1), (2, 0), (2, 1)]
     last_one, next_one = shifted(mixed, "tp_y", 1), shifted(mixed, "tp_y", -1)
-    near = ups([mixed, shifted(mixed, "tp_c", 1)], weights, width, 3.0)
+    near = ups([mixed, shifted(mixed, "tp_c", 1)], weights, width, 3.0, place=place)
     near, last_one, next_one = lax.optimization_barrier((near, last_one, next_one))
     opposite = [shifted(last_one[:half], "tp_y", 1), shifted(next_one[half:], "tp_y", -1)]
     beside = [last_one, next_one] + [shifted(a, "tp_c", 1) for a in (last_one, next_one)]
-    beside = ups(beside, weights, width, 4.0)
+    beside = ups(beside, weights, width, 4.0, place=place)
     beside, opposite = lax.optimization_barrier((beside, opposite))
-    opposite = ups(opposite + [shifted(a, "tp_c", 1) for a in opposite], weights, width, 3.0)
-    pieces = [near, beside, opposite]
-    *tails, leaving = ends(place, pieces, spots, own_rows, turns_y, cores)
+    opposite += [shifted(a, "tp_c", 1) for a in opposite]
+    up_value, up_gate, *tails, leaving = ups(
+        opposite, weights, width, 3.0, (near, beside), place, spots, turns_y, cores
+    )
+    opposite = [up_value, up_gate]
     halo = passed_along(leaving, SP, 1)
     down = lambda chosen, groups, cost: downs(
         place,

time: 234 us -> 221 us (0.944)
  the two profiles are of different devices: /device:TPU:32 before, /device:TPU:0 now
where the time goes in v2:
time: 221 us; the launch traced here: 219 us
  waiting for transfers between devices  89.5 us (40%)
  Pallas kernels  59.7 us (27%)
  starting transfers between devices  46.9 us (21%)
  between operations  13.7 us (6%)
  local copies, waits for them, and re-layouts  9.57 us (4%)
    ppermute x27, waiting for transfers between devices, shifted(): lax.ppermute(value, axis, [(i, (i + steps) % count) for i in range(count)])  47.7 us
    ppermute x27, starting transfers between devices, shifted(): lax.ppermute(value, axis, [(i, (i + steps) % count) for i in range(count)])  30.4 us
    pallas_call x3, Pallas kernels, attend(): pl.pallas_call(body, in_specs=[sm, sm] + [vm] * (len(args) - 2), out_spec...  27.3 us
    all_to_all x1, waiting for transfers between devices, per_device(): lax.all_to_all(state, ('sp_z',) + TP, split_axis=0, concat_axis=0, tiled=...  17 us
    all_gather x1, waiting for transfers between devices, per_device(): weights = lax.all_gather(shards, SP, axis=0, tiled=True)  12.9 us
    all_to_all x1, waiting for transfers between devices, per_device(): lax.all_to_all(packed, 'sp_z', split_axis=0, concat_axis=0, tiled=True)  10.3 us
    unnamed x49, local copies, waits for them, and re-layouts  9.5 us
    all_to_all x1, starting transfers between devices, per_device(): lax.all_to_all(state, ('sp_z',) + TP, split_axis=0, concat_axis=0, tiled=...  7.3 us
  transfers between devices with their start and end apart: 31, of which 17 were waited for; matrix products, arithmetic and copies ran while one was open for 0% of the time, Pallas kernels for 17%

profile of v2, /device:TPU:0, one launch (start us, length us, event | category | flops | bytes accessed | tf_op | source)
XLA Modules:
  0.0 219.5 jit_solution(4394379838230967396)
XLA Ops:
  6.5 2.9 %shard_map.199 = (bf16[4,800,128]{2,1,0:T(8,128)(2,1)}, bf16[768,128]{1,0:T(8,128)(2,1)}, bf16[768,128]{1,0:T(8,128)(2,1)}, bf16[768,128]{1,0:T(8,128)(2,1)}, bf16[768,128]{1,0:T(8,128)(2,1)}) custom-call(s32[1]{0:T(128)} %bitcast.2.slot_ref, bf16[768,128]{1,0:T(8,128)(2,1)} %ks.1, bf16[768,128]{1,0:T(8,128)(2,1)} %vs.1, bf16[768,128]{1,0:T(8,128)(2,1)} %kl.1, ...), custom_call_target="tpu_custom_call" | custom-call | flops 625000000 | tf_op jit(solution)/shard_map/pallas_call | solution.py:89
  9.5 5.6 %all-to-all-start = ((bf16[4,800,128]{2,1,0:T(8,128)(2,1)}), bf16[4,800,128]{2,1,0:T(8,128)(2,1)S(1)}, u32[]{:S(2)}, u32[]{:S(2)}) async-start(bf16[4,800,128]{2,1,0:T(8,128)(2,1)} %get-tuple-element.68), calls=%async_computation | async-start | bytes 1638400 | tf_op jit(solution)/shard_map/all_to_all | solution.py:626
  15.1 2.3 %shard_map.200 = bf16[128,2304]{1,0:T(8,128)(2,1)} custom-call(bf16[704,128]{1,0:T(8,128)(2,1)} %bitcast.12, bf16[704,128]{1,0:T(8,128)(2,1)} %bitcast.13, bf16[704,128]{1,0:T(8,128)(2,1)} %d), custom_call_target="tpu_custom_call" | custom-call | flops 375000000 | tf_op jit(solution)/shard_map/pallas_call | solution.py:420
  17.4 10.3 %all-to-all-done.refs_6_ = bf16[4,800,128]{2,1,0:T(8,128)(2,1)S(1)} async-done(((bf16[4,800,128]{2,1,0:T(8,128)(2,1)}), bf16[4,800,128]{2,1,0:T(8,128)(2,1)S(1)}, u32[]{:S(2)}, u32[]{:S(2)}) %all-to-all-start) | async-done | bytes 819232 | tf_op jit(solution)/shard_map/all_to_all | solution.py:626
  27.7 1.6 collective-permute-start.3
  29.3 1.7 collective-permute-start.4
  31.1 0.6 collective-permute-start
  31.8 2.1 collective-permute-start.1
  33.8 0.7 collective-permute-start.2
  34.6 7.2 %collective-permute-done.refs_3_ = bf16[768,128]{1,0:T(8,128)(2,1)S(1)} collective-permute-done((bf16[768,128]{1,0:T(8,128)(2,1)}, bf16[768,128]{1,0:T(8,128)(2,1)S(1)}, u32[]{:S(2)}, u32[]{:S(2)}) %collective-permute-start) | collective-permute-done | bytes 196640 | tf_op jit(solution)/shard_map/ppermute | solution.py:24
  41.8 1.6 collective-permute-start.6
  43.4 1.6 collective-permute-start.7
  45.0 0.2 collective-permute-done.2.refs_5_
  45.2 3.3 %collective-permute-start.8 = (bf16[256,2048]{1,0:T(8,128)(2,1)S(1)}, bf16[256,2048]{1,0:T(8,128)(2,1)}, u32[]{:S(2)}, u32[]{:S(2)}) collective-permute-start(bf16[256,2048]{1,0:T(8,128)(2,1)S(1)} %constant_dynamic-update-slice_fusion.refs_0_), channel_id=1, source_target_pairs={{0,4},{2,6},{4,0},{6,2},{1,5},{3,7},{5,1},{7,3},{8,12},{10,14},{12... | collective-permute-start | bytes 3145736 | tf_op jit(solution)/shard_map/ppermute | solution.py:24
  48.6 9.4 %shard_map.201 = (f32[4,144,768]{2,1,0:T(8,128)S(1)}, f32[4,8,768]{2,1,0:T(8,128)S(1)}) custom-call(s32[2]{0:T(128)S(1)} %pad_add_fusion.1.refs_0_, s32[4,34]{1,0:T(4,128)S(1)} %copy-done.12, bf16[768,128]{1,0:T(8,128)(2,1)S(1)} %copy-done.13, bf16[768,128]{1,0:T(8,128)(2,1)S(1)} %collective-permute-done.refs_3_, ...), custom_call_target="tpu_custom_call" | custom-call | flops 3000000000 | tf_op jit(solution)/shard_map/pallas_call | solution.py:346
  58.0 7.4 %collective-permute-done.4.refs_7_ = bf16[4,800,128]{2,1,0:T(8,128)(2,1)S(1)} collective-permute-done((bf16[4,800,128]{2,1,0:T(8,128)(2,1)S(1)}, bf16[4,800,128]{2,1,0:T(8,128)(2,1)S(1)}, u32[]{:S(2)}, u32[]{:S(2)}) %collective-permute-start.4) | collective-permute-done | bytes 819232 | tf_op jit(solution)/shard_map/ppermute | solution.py:24
  65.4 2.5 %collective-permute-start.5 = (bf16[4,800,128]{2,1,0:T(8,128)(2,1)S(1)}, bf16[4,800,128]{2,1,0:T(8,128)(2,1)S(1)}, u32[]{:S(2)}, u32[]{:S(2)}) collective-permute-start(bf16[4,800,128]{2,1,0:T(8,128)(2,1)S(1)} %all-to-all-done.refs_6_), channel_id=1, source_target_pairs={{0,16},{8,24},{16,0},{24,8},{1,17},{9,25},{17,1},{25,9},{2,18},{10... | collective-permute-start | bytes 2457608 | tf_op jit(solution)/shard_map/ppermute | solution.py:24
  67.9 11.0 %shard_map.202 = (f32[4,144,768]{2,1,0:T(8,128)S(1)}, f32[4,8,768]{2,1,0:T(8,128)S(1)}) custom-call(s32[2]{0:T(128)S(1)} %pad_add_fusion.1.refs_0_, s32[4,64]{1,0:T(4,128)S(1)} %copy-done.11, bf16[768,128]{1,0:T(8,128)(2,1)S(1)} %copy-done.13, bf16[768,128]{1,0:T(8,128)(2,1)S(1)} %collective-permute-done.refs_3_, ...), custom_call_target="tpu_custom_call" | custom-call | flops 6000000000 | tf_op jit(solution)/shard_map/pallas_call | solution.py:346
  79.0 7.3 %collective-permute-done.7.refs_2_ = bf16[256,2048]{1,0:T(8,128)(2,1)} collective-permute-done((bf16[256,2048]{1,0:T(8,128)(2,1)S(1)}, bf16[256,2048]{1,0:T(8,128)(2,1)}, u32[]{:S(2)}, u32[]{:S(2)}) %collective-permute-start.7) | collective-permute-done | bytes 1048608 | tf_op jit(solution)/shard_map/ppermute | solution.py:24
  86.3 1.3 collective-permute-done.8.refs_3_
  87.6 0.5 collective-permute-start.10
  88.1 0.5 collective-permute-start.12
  88.6 6.9 %shard_map.203 = bf16[32,112,128]{2,1,0:T(8,128)(2,1)S(1)} custom-call(s32[2]{0:T(128)S(1)} %pad_add_fusion.1.refs_0_, s32[4,34]{1,0:T(4,128)S(1)} %copy-done.10, bf16[768,128]{1,0:T(8,128)(2,1)S(1)} %copy-done.13, bf16[768,128]{1,0:T(8,128)(2,1)S(1)} %collective-permute-done.refs_3_, bf16[768,128]{1,0:T(8,128)(2,1)S(1)} %collective-permute-done.1.refs_4_, ...), custom_call_target="tpu_custom_call" | custom-call | flops 3000000000 | tf_op jit(solution)/shard_map/pallas_call | solution.py:346
  95.5 0.9 copy-done.4
  96.4 7.3 %all-to-all-start.1 = ((bf16[32,112,128]{2,1,0:T(8,128)(2,1)}), bf16[32,112,128]{2,1,0:T(8,128)(2,1)S(1)}, u32[]{:S(2)}, u32[]{:S(2)}) async-start(bf16[32,112,128]{2,1,0:T(8,128)(2,1)} %copy-done.4), calls=%async_computation.1 | async-start | bytes 1835008 | tf_op jit(solution)/shard_map/all_to_all | solution.py:659
  103.8 17.0 %all-to-all-done.1.arrived_ref = bf16[32,112,128]{2,1,0:T(8,128)(2,1)S(1)} async-done(((bf16[32,112,128]{2,1,0:T(8,128)(2,1)}), bf16[32,112,128]{2,1,0:T(8,128)(2,1)S(1)}, u32[]{:S(2)}, u32[]{:S(2)}) %all-to-all-start.1) | async-done | bytes 917536 | tf_op jit(solution)/shard_map/all_to_all | solution.py:659
  120.8 12.9 %all-gather.2.cloned.1.call-done.refs_3_.refs_4_.refs_5_.refs_6_.refs_2_ = bf16[2048,2304]{1,0:T(8,128)(2,1)} async-done(((bf16[128,2304]{1,0:T(8,128)(2,1)}), bf16[2048,2304]{1,0:T(8,128)(2,1)}) %all-gather.2.cloned.1.call-update) | async-done | bytes 9437200 | tf_op jit(solution)/shard_map/all_gather | solution.py:629
  133.8 4.9 %shard_map.204.refs_1_.refs_0_ = bf16[96,2048]{1,0:T(8,128)(2,1)S(1)} custom-call(s32[2]{0:T(128)S(1)} %pad_add_fusion.place_ref.refs_0_, bf16[32,112,128]{2,1,0:T(8,128)(2,1)S(1)} %all-to-all-done.1.arrived_ref, bf16[256,2048]{1,0:T(8,128)(2,1)S(1)} %constant_dynamic-update-slice_fusion.refs_0_, bf16[256,2048]{1,0:T(8,128)(2,1)S(1)} %collective-permute-done.6.refs_1_, ...), custom_call_target="tpu_custom_call" | custom-call | flops 1250000000 | tf_op jit(solution)/shard_map/pallas_call | solution.py:396
  138.7 0.1 collective-permute-start.13
  138.8 1.6 collective-permute-start.14
  140.3 1.7 collective-permute-start.15
  142.1 1.9 shard_map.205
  144.1 7.5 %collective-permute-done.14.refs_1_ = bf16[96,2048]{1,0:T(8,128)(2,1)S(1)} collective-permute-done((bf16[96,2048]{1,0:T(8,128)(2,1)S(1)}, bf16[96,2048]{1,0:T(8,128)(2,1)S(1)}, u32[]{:S(2)}, u32[]{:S(2)}) %collective-permute-start.14) | collective-permute-done | bytes 393248 | tf_op jit(solution)/shard_map/ppermute | solution.py:24
  151.5 0.5 collective-permute-start.17
  152.1 1.5 collective-permute-start.18
  153.6 1.8 collective-permute-start.19
  155.4 3.1 %shard_map.206 = (bf16[384,704]{1,0:T(8,128)(2,1)S(1)}, bf16[384,704]{1,0:T(8,128)(2,1)S(1)}) custom-call(s32[2]{0:T(128)S(1)} %pad_add_fusion.place_ref.refs_0_, bf16[96,2048]{1,0:T(8,128)(2,1)S(1)} %collective-permute-done.14.refs_1_, bf16[96,2048]{1,0:T(8,128)(2,1)S(1)} %collective-permute-done.15.refs_2_, ...), custom_call_target="tpu_custom_call" | custom-call | flops 1000000000 | tf_op jit(solution)/shard_map/pallas_call | solution.py:470
  158.5 1.6 collective-permute-done.18.refs_1_
  160.2 0.1 collective-permute-start.20
  160.3 0.5 collective-permute-start.21
  160.8 0.9 collective-permute-done.20.refs_3_
  161.7 0.3 collective-permute-done.21.refs_4_
  162.0 2.0 shard_map.207
  163.9 3.6 %collective-permute-start.22 = (bf16[32,704]{1,0:T(8,128)(2,1)S(1)}, bf16[32,704]{1,0:T(8,128)(2,1)S(1)}, u32[]{:S(2)}, u32[]{:S(2)}) collective-permute-start(bf16[32,704]{1,0:T(8,128)(2,1)S(1)} %get-tuple-element.112), channel_id=1, source_target_pairs={{0,8},{8,16},{16,24},{24,32},{32,40},{40,48},{48,56},{56,64},{64,7... | collective-permute-start | bytes 135176 | tf_op jit(solution)/shard_map/ppermute | solution.py:30
  167.5 1.5 collective-permute-done.22.refs_3_
  169.0 2.9 %shard_map.208 = (bf16[1,96,2048]{2,1,0:T(8,128)(2,1)S(1)}, f32[1,96,2048]{2,1,0:T(8,128)S(1)}) custom-call(s32[2]{0:T(128)S(1)} %pad_add_fusion.place_ref.refs_0_, f32[3,704]{1,0:T(4,128)S(1)} %copy-done.7, f32[3,704]{1,0:T(4,128)S(1)} %copy-done.8, bf16[2048,2304]{1,0:T(8,128)(2,1)S(1)} %copy-done, bf16[32,704]{1,0:T(8,128)(2,1)S(1)} %collective-permute-done.22.refs_3_, ...), custom_call_target="tpu_custom_call" | custom-call | flops 1000000000 | tf_op jit(solution)/shard_map/pallas_call | solution.py:530
  171.9 0.9 copy-done.5
  172.8 1.7 collective-permute-done.23.their_ref
  174.5 0.7 copy-done.18
  175.3 2.0 shard_map.209
  177.3 3.7 %copy-done.1 = bf16[2048,2304]{1,0:T(8,128)(2,1)S(1)} copy-done((bf16[2048,2304]{1,0:T(8,128)(2,1)S(1)}, bf16[2048,2304]{1,0:T(8,128)(2,1)}, u32[]{:S(2)}) %copy-start.1) | copy-done | bytes 9437208
  181.0 4.3 %shard_map.210 = (bf16[3,96,2048]{2,1,0:T(8,128)(2,1)S(1)}, f32[3,96,2048]{2,1,0:T(8,128)S(1)}) custom-call(s32[2]{0:T(128)S(1)} %pad_add_fusion.place_ref.refs_0_, f32[3,704]{1,0:T(4,128)S(1)} %copy-done.7, f32[3,704]{1,0:T(4,128)S(1)} %copy-done.8, bf16[2048,2304]{1,0:T(8,128)(2,1)S(1)} %copy-done.1, bf16[32,704]{1,0:T(8,128)(2,1)S(1)} %collective-permute-done.22.refs_3_, ...), custom_call_target="tpu_custom_call" | custom-call | flops 2000000000 | tf_op jit(solution)/shard_map/pallas_call | solution.py:530
  185.3 1.4 copy-done.3
  186.7 0.1 collective-permute-start.24
  186.9 2.8 %collective-permute-start.25 = (bf16[96,2048]{1,0:T(8,128)(2,1)S(1)}, bf16[96,2048]{1,0:T(8,128)(2,1)S(1)}, u32[]{:S(2)}, u32[]{:S(2)}) collective-permute-start(bf16[96,2048]{1,0:T(8,128)(2,1)S(1)} %copy-done.17), channel_id=1, source_target_pairs={{0,4},{2,6},{4,0},{6,2},{1,5},{3,7},{5,1},{7,3},{8,12},{10,14},{12... | collective-permute-start | bytes 1179656 | tf_op jit(solution)/shard_map/ppermute | solution.py:24
  189.7 1.0 copy-done.14
  190.7 3.2 %shard_map.211 = (f32[96,2048]{1,0:T(8,128)}, bf16[96,2048]{1,0:T(8,128)(2,1)}, bf16[96,2048]{1,0:T(8,128)(2,1)}) custom-call(f32[3,96,2048]{2,1,0:T(8,128)} %copy-done.3, bf16[3,96,2048]{2,1,0:T(8,128)(2,1)} %copy-done.14), custom_call_target="tpu_custom_call" | custom-call | flops 525000000 | tf_op jit(solution)/shard_map/pallas_call | solution.py:555
  193.9 2.8 %collective-permute-start.26 = (bf16[96,2048]{1,0:T(8,128)(2,1)}, bf16[96,2048]{1,0:T(8,128)(2,1)S(1)}, u32[]{:S(2)}, u32[]{:S(2)}) collective-permute-start(bf16[96,2048]{1,0:T(8,128)(2,1)} %get-tuple-element.127), channel_id=1, source_target_pairs={{0,6},{2,0},{4,2},{6,4},{1,7},{3,1},{5,3},{7,5},{8,14},{10,8},{12,... | collective-permute-start | bytes 1179656 | tf_op jit(solution)/shard_map/ppermute | solution.py:24
  196.8 3.5 %collective-permute-done.25.refs_2_ = bf16[96,2048]{1,0:T(8,128)(2,1)S(1)} collective-permute-done((bf16[96,2048]{1,0:T(8,128)(2,1)S(1)}, bf16[96,2048]{1,0:T(8,128)(2,1)S(1)}, u32[]{:S(2)}, u32[]{:S(2)}) %collective-permute-start.25) | collective-permute-done | bytes 393248 | tf_op jit(solution)/shard_map/ppermute | solution.py:24
  200.2 8.3 %collective-permute-done.26.refs_3_ = bf16[96,2048]{1,0:T(8,128)(2,1)S(1)} collective-permute-done((bf16[96,2048]{1,0:T(8,128)(2,1)}, bf16[96,2048]{1,0:T(8,128)(2,1)S(1)}, u32[]{:S(2)}, u32[]{:S(2)}) %collective-permute-start.26) | collective-permute-done | bytes 393248 | tf_op jit(solution)/shard_map/ppermute | solution.py:24
  208.5 0.6 collective-permute-done.27.refs_4_
  209.1 0.2 copy-done.20
  209.2 0.6 copy-done.21
  209.8 2.8 %shard_map.212 = bf16[96,2048]{1,0:T(8,128)(2,1)} custom-call(bf16[96,2048]{1,0:T(8,128)(2,1)} %copy-done.2, f32[96,2048]{1,0:T(8,128)} %get-tuple-element.125.refs_1_, bf16[96,2048]{1,0:T(8,128)(2,1)} %copy-done.19, bf16[96,2048]{1,0:T(8,128)(2,1)} %copy-done.20, bf16[96,2048]{1,0:T(8,128)(2,1)} %copy-done.21, f32[1,2048]{1,0:T(1,128)} %bitcast.11), custom_call_target="tpu_custom_call" | custom-call | flops 500000000 | tf_op jit(solution)/shard_map/pallas_call | solution.py:580
  (67 shorter events, 0.5 us)
Async XLA Ops:
  9.5 21.6 %copy-start.15 = (bf16[128,2048]{1,0:T(8,128)(2,1)S(1)}, bf16[128,2048]{1,0:T(8,128)(2,1)}, u32[]{:S(2)}) copy-start(bf16[128,2048]{1,0:T(8,128)(2,1)} %param.30) | copy-start | bytes 1572868
  9.5 18.2 %all-to-all-start = ((bf16[4,800,128]{2,1,0:T(8,128)(2,1)}), bf16[4,800,128]{2,1,0:T(8,128)(2,1)S(1)}, u32[]{:S(2)}, u32[]{:S(2)}) async-start(bf16[4,800,128]{2,1,0:T(8,128)(2,1)} %get-tuple-element.68), calls=%async_computation | async-start | bytes 1638400 | tf_op jit(solution)/shard_map/all_to_all | solution.py:626
  15.0 16.7 %copy-start.23 = (bf16[768,128]{1,0:T(8,128)(2,1)S(1)}, bf16[768,128]{1,0:T(8,128)(2,1)}, u32[]{:S(2)}) copy-start(bf16[768,128]{1,0:T(8,128)(2,1)} %get-tuple-element.78) | copy-start | bytes 589828
  15.0 18.8 %copy-start.22 = (bf16[768,128]{1,0:T(8,128)(2,1)S(1)}, bf16[768,128]{1,0:T(8,128)(2,1)}, u32[]{:S(2)}) copy-start(bf16[768,128]{1,0:T(8,128)(2,1)} %get-tuple-element.79) | copy-start | bytes 589828
  15.0 19.5 %copy-start.16 = (bf16[128,2048]{1,0:T(8,128)(2,1)S(1)}, bf16[128,2048]{1,0:T(8,128)(2,1)}, u32[]{:S(2)}) copy-start(bf16[128,2048]{1,0:T(8,128)(2,1)} %param.31) | copy-start | bytes 1572868
  15.0 33.5 %copy-start.12 = (s32[4,34]{1,0:T(4,128)S(1)}, s32[4,34]{1,0:T(4,128)}, u32[]{:S(2)}) copy-start(s32[4,34]{1,0:T(4,128)} %constant.21.clone.refs_1_) | copy-start | bytes 1636
  15.0 33.5 %copy-start.13 = (bf16[768,128]{1,0:T(8,128)(2,1)S(1)}, bf16[768,128]{1,0:T(8,128)(2,1)}, u32[]{:S(2)}) copy-start(bf16[768,128]{1,0:T(8,128)(2,1)} %get-tuple-element.76.refs_2_) | copy-start | bytes 589828
  15.1 118.7 %all-gather.2.cloned.1.call-start = ((), (), s32[]{:S(2)}) async-start(), calls=%async_computation.2 | async-start | bytes 10027008 | tf_op jit(solution)/shard_map/all_gather | solution.py:629
  27.7 30.3 %collective-permute-start.3 = (bf16[4,800,128]{2,1,0:T(8,128)(2,1)S(1)}, bf16[4,800,128]{2,1,0:T(8,128)(2,1)S(1)}, u32[]{:S(2)}, u32[]{:S(2)}) collective-permute-start(bf16[4,800,128]{2,1,0:T(8,128)(2,1)S(1)} %all-to-all-done.refs_6_), channel_id=1, source_target_pairs={{0,8},{8,16},{16,24},{24,0},{1,9},{9,17},{17,25},{25,1},{2,10},{10... | collective-permute-start | bytes 2457608 | tf_op jit(solution)/shard_map/ppermute | solution.py:24
  29.3 36.1 %collective-permute-start.4 = (bf16[4,800,128]{2,1,0:T(8,128)(2,1)S(1)}, bf16[4,800,128]{2,1,0:T(8,128)(2,1)S(1)}, u32[]{:S(2)}, u32[]{:S(2)}) collective-permute-start(bf16[4,800,128]{2,1,0:T(8,128)(2,1)S(1)} %all-to-all-done.refs_6_), channel_id=1, source_target_pairs={{0,24},{8,0},{16,8},{24,16},{1,25},{9,1},{17,9},{25,17},{2,26},{10... | collective-permute-start | bytes 2457608 | tf_op jit(solution)/shard_map/ppermute | solution.py:24
  31.1 10.7 %collective-permute-start = (bf16[768,128]{1,0:T(8,128)(2,1)}, bf16[768,128]{1,0:T(8,128)(2,1)S(1)}, u32[]{:S(2)}, u32[]{:S(2)}) collective-permute-start(bf16[768,128]{1,0:T(8,128)(2,1)} %get-tuple-element.77), channel_id=1, source_target_pairs={{0,32},{32,64},{64,96},{96,0},{1,33},{33,65},{65,97},{97,1},{2,34}... | collective-permute-start | bytes 589832 | tf_op jit(solution)/shard_map/ppermute | solution.py:24
  31.8 11.6 %collective-permute-start.1 = (bf16[768,128]{1,0:T(8,128)(2,1)S(1)}, bf16[768,128]{1,0:T(8,128)(2,1)S(1)}, u32[]{:S(2)}, u32[]{:S(2)}) collective-permute-start(bf16[768,128]{1,0:T(8,128)(2,1)S(1)} %copy-done.23), channel_id=1, source_target_pairs={{0,64},{32,96},{64,0},{96,32},{1,65},{33,97},{65,1},{97,33},{2,66}... | collective-permute-start | bytes 589832 | tf_op jit(solution)/shard_map/ppermute | solution.py:24
  33.8 11.4 %collective-permute-start.2 = (bf16[768,128]{1,0:T(8,128)(2,1)S(1)}, bf16[768,128]{1,0:T(8,128)(2,1)S(1)}, u32[]{:S(2)}, u32[]{:S(2)}) collective-permute-start(bf16[768,128]{1,0:T(8,128)(2,1)S(1)} %copy-done.22), channel_id=1, source_target_pairs={{0,96},{32,0},{64,32},{96,64},{1,97},{33,1},{65,33},{97,65},{2,98}... | collective-permute-start | bytes 589832 | tf_op jit(solution)/shard_map/ppermute | solution.py:24
  34.6 33.3 %copy-start.11 = (s32[4,64]{1,0:T(4,128)S(1)}, s32[4,64]{1,0:T(4,128)}, u32[]{:S(2)}) copy-start(s32[4,64]{1,0:T(4,128)} %constant.22.clone.refs_1_) | copy-start | bytes 3076
  41.8 37.2 %collective-permute-start.6 = (bf16[256,2048]{1,0:T(8,128)(2,1)S(1)}, bf16[256,2048]{1,0:T(8,128)(2,1)S(1)}, u32[]{:S(2)}, u32[]{:S(2)}) collective-permute-start(bf16[256,2048]{1,0:T(8,128)(2,1)S(1)} %constant_dynamic-update-slice_fusion.refs_0_), channel_id=1, source_target_pairs={{0,2},{2,4},{4,6},{6,0},{1,3},{3,5},{5,7},{7,1},{8,10},{10,12},{12... | collective-permute-start | bytes 3145736 | tf_op jit(solution)/shard_map/ppermute | solution.py:24
  43.4 42.9 %collective-permute-start.7 = (bf16[256,2048]{1,0:T(8,128)(2,1)S(1)}, bf16[256,2048]{1,0:T(8,128)(2,1)}, u32[]{:S(2)}, u32[]{:S(2)}) collective-permute-start(bf16[256,2048]{1,0:T(8,128)(2,1)S(1)} %constant_dynamic-update-slice_fusion.refs_0_), channel_id=1, source_target_pairs={{0,6},{2,0},{4,2},{6,4},{1,7},{3,1},{5,3},{7,5},{8,14},{10,8},{12,... | collective-permute-start | bytes 3145736 | tf_op jit(solution)/shard_map/ppermute | solution.py:24
  45.2 42.4 %collective-permute-start.8 = (bf16[256,2048]{1,0:T(8,128)(2,1)S(1)}, bf16[256,2048]{1,0:T(8,128)(2,1)}, u32[]{:S(2)}, u32[]{:S(2)}) collective-permute-start(bf16[256,2048]{1,0:T(8,128)(2,1)S(1)} %constant_dynamic-update-slice_fusion.refs_0_), channel_id=1, source_target_pairs={{0,4},{2,6},{4,0},{6,2},{1,5},{3,7},{5,1},{7,3},{8,12},{10,14},{12... | collective-permute-start | bytes 3145736 | tf_op jit(solution)/shard_map/ppermute | solution.py:24
  65.4 23.2 %copy-start.10 = (s32[4,34]{1,0:T(4,128)S(1)}, s32[4,34]{1,0:T(4,128)}, u32[]{:S(2)}) copy-start(s32[4,34]{1,0:T(4,128)} %constant.23.clone.refs_1_) | copy-start | bytes 1636
  65.4 22.2 %collective-permute-start.5 = (bf16[4,800,128]{2,1,0:T(8,128)(2,1)S(1)}, bf16[4,800,128]{2,1,0:T(8,128)(2,1)S(1)}, u32[]{:S(2)}, u32[]{:S(2)}) collective-permute-start(bf16[4,800,128]{2,1,0:T(8,128)(2,1)S(1)} %all-to-all-done.refs_6_), channel_id=1, source_target_pairs={{0,16},{8,24},{16,0},{24,8},{1,17},{9,25},{17,1},{25,9},{2,18},{10... | collective-permute-start | bytes 2457608 | tf_op jit(solution)/shard_map/ppermute | solution.py:24
  87.6 46.1 %collective-permute-start.9 = (bf16[256,2048]{1,0:T(8,128)(2,1)S(1)}, bf16[256,2048]{1,0:T(8,128)(2,1)}, u32[]{:S(2)}, u32[]{:S(2)}) collective-permute-start(bf16[256,2048]{1,0:T(8,128)(2,1)S(1)} %constant_dynamic-update-slice_fusion.refs_0_), channel_id=1, source_target_pairs={{0,1},{1,0},{2,3},{3,2},{4,5},{5,4},{6,7},{7,6},{8,9},{9,8},{10,11... | collective-permute-start | bytes 3145736 | tf_op jit(solution)/shard_map/ppermute | solution.py:24
  87.6 46.1 %collective-permute-start.10 = (bf16[256,2048]{1,0:T(8,128)(2,1)S(1)}, bf16[256,2048]{1,0:T(8,128)(2,1)}, u32[]{:S(2)}, u32[]{:S(2)}) collective-permute-start(bf16[256,2048]{1,0:T(8,128)(2,1)S(1)} %collective-permute-done.6.refs_1_), channel_id=1, source_target_pairs={{0,1},{1,0},{2,3},{3,2},{4,5},{5,4},{6,7},{7,6},{8,9},{9,8},{10,11... | collective-permute-start | bytes 3145736 | tf_op jit(solution)/shard_map/ppermute | solution.py:24
  88.1 45.6 %collective-permute-start.11 = (bf16[256,2048]{1,0:T(8,128)(2,1)}, bf16[256,2048]{1,0:T(8,128)(2,1)}, u32[]{:S(2)}, u32[]{:S(2)}) collective-permute-start(bf16[256,2048]{1,0:T(8,128)(2,1)} %collective-permute-done.7.refs_2_), channel_id=1, source_target_pairs={{0,1},{1,0},{2,3},{3,2},{4,5},{5,4},{6,7},{7,6},{8,9},{9,8},{10,11... | collective-permute-start | bytes 3145736 | tf_op jit(solution)/shard_map/ppermute | solution.py:24
  88.1 45.6 %collective-permute-start.12 = (bf16[256,2048]{1,0:T(8,128)(2,1)}, bf16[256,2048]{1,0:T(8,128)(2,1)}, u32[]{:S(2)}, u32[]{:S(2)}) collective-permute-start(bf16[256,2048]{1,0:T(8,128)(2,1)} %collective-permute-done.8.refs_3_), channel_id=1, source_target_pairs={{0,1},{1,0},{2,3},{3,2},{4,5},{5,4},{6,7},{7,6},{8,9},{9,8},{10,11... | collective-permute-start | bytes 3145736 | tf_op jit(solution)/shard_map/ppermute | solution.py:24
  95.5 0.9 copy-start.4
  96.4 37.3 %copy-start.6 = (bf16[96,2048]{1,0:T(8,128)(2,1)S(1)}, bf16[96,2048]{1,0:T(8,128)(2,1)}, u32[]{:S(2)}) copy-start(bf16[96,2048]{1,0:T(8,128)(2,1)} %refs_8_.1) | copy-start | bytes 1179652
  96.4 37.3 %copy-start.9 = (f32[2048]{0:T(1024)S(1)}, f32[2048]{0:T(1024)}, u32[]{:S(2)}) copy-start(f32[2048]{0:T(1024)} %param.32) | copy-start | bytes 24580
  96.4 24.4 %all-to-all-start.1 = ((bf16[32,112,128]{2,1,0:T(8,128)(2,1)}), bf16[32,112,128]{2,1,0:T(8,128)(2,1)S(1)}, u32[]{:S(2)}, u32[]{:S(2)}) async-start(bf16[32,112,128]{2,1,0:T(8,128)(2,1)} %copy-done.4), calls=%async_computation.1 | async-start | bytes 1835008 | tf_op jit(solution)/shard_map/all_to_all | solution.py:659
  133.8 8.3 %copy-start = (bf16[2048,2304]{1,0:T(8,128)(2,1)S(1)}, bf16[2048,2304]{1,0:T(8,128)(2,1)}, u32[]{:S(2)}) copy-start(bf16[2048,2304]{1,0:T(8,128)(2,1)} %all-gather.2.cloned.1.call-done.refs_3_.refs_4_.refs_5_.refs_6_.refs_2_) | copy-start | bytes 28311556
  138.7 5.4 %copy-start.2 = (bf16[96,2048]{1,0:T(8,128)(2,1)}, bf16[96,2048]{1,0:T(8,128)(2,1)S(1)}, u32[]{:S(2)}) copy-start(bf16[96,2048]{1,0:T(8,128)(2,1)S(1)} %shard_map.204.refs_1_.refs_0_) | copy-start | bytes 1179652
  138.7 3.4 %collective-permute-start.13 = (bf16[96,2048]{1,0:T(8,128)(2,1)S(1)}, bf16[96,2048]{1,0:T(8,128)(2,1)S(1)}, u32[]{:S(2)}, u32[]{:S(2)}) collective-permute-start(bf16[96,2048]{1,0:T(8,128)(2,1)S(1)} %shard_map.204.refs_1_.refs_0_), channel_id=1, source_target_pairs={{0,1},{1,0},{2,3},{3,2},{4,5},{5,4},{6,7},{7,6},{8,9},{9,8},{10,11... | collective-permute-start | bytes 1179656 | tf_op jit(solution)/shard_map/ppermute | solution.py:24
  138.8 12.7 %collective-permute-start.14 = (bf16[96,2048]{1,0:T(8,128)(2,1)S(1)}, bf16[96,2048]{1,0:T(8,128)(2,1)S(1)}, u32[]{:S(2)}, u32[]{:S(2)}) collective-permute-start(bf16[96,2048]{1,0:T(8,128)(2,1)S(1)} %shard_map.204.refs_1_.refs_0_), channel_id=1, source_target_pairs={{0,2},{2,4},{4,6},{6,0},{1,3},{3,5},{5,7},{7,1},{8,10},{10,12},{12... | collective-permute-start | bytes 1179656 | tf_op jit(solution)/shard_map/ppermute | solution.py:24
  140.3 11.2 %collective-permute-start.15 = (bf16[96,2048]{1,0:T(8,128)(2,1)S(1)}, bf16[96,2048]{1,0:T(8,128)(2,1)S(1)}, u32[]{:S(2)}, u32[]{:S(2)}) collective-permute-start(bf16[96,2048]{1,0:T(8,128)(2,1)S(1)} %shard_map.204.refs_1_.refs_0_), channel_id=1, source_target_pairs={{0,6},{2,0},{4,2},{6,4},{1,7},{3,1},{5,3},{7,5},{8,14},{10,8},{12,... | collective-permute-start | bytes 1179656 | tf_op jit(solution)/shard_map/ppermute | solution.py:24
  151.5 3.9 %collective-permute-start.16 = (bf16[96,2048]{1,0:T(8,128)(2,1)S(1)}, bf16[96,2048]{1,0:T(8,128)(2,1)S(1)}, u32[]{:S(2)}, u32[]{:S(2)}) collective-permute-start(bf16[96,2048]{1,0:T(8,128)(2,1)S(1)} %collective-permute-done.14.refs_1_), channel_id=1, source_target_pairs={{0,1},{1,0},{2,3},{3,2},{4,5},{5,4},{6,7},{7,6},{8,9},{9,8},{10,11... | collective-permute-start | bytes 1179656 | tf_op jit(solution)/shard_map/ppermute | solution.py:24
  151.5 3.9 %collective-permute-start.17 = (bf16[96,2048]{1,0:T(8,128)(2,1)S(1)}, bf16[96,2048]{1,0:T(8,128)(2,1)S(1)}, u32[]{:S(2)}, u32[]{:S(2)}) collective-permute-start(bf16[96,2048]{1,0:T(8,128)(2,1)S(1)} %collective-permute-done.15.refs_2_), channel_id=1, source_target_pairs={{0,1},{1,0},{2,3},{3,2},{4,5},{5,4},{6,7},{7,6},{8,9},{9,8},{10,11... | collective-permute-start | bytes 1179656 | tf_op jit(solution)/shard_map/ppermute | solution.py:24
  152.1 8.1 %collective-permute-start.18 = (bf16[48,2048]{1,0:T(8,128)(2,1)S(1)}, bf16[48,2048]{1,0:T(8,128)(2,1)S(1)}, u32[]{:S(2)}, u32[]{:S(2)}) collective-permute-start(bf16[48,2048]{1,0:T(8,128)(2,1)S(1)} %slice.6), channel_id=1, source_target_pairs={{0,2},{2,4},{4,6},{6,0},{1,3},{3,5},{5,7},{7,1},{8,10},{10,12},{12... | collective-permute-start | bytes 589832 | tf_op jit(solution)/shard_map/ppermute | solution.py:24
  153.6 6.5 %collective-permute-start.19 = (bf16[48,2048]{1,0:T(8,128)(2,1)S(1)}, bf16[48,2048]{1,0:T(8,128)(2,1)S(1)}, u32[]{:S(2)}, u32[]{:S(2)}) collective-permute-start(bf16[48,2048]{1,0:T(8,128)(2,1)S(1)} %slice.7), channel_id=1, source_target_pairs={{0,6},{2,0},{4,2},{6,4},{1,7},{3,1},{5,3},{7,5},{8,14},{10,8},{12,... | collective-permute-start | bytes 589832 | tf_op jit(solution)/shard_map/ppermute | solution.py:24
  160.2 8.9 %copy-start.7 = (f32[3,704]{1,0:T(4,128)S(1)}, f32[3,704]{1,0:T(4,128)}, u32[]{:S(2)}) copy-start(f32[3,704]{1,0:T(4,128)} %refs_0_.3) | copy-start | bytes 25348
  160.2 8.9 %copy-start.8 = (f32[3,704]{1,0:T(4,128)S(1)}, f32[3,704]{1,0:T(4,128)}, u32[]{:S(2)}) copy-start(f32[3,704]{1,0:T(4,128)} %refs_1_.6) | copy-start | bytes 25348
  160.2 1.5 collective-permute-start.20
  160.3 1.7 collective-permute-start.21
  163.9 5.1 %collective-permute-start.22 = (bf16[32,704]{1,0:T(8,128)(2,1)S(1)}, bf16[32,704]{1,0:T(8,128)(2,1)S(1)}, u32[]{:S(2)}, u32[]{:S(2)}) collective-permute-start(bf16[32,704]{1,0:T(8,128)(2,1)S(1)} %get-tuple-element.112), channel_id=1, source_target_pairs={{0,8},{8,16},{16,24},{24,32},{32,40},{40,48},{48,56},{56,64},{64,7... | collective-permute-start | bytes 135176 | tf_op jit(solution)/shard_map/ppermute | solution.py:30
  171.9 0.9 copy-start.5
  172.8 1.7 collective-permute-start.23
  174.5 0.7 copy-start.18
  177.3 3.7 %copy-start.1 = (bf16[2048,2304]{1,0:T(8,128)(2,1)S(1)}, bf16[2048,2304]{1,0:T(8,128)(2,1)}, u32[]{:S(2)}) copy-start(bf16[2048,2304]{1,0:T(8,128)(2,1)} %all-gather.2.cloned.1.call-done.refs_3_.refs_4_.refs_5_.refs_6_.refs_2_) | copy-start | bytes 28311556
  181.0 5.9 %copy-start.17 = (bf16[96,2048]{1,0:T(8,128)(2,1)S(1)}, bf16[96,2048]{1,0:T(8,128)(2,1)}, u32[]{:S(2)}) copy-start(bf16[96,2048]{1,0:T(8,128)(2,1)} %shard_map.209) | copy-start | bytes 1179652
  185.3 1.4 copy-start.3
  186.7 3.0 %collective-permute-start.24 = (bf16[3,96,2048]{2,1,0:T(8,128)(2,1)S(1)}, bf16[3,96,2048]{2,1,0:T(8,128)(2,1)S(1)}, u32[]{:S(2)}, u32[]{:S(2)}) collective-permute-start(bf16[3,96,2048]{2,1,0:T(8,128)(2,1)S(1)} %get-tuple-element.124), channel_id=1, source_target_pairs={{0,1},{1,0},{2,3},{3,2},{4,5},{5,4},{6,7},{7,6},{8,9},{9,8},{10,11... | collective-permute-start | bytes 3538952 | tf_op jit(solution)/shard_map/ppermute | solution.py:24
  186.9 13.3 %collective-permute-start.25 = (bf16[96,2048]{1,0:T(8,128)(2,1)S(1)}, bf16[96,2048]{1,0:T(8,128)(2,1)S(1)}, u32[]{:S(2)}, u32[]{:S(2)}) collective-permute-start(bf16[96,2048]{1,0:T(8,128)(2,1)S(1)} %copy-done.17), channel_id=1, source_target_pairs={{0,4},{2,6},{4,0},{6,2},{1,5},{3,7},{5,1},{7,3},{8,12},{10,14},{12... | collective-permute-start | bytes 1179656 | tf_op jit(solution)/shard_map/ppermute | solution.py:24
  189.7 1.0 copy-start.14
  193.9 14.5 %collective-permute-start.26 = (bf16[96,2048]{1,0:T(8,128)(2,1)}, bf16[96,2048]{1,0:T(8,128)(2,1)S(1)}, u32[]{:S(2)}, u32[]{:S(2)}) collective-permute-start(bf16[96,2048]{1,0:T(8,128)(2,1)} %get-tuple-element.127), channel_id=1, source_target_pairs={{0,6},{2,0},{4,2},{6,4},{1,7},{3,1},{5,3},{7,5},{8,14},{10,8},{12,... | collective-permute-start | bytes 1179656 | tf_op jit(solution)/shard_map/ppermute | solution.py:24
  196.8 12.3 %collective-permute-start.27 = (bf16[96,2048]{1,0:T(8,128)(2,1)}, bf16[96,2048]{1,0:T(8,128)(2,1)S(1)}, u32[]{:S(2)}, u32[]{:S(2)}) collective-permute-start(bf16[96,2048]{1,0:T(8,128)(2,1)} %get-tuple-element.128), channel_id=1, source_target_pairs={{0,2},{2,4},{4,6},{6,0},{1,3},{3,5},{5,7},{7,1},{8,10},{10,12},{12... | collective-permute-start | bytes 1179656 | tf_op jit(solution)/shard_map/ppermute | solution.py:24
  200.2 8.8 %copy-start.19 = (bf16[96,2048]{1,0:T(8,128)(2,1)}, bf16[96,2048]{1,0:T(8,128)(2,1)S(1)}, u32[]{:S(2)}) copy-start(bf16[96,2048]{1,0:T(8,128)(2,1)S(1)} %collective-permute-done.25.refs_2_) | copy-start | bytes 1179652
  208.5 0.7 copy-start.20
  209.1 0.8 copy-start.21
Sparse Core Ops, SparseCore 0:
  27.8 105.8 all-gather.1

commit v3 on v2

--- a/solution.py
+++ b/solution.py
@@ -411,8 +411,8 @@
 def pack_weights(value_weight, gate_weight, down_weight):
     width, rows = value_weight.shape
 
-    def body(v, g, d, out):
-        for k, part in enumerate((v, g, d)):
+    def body(v, g, d, ups_out, down_out):
+        for out, k, part in ((ups_out, 0, v), (ups_out, 1, g), (down_out, 0, d)):
             out[:, k * BLOCK : k * BLOCK + width] = part[...].T
             out[:, k * BLOCK + width : (k + 1) * BLOCK] = jnp.zeros((rows, BLOCK - width), bf16)
 
@@ -420,8 +420,8 @@
     return pl.pallas_call(
         body,
         in_specs=[vm] * 3,
-        out_specs=vm,
-        out_shape=jax.ShapeDtypeStruct((rows, 3 * BLOCK), bf16),
+        out_specs=[vm, vm],
+        out_shape=[jax.ShapeDtypeStruct((rows, k * BLOCK), bf16) for k in (2, 1)],
         cost_estimate=cost_of(1.5),
     )(value_weight, gate_weight, down_weight)
 
@@ -531,7 +531,7 @@
         body,
         grid=(1,),
         in_specs=[pl.BlockSpec(memory_space=pltpu.SMEM), whole(value_taps), whole(gate_taps)]
-        + [window(weights, 2), whole(halo), whole(tails[0]), whole(tails[1])]
+        + [whole(weights), whole(halo), whole(tails[0]), whole(tails[1])]
         + [whole(a) for a in flat],
         out_specs=[whole(x) for x in shapes],
         out_shape=shapes,
@@ -626,7 +626,7 @@
     pairs = lax.all_to_all(packed, "sp_z", split_axis=0, concat_axis=0, tiled=True)
     shards = pack_weights(value_turned, gate_turned, down_turned)
     pairs, shards, asked = lax.optimization_barrier((pairs, shards, asked))
-    weights = lax.all_gather(shards, SP, axis=0, tiled=True)
+    weights = lax.all_gather(shards[0], SP, axis=0, tiled=True)
     before = shifted(pairs, "sp_x", 1)
     after = shifted(pairs, "sp_x", -1)
     queries = [asked[0]] + [shifted(asked[k], "sp_z", k) for k in range(1, depth)]
@@ -647,7 +647,10 @@
         12.0 * len(calls[k]),
     )
     state = call(0, [pairs], None)
-    pairs, before, after, state = lax.optimization_barrier((pairs, before, after, state))
+    pairs, before, after, state, down_shard = lax.optimization_barrier(
+        (pairs, before, after, state, shards[1])
+    )
+    down_weights = lax.all_gather(down_shard, SP, axis=0, tiled=True)
     far = shifted(pairs, "sp_x", 2)
     state = call(1, [before, after], state)
     far, state, mixers = lax.optimization_barrier((far, state, mixers))
@@ -658,7 +661,6 @@
     state = call(2, [far], state)
     arrived = lax.all_to_all(state, ("sp_z",) + TP, split_axis=0, concat_axis=0, tiled=True)
     place = jnp.stack([lax.axis_index("tp_y"), lax.axis_index("tp_c")]).astype(jnp.int32)
-    arrived, weights = lax.optimization_barrier((arrived, weights))
     mixed = mix_rows(place, arrived, mixers, residual, mix_gain)
     turns_y, cores = lax.axis_size("tp_y"), lax.axis_size("tp_c")
     own_rows = mixed.shape[0]
@@ -666,15 +668,14 @@
     width = value_weight.shape[1]
     spots = [(0, 0), (0, 1), (-1, 0), (1, 0), (-1, 1), (1, 1), (2, 0), (2, 1)]
     last_one, next_one = shifted(mixed, "tp_y", 1), shifted(mixed, "tp_y", -1)
-    near = ups([mixed, shifted(mixed, "tp_c", 1)], weights, width, 3.0, place=place)
-    near, last_one, next_one = lax.optimization_barrier((near, last_one, next_one))
+    near = [mixed, shifted(mixed, "tp_c", 1)]
     opposite = [shifted(last_one[:half], "tp_y", 1), shifted(next_one[half:], "tp_y", -1)]
     beside = [last_one, next_one] + [shifted(a, "tp_c", 1) for a in (last_one, next_one)]
-    beside = ups(beside, weights, width, 4.0, place=place)
-    beside, opposite = lax.optimization_barrier((beside, opposite))
+    first_six = ups(near + beside, weights, width, 5.0, place=place)
+    first_six, opposite = lax.optimization_barrier((first_six, opposite))
     opposite += [shifted(a, "tp_c", 1) for a in opposite]
     up_value, up_gate, *tails, leaving = ups(
-        opposite, weights, width, 3.0, (near, beside), place, spots, turns_y, cores
+        opposite, weights, width, 3.0, (first_six,), place, spots, turns_y, cores
     )
     opposite = [up_value, up_gate]
     halo = passed_along(leaving, SP, 1)
@@ -686,7 +687,7 @@
         halo,
         value_taps,
         gate_taps,
-        weights,
+        down_weights,
         own_rows,
         turns_y,
         cores,
@@ -694,9 +695,9 @@
     )
     theirs, mine = down([opposite], [(0, 0, 1, 2)], 4.0)
     (distant,) = paired(mine, shifted(theirs, "tp_c", 1), [bf16])
-    near, beside, distant = lax.optimization_barrier((near, beside, distant))
+    first_six, distant = lax.optimization_barrier((first_six, distant))
     shares = [shifted(distant, "tp_y", 2)]
-    theirs, mine = down([near, beside], [(0, 0, 1, 0), (1, 0, 2, -1), (1, 1, 3, 1)], 8.0)
+    theirs, mine = down([first_six], [(0, 0, 1, 0), (0, 2, 4, -1), (0, 3, 5, 1)], 8.0)
     own, before, after = paired(mine, shifted(theirs, "tp_c", 1), [f32, bf16, bf16])
     shares += [shifted(before, "tp_y", -1), shifted(after, "tp_y", 1)]
     return finish(mixed, own, shares, final_gain)

time: 221 us -> 242 us (1.095)
  the two profiles are of different devices: /device:TPU:0 before, /device:TPU:32 now
where the time goes in v3:
time: 242 us; the launch traced here: 241 us
  waiting for transfers between devices  93.7 us (39%)
  Pallas kernels  58.6 us (24%)
  starting transfers between devices  45.7 us (19%)
  local copies, waits for them, and re-layouts  28.9 us (12%)
  between operations  13.8 us (6%)
    ppermute x27, waiting for transfers between devices, shifted(): lax.ppermute(value, axis, [(i, (i + steps) % count) for i in range(count)])  62.2 us
    unnamed x87, local copies, waits for them, and re-layouts  27.8 us
    pallas_call x3, Pallas kernels, attend(): pl.pallas_call(body, in_specs=[sm, sm] + [vm] * (len(args) - 2), out_spec...  27.3 us
    ppermute x27, starting transfers between devices, shifted(): lax.ppermute(value, axis, [(i, (i + steps) % count) for i in range(count)])  26.2 us
    all_to_all x1, waiting for transfers between devices, per_device(): lax.all_to_all(state, ('sp_z',) + TP, split_axis=0, concat_axis=0, tiled=...  13.2 us
    all_to_all x1, starting transfers between devices, per_device(): lax.all_to_all(state, ('sp_z',) + TP, split_axis=0, concat_axis=0, tiled=...  11.9 us
    all_to_all x1, waiting for transfers between devices, per_device(): lax.all_to_all(packed, 'sp_z', split_axis=0, concat_axis=0, tiled=True)  9.13 us
    ppermute x1, waiting for transfers between devices, passed_along(): lax.ppermute(value, axis, [(source, source + steps) for source in range(f...  9.11 us
  transfers between devices with their start and end apart: 32, of which 17 were waited for; matrix products, arithmetic and copies ran while one was open for 1% of the time, Pallas kernels for 18%

profile of v3, /device:TPU:32, one launch (start us, length us, event | category | flops | bytes accessed | tf_op | source)
XLA Modules:
  0.0 240.9 jit_solution(9650910096325523367)
XLA Ops:
  6.5 3.0 %shard_map.199 = (bf16[4,800,128]{2,1,0:T(8,128)(2,1)}, bf16[768,128]{1,0:T(8,128)(2,1)}, bf16[768,128]{1,0:T(8,128)(2,1)}, bf16[768,128]{1,0:T(8,128)(2,1)}, bf16[768,128]{1,0:T(8,128)(2,1)}) custom-call(s32[1]{0:T(128)} %bitcast.2.slot_ref, bf16[768,128]{1,0:T(8,128)(2,1)} %ks.1, bf16[768,128]{1,0:T(8,128)(2,1)} %vs.1, bf16[768,128]{1,0:T(8,128)(2,1)} %kl.1, ...), custom_call_target="tpu_custom_call" | custom-call | flops 625000000 | tf_op jit(solution)/shard_map/pallas_call | solution.py:89
  9.6 5.6 %all-to-all-start = ((bf16[4,800,128]{2,1,0:T(8,128)(2,1)}), bf16[4,800,128]{2,1,0:T(8,128)(2,1)S(1)}, u32[]{:S(2)}, u32[]{:S(2)}) async-start(bf16[4,800,128]{2,1,0:T(8,128)(2,1)} %get-tuple-element.62), calls=%async_computation | async-start | bytes 1638400 | tf_op jit(solution)/shard_map/all_to_all | solution.py:626
  15.1 2.0 shard_map.200
  17.2 9.1 %all-to-all-done.refs_6_ = bf16[4,800,128]{2,1,0:T(8,128)(2,1)S(1)} async-done(((bf16[4,800,128]{2,1,0:T(8,128)(2,1)}), bf16[4,800,128]{2,1,0:T(8,128)(2,1)S(1)}, u32[]{:S(2)}, u32[]{:S(2)}) %all-to-all-start) | async-done | bytes 819232 | tf_op jit(solution)/shard_map/all_to_all | solution.py:626
  26.4 1.6 collective-permute-start.3
  27.9 1.7 collective-permute-start.4
  29.7 3.5 %collective-permute-start.1 = (bf16[768,128]{1,0:T(8,128)(2,1)}, bf16[768,128]{1,0:T(8,128)(2,1)S(1)}, u32[]{:S(2)}, u32[]{:S(2)}) collective-permute-start(bf16[768,128]{1,0:T(8,128)(2,1)} %get-tuple-element.74), channel_id=1, source_target_pairs={{0,64},{32,96},{64,0},{96,32},{1,65},{33,97},{65,1},{97,33},{2,66}... | collective-permute-start | bytes 589832 | tf_op jit(solution)/shard_map/ppermute | solution.py:24
  33.9 3.1 %collective-permute-done.refs_3_ = bf16[768,128]{1,0:T(8,128)(2,1)S(1)} collective-permute-done((bf16[768,128]{1,0:T(8,128)(2,1)}, bf16[768,128]{1,0:T(8,128)(2,1)S(1)}, u32[]{:S(2)}, u32[]{:S(2)}) %collective-permute-start) | collective-permute-done | bytes 196640 | tf_op jit(solution)/shard_map/ppermute | solution.py:24
  36.9 1.6 collective-permute-done.1.refs_4_
  38.6 3.4 %collective-permute-done.2.refs_5_ = bf16[768,128]{1,0:T(8,128)(2,1)S(1)} collective-permute-done((bf16[768,128]{1,0:T(8,128)(2,1)S(1)}, bf16[768,128]{1,0:T(8,128)(2,1)S(1)}, u32[]{:S(2)}, u32[]{:S(2)}) %collective-permute-start.2) | collective-permute-done | bytes 196640 | tf_op jit(solution)/shard_map/ppermute | solution.py:24
  42.0 9.4 %shard_map.201 = (f32[4,144,768]{2,1,0:T(8,128)S(1)}, f32[4,8,768]{2,1,0:T(8,128)S(1)}) custom-call(s32[2]{0:T(128)S(1)} %pad_add_fusion.1.refs_0_, s32[4,34]{1,0:T(4,128)S(1)} %copy-done.30, bf16[768,128]{1,0:T(8,128)(2,1)S(1)} %copy-done.31, bf16[768,128]{1,0:T(8,128)(2,1)S(1)} %collective-permute-done.refs_3_, ...), custom_call_target="tpu_custom_call" | custom-call | flops 3000000000 | tf_op jit(solution)/shard_map/pallas_call | solution.py:346
  51.4 1.2 copy-done.33
  53.2 0.9 copy-done.24
  54.2 0.9 copy-done.26
  55.1 1.2 constant_dynamic-update-slice_fusion.1
  56.3 1.1 constant_dynamic-update-slice_fusion.refs_0_
  57.4 1.6 collective-permute-start.6
  59.1 1.7 collective-permute-start.7
  60.7 2.0 collective-permute-start.8
  62.7 1.4 collective-permute-start.5
  64.1 0.9 copy-done.32
  65.0 1.5 copy-done.34
  66.5 11.0 %shard_map.202 = (f32[4,144,768]{2,1,0:T(8,128)S(1)}, f32[4,8,768]{2,1,0:T(8,128)S(1)}) custom-call(s32[2]{0:T(128)S(1)} %pad_add_fusion.1.refs_0_, s32[4,64]{1,0:T(4,128)S(1)} %copy-done.29, bf16[768,128]{1,0:T(8,128)(2,1)S(1)} %copy-done.32, bf16[768,128]{1,0:T(8,128)(2,1)S(1)} %collective-permute-done.refs_3_, ...), custom_call_target="tpu_custom_call" | custom-call | flops 6000000000 | tf_op jit(solution)/shard_map/pallas_call | solution.py:346
  77.6 6.1 %collective-permute-done.6.refs_1_ = bf16[256,2048]{1,0:T(8,128)(2,1)S(1)} collective-permute-done((bf16[256,2048]{1,0:T(8,128)(2,1)S(1)}, bf16[256,2048]{1,0:T(8,128)(2,1)S(1)}, u32[]{:S(2)}, u32[]{:S(2)}) %collective-permute-start.6) | collective-permute-done | bytes 1048608 | tf_op jit(solution)/shard_map/ppermute | solution.py:24
  83.7 19.0 %collective-permute-done.7.refs_2_ = bf16[256,2048]{1,0:T(8,128)(2,1)} collective-permute-done((bf16[256,2048]{1,0:T(8,128)(2,1)S(1)}, bf16[256,2048]{1,0:T(8,128)(2,1)}, u32[]{:S(2)}, u32[]{:S(2)}) %collective-permute-start.7) | collective-permute-done | bytes 1048608 | tf_op jit(solution)/shard_map/ppermute | solution.py:24
  102.7 1.9 collective-permute-done.8.refs_3_
  105.7 6.8 %shard_map.203 = bf16[32,112,128]{2,1,0:T(8,128)(2,1)S(1)} custom-call(s32[2]{0:T(128)S(1)} %pad_add_fusion.1.refs_0_, s32[4,34]{1,0:T(4,128)S(1)} %copy-done.28, bf16[768,128]{1,0:T(8,128)(2,1)S(1)} %copy-done.32, bf16[768,128]{1,0:T(8,128)(2,1)S(1)} %collective-permute-done.refs_3_, bf16[768,128]{1,0:T(8,128)(2,1)S(1)} %collective-permute-done.1.refs_4_, ...), custom_call_target="tpu_custom_call" | custom-call | flops 3000000000 | tf_op jit(solution)/shard_map/pallas_call | solution.py:346
  112.5 0.9 copy-done.6
  113.5 11.9 %all-to-all-start.1 = ((bf16[32,112,128]{2,1,0:T(8,128)(2,1)}), bf16[32,112,128]{2,1,0:T(8,128)(2,1)S(1)}, u32[]{:S(2)}, u32[]{:S(2)}) async-start(bf16[32,112,128]{2,1,0:T(8,128)(2,1)} %copy-done.6), calls=%async_computation.1 | async-start | bytes 1835008 | tf_op jit(solution)/shard_map/all_to_all | solution.py:662
  125.5 13.2 %all-to-all-done.1.arrived_ref = bf16[32,112,128]{2,1,0:T(8,128)(2,1)S(1)} async-done(((bf16[32,112,128]{2,1,0:T(8,128)(2,1)}), bf16[32,112,128]{2,1,0:T(8,128)(2,1)S(1)}, u32[]{:S(2)}, u32[]{:S(2)}) %all-to-all-start.1) | async-done | bytes 917536 | tf_op jit(solution)/shard_map/all_to_all | solution.py:662
  138.7 1.0 copy-done.12
  139.7 4.7 %shard_map.204.refs_1_.refs_0_ = bf16[96,2048]{1,0:T(8,128)(2,1)S(1)} custom-call(s32[2]{0:T(128)S(1)} %pad_add_fusion.place_ref.refs_0_, bf16[32,112,128]{2,1,0:T(8,128)(2,1)S(1)} %all-to-all-done.1.arrived_ref, bf16[256,2048]{1,0:T(8,128)(2,1)S(1)} %constant_dynamic-update-slice_fusion.refs_0_, bf16[256,2048]{1,0:T(8,128)(2,1)S(1)} %collective-permute-done.6.refs_1_, ...), custom_call_target="tpu_custom_call" | custom-call | flops 1250000000 | tf_op jit(solution)/shard_map/pallas_call | solution.py:396
  144.5 1.7 collective-permute-start.14
  146.2 1.9 collective-permute-start.15
  148.3 9.6 %collective-permute-done.14.refs_3_ = bf16[96,2048]{1,0:T(8,128)(2,1)S(1)} collective-permute-done((bf16[96,2048]{1,0:T(8,128)(2,1)S(1)}, bf16[96,2048]{1,0:T(8,128)(2,1)S(1)}, u32[]{:S(2)}, u32[]{:S(2)}) %collective-permute-start.14) | collective-permute-done | bytes 393248 | tf_op jit(solution)/shard_map/ppermute | solution.py:24
  159.0 2.7 %collective-permute-start.19 = (bf16[48,2048]{1,0:T(8,128)(2,1)S(1)}, bf16[48,2048]{1,0:T(8,128)(2,1)S(1)}, u32[]{:S(2)}, u32[]{:S(2)}) collective-permute-start(bf16[48,2048]{1,0:T(8,128)(2,1)S(1)} %slice.9), channel_id=1, source_target_pairs={{0,6},{2,0},{4,2},{6,4},{1,7},{3,1},{5,3},{7,5},{8,14},{10,8},{12,... | collective-permute-start | bytes 589832 | tf_op jit(solution)/shard_map/ppermute | solution.py:24
  161.8 2.8 %copy-done = bf16[2048,1536]{1,0:T(8,128)(2,1)S(1)} copy-done((bf16[2048,1536]{1,0:T(8,128)(2,1)S(1)}, bf16[2048,1536]{1,0:T(8,128)(2,1)}, u32[]{:S(2)}) %copy-start) | copy-done | bytes 6291480
  164.6 4.3 %shard_map.205 = (bf16[576,704]{1,0:T(8,128)(2,1)S(1)}, bf16[576,704]{1,0:T(8,128)(2,1)S(1)}) custom-call(s32[2]{0:T(128)S(1)} %pad_add_fusion.place_ref.refs_0_, bf16[96,2048]{1,0:T(8,128)(2,1)S(1)} %shard_map.204.refs_1_.refs_0_, bf16[96,2048]{1,0:T(8,128)(2,1)S(1)} %collective-permute-done.13.refs_2_, ...), custom_call_target="tpu_custom_call" | custom-call | flops 1250000000 | tf_op jit(solution)/shard_map/pallas_call | solution.py:470
  169.6 0.9 collective-permute-done.20.refs_3_
  170.8 1.9 shard_map.206
  174.8 1.9 collective-permute-start.22
  176.8 9.1 %collective-permute-done.22.refs_3_ = bf16[32,704]{1,0:T(8,128)(2,1)S(1)} collective-permute-done((bf16[32,704]{1,0:T(8,128)(2,1)S(1)}, bf16[32,704]{1,0:T(8,128)(2,1)S(1)}, u32[]{:S(2)}, u32[]{:S(2)}) %collective-permute-start.22) | collective-permute-done | bytes 45088 | tf_op jit(solution)/shard_map/ppermute | solution.py:30
  185.9 1.9 copy-done.3
  187.8 1.0 copy-done.14
  188.8 0.9 copy-done.16
  189.7 0.9 copy-done.19
  190.6 2.9 %shard_map.207 = (bf16[1,96,2048]{2,1,0:T(8,128)(2,1)S(1)}, f32[1,96,2048]{2,1,0:T(8,128)S(1)}) custom-call(s32[2]{0:T(128)S(1)} %pad_add_fusion.place_ref.refs_0_, f32[3,704]{1,0:T(4,128)S(1)} %copy-done.21, f32[3,704]{1,0:T(4,128)S(1)} %copy-done.22, bf16[2048,768]{1,0:T(8,128)(2,1)S(1)} %copy-done.3, bf16[32,704]{1,0:T(8,128)(2,1)S(1)} %collective-permute-done.22.refs_3_, ...), custom_call_target="tpu_custom_call" | custom-call | flops 1000000000 | tf_op jit(solution)/shard_map/pallas_call | solution.py:530
  193.5 0.9 copy-done.11
  194.4 1.7 collective-permute-done.23.their_ref
  196.8 2.0 shard_map.208
  198.9 1.2 copy-done.8
  200.1 1.2 copy-done.10
  201.2 0.9 copy-done.17
  202.2 0.9 copy-done.20
  203.1 4.3 %shard_map.209 = (bf16[3,96,2048]{2,1,0:T(8,128)(2,1)S(1)}, f32[3,96,2048]{2,1,0:T(8,128)S(1)}) custom-call(s32[2]{0:T(128)S(1)} %pad_add_fusion.place_ref.refs_0_, f32[3,704]{1,0:T(4,128)S(1)} %copy-done.21, f32[3,704]{1,0:T(4,128)S(1)} %copy-done.22, bf16[2048,768]{1,0:T(8,128)(2,1)S(1)} %copy-done.4, bf16[32,704]{1,0:T(8,128)(2,1)S(1)} %collective-permute-done.22.refs_3_, ...), custom_call_target="tpu_custom_call" | custom-call | flops 2000000000 | tf_op jit(solution)/shard_map/pallas_call | solution.py:530
  207.4 1.4 copy-done.5
  209.7 2.0 collective-permute-done.24.their_ref
  211.7 1.1 copy-done.37
  212.8 3.2 %shard_map.210 = (f32[96,2048]{1,0:T(8,128)}, bf16[96,2048]{1,0:T(8,128)(2,1)}, bf16[96,2048]{1,0:T(8,128)(2,1)}) custom-call(f32[3,96,2048]{2,1,0:T(8,128)} %copy-done.5, bf16[3,96,2048]{2,1,0:T(8,128)(2,1)} %copy-done.37), custom_call_target="tpu_custom_call" | custom-call | flops 525000000 | tf_op jit(solution)/shard_map/pallas_call | solution.py:555
  216.0 1.2 collective-permute-start.26
  218.0 4.7 %collective-permute-done.25.refs_2_ = bf16[96,2048]{1,0:T(8,128)(2,1)S(1)} collective-permute-done((bf16[96,2048]{1,0:T(8,128)(2,1)}, bf16[96,2048]{1,0:T(8,128)(2,1)S(1)}, u32[]{:S(2)}, u32[]{:S(2)}) %collective-permute-start.25) | collective-permute-done | bytes 393248 | tf_op jit(solution)/shard_map/ppermute | solution.py:24
  222.7 6.4 %collective-permute-done.26.refs_3_ = bf16[96,2048]{1,0:T(8,128)(2,1)S(1)} collective-permute-done((bf16[96,2048]{1,0:T(8,128)(2,1)}, bf16[96,2048]{1,0:T(8,128)(2,1)S(1)}, u32[]{:S(2)}, u32[]{:S(2)}) %collective-permute-start.26) | collective-permute-done | bytes 393248 | tf_op jit(solution)/shard_map/ppermute | solution.py:24
  229.1 1.4 collective-permute-done.27.refs_4_
  231.3 2.8 %shard_map.211 = bf16[96,2048]{1,0:T(8,128)(2,1)} custom-call(bf16[96,2048]{1,0:T(8,128)(2,1)} %copy-done.2, f32[96,2048]{1,0:T(8,128)} %get-tuple-element.113.refs_1_, bf16[96,2048]{1,0:T(8,128)(2,1)} %copy-done.39, bf16[96,2048]{1,0:T(8,128)(2,1)} %copy-done.40, bf16[96,2048]{1,0:T(8,128)(2,1)} %copy-done.41, f32[1,2048]{1,0:T(1,128)} %bitcast.11), custom_call_target="tpu_custom_call" | custom-call | flops 500000000 | tf_op jit(solution)/shard_map/pallas_call | solution.py:580
  (107 shorter events, 10.0 us)
Async XLA Ops:
  9.5 23.7 %copy-start.42 = (bf16[768,128]{1,0:T(8,128)(2,1)S(1)}, bf16[768,128]{1,0:T(8,128)(2,1)}, u32[]{:S(2)}) copy-start(bf16[768,128]{1,0:T(8,128)(2,1)} %get-tuple-element.75) | copy-start | bytes 589828
  9.5 32.4 %copy-start.30 = (s32[4,34]{1,0:T(4,128)S(1)}, s32[4,34]{1,0:T(4,128)}, u32[]{:S(2)}) copy-start(s32[4,34]{1,0:T(4,128)} %constant.21.clone.refs_1_) | copy-start | bytes 1636
  9.6 32.4 %copy-start.31 = (bf16[768,128]{1,0:T(8,128)(2,1)S(1)}, bf16[768,128]{1,0:T(8,128)(2,1)}, u32[]{:S(2)}) copy-start(bf16[768,128]{1,0:T(8,128)(2,1)} %get-tuple-element.72.refs_2_) | copy-start | bytes 589828
  9.6 16.7 %all-to-all-start = ((bf16[4,800,128]{2,1,0:T(8,128)(2,1)}), bf16[4,800,128]{2,1,0:T(8,128)(2,1)S(1)}, u32[]{:S(2)}, u32[]{:S(2)}) async-start(bf16[4,800,128]{2,1,0:T(8,128)(2,1)} %get-tuple-element.62), calls=%async_computation | async-start | bytes 1638400 | tf_op jit(solution)/shard_map/all_to_all | solution.py:626
  15.1 146.6 %all-gather.5.cloned.1.call-start = ((), (), s32[]{:S(2)}) async-start(), calls=%async_computation.3 | async-start | bytes 6684672 | tf_op jit(solution)/shard_map/all_gather | solution.py:629
  26.3 150.5 %all-gather.3.cloned.1.call-start = ((), (), s32[]{:S(2)}) async-start(), calls=%async_computation.2 | async-start | bytes 3342336 | tf_op jit(solution)/shard_map/all_gather | solution.py:653
  26.4 26.9 %collective-permute-start.3 = (bf16[4,800,128]{2,1,0:T(8,128)(2,1)S(1)}, bf16[4,800,128]{2,1,0:T(8,128)(2,1)S(1)}, u32[]{:S(2)}, u32[]{:S(2)}) collective-permute-start(bf16[4,800,128]{2,1,0:T(8,128)(2,1)S(1)} %all-to-all-done.refs_6_), channel_id=1, source_target_pairs={{0,8},{8,16},{16,24},{24,0},{1,9},{9,17},{17,25},{25,1},{2,10},{10... | collective-permute-start | bytes 2457608 | tf_op jit(solution)/shard_map/ppermute | solution.py:24
  27.9 26.2 %collective-permute-start.4 = (bf16[4,800,128]{2,1,0:T(8,128)(2,1)S(1)}, bf16[4,800,128]{2,1,0:T(8,128)(2,1)S(1)}, u32[]{:S(2)}, u32[]{:S(2)}) collective-permute-start(bf16[4,800,128]{2,1,0:T(8,128)(2,1)S(1)} %all-to-all-done.refs_6_), channel_id=1, source_target_pairs={{0,24},{8,0},{16,8},{24,16},{1,25},{9,1},{17,9},{25,17},{2,26},{10... | collective-permute-start | bytes 2457608 | tf_op jit(solution)/shard_map/ppermute | solution.py:24
  29.7 7.3 %collective-permute-start = (bf16[768,128]{1,0:T(8,128)(2,1)}, bf16[768,128]{1,0:T(8,128)(2,1)S(1)}, u32[]{:S(2)}, u32[]{:S(2)}) collective-permute-start(bf16[768,128]{1,0:T(8,128)(2,1)} %get-tuple-element.73), channel_id=1, source_target_pairs={{0,32},{32,64},{64,96},{96,0},{1,33},{33,65},{65,97},{97,1},{2,34}... | collective-permute-start | bytes 589832 | tf_op jit(solution)/shard_map/ppermute | solution.py:24
  29.7 8.9 %collective-permute-start.1 = (bf16[768,128]{1,0:T(8,128)(2,1)}, bf16[768,128]{1,0:T(8,128)(2,1)S(1)}, u32[]{:S(2)}, u32[]{:S(2)}) collective-permute-start(bf16[768,128]{1,0:T(8,128)(2,1)} %get-tuple-element.74), channel_id=1, source_target_pairs={{0,64},{32,96},{64,0},{96,32},{1,65},{33,97},{65,1},{97,33},{2,66}... | collective-permute-start | bytes 589832 | tf_op jit(solution)/shard_map/ppermute | solution.py:24
  33.2 8.8 %collective-permute-start.2 = (bf16[768,128]{1,0:T(8,128)(2,1)S(1)}, bf16[768,128]{1,0:T(8,128)(2,1)S(1)}, u32[]{:S(2)}, u32[]{:S(2)}) collective-permute-start(bf16[768,128]{1,0:T(8,128)(2,1)S(1)} %copy-done.42), channel_id=1, source_target_pairs={{0,96},{32,0},{64,32},{96,64},{1,97},{33,1},{65,33},{97,65},{2,98}... | collective-permute-start | bytes 589832 | tf_op jit(solution)/shard_map/ppermute | solution.py:24
  51.4 1.2 copy-start.33
  53.2 10.9 %copy-start.29 = (s32[4,64]{1,0:T(4,128)S(1)}, s32[4,64]{1,0:T(4,128)}, u32[]{:S(2)}) copy-start(s32[4,64]{1,0:T(4,128)} %constant.22.clone.refs_1_) | copy-start | bytes 3076
  55.1 9.0 %copy-start.25 = (bf16[4,800,128]{2,1,0:T(8,128)(2,1)S(1)}, bf16[4,800,128]{2,1,0:T(8,128)(2,1)}, u32[]{:S(2)}) copy-start(bf16[4,800,128]{2,1,0:T(8,128)(2,1)} %copy-done.24) | copy-start | bytes 2457604
  55.1 9.0 %copy-start.27 = (bf16[4,800,128]{2,1,0:T(8,128)(2,1)S(1)}, bf16[4,800,128]{2,1,0:T(8,128)(2,1)}, u32[]{:S(2)}) copy-start(bf16[4,800,128]{2,1,0:T(8,128)(2,1)} %copy-done.26) | copy-start | bytes 2457604
  55.1 9.0 %copy-start.36 = (f32[4,8,768]{2,1,0:T(8,128)S(1)}, f32[4,8,768]{2,1,0:T(8,128)}, u32[]{:S(2)}) copy-start(f32[4,8,768]{2,1,0:T(8,128)} %copy-done.35) | copy-start | bytes 294916
  57.4 48.3 %copy-start.28 = (s32[4,34]{1,0:T(4,128)S(1)}, s32[4,34]{1,0:T(4,128)}, u32[]{:S(2)}) copy-start(s32[4,34]{1,0:T(4,128)} %constant.23.clone.refs_1_) | copy-start | bytes 1636
  57.4 26.3 %collective-permute-start.6 = (bf16[256,2048]{1,0:T(8,128)(2,1)S(1)}, bf16[256,2048]{1,0:T(8,128)(2,1)S(1)}, u32[]{:S(2)}, u32[]{:S(2)}) collective-permute-start(bf16[256,2048]{1,0:T(8,128)(2,1)S(1)} %constant_dynamic-update-slice_fusion.refs_0_), channel_id=1, source_target_pairs={{0,2},{2,4},{4,6},{6,0},{1,3},{3,5},{5,7},{7,1},{8,10},{10,12},{12... | collective-permute-start | bytes 3145736 | tf_op jit(solution)/shard_map/ppermute | solution.py:24
  59.1 43.7 %collective-permute-start.7 = (bf16[256,2048]{1,0:T(8,128)(2,1)S(1)}, bf16[256,2048]{1,0:T(8,128)(2,1)}, u32[]{:S(2)}, u32[]{:S(2)}) collective-permute-start(bf16[256,2048]{1,0:T(8,128)(2,1)S(1)} %constant_dynamic-update-slice_fusion.refs_0_), channel_id=1, source_target_pairs={{0,6},{2,0},{4,2},{6,4},{1,7},{3,1},{5,3},{7,5},{8,14},{10,8},{12,... | collective-permute-start | bytes 3145736 | tf_op jit(solution)/shard_map/ppermute | solution.py:24
  60.7 43.9 %collective-permute-start.8 = (bf16[256,2048]{1,0:T(8,128)(2,1)S(1)}, bf16[256,2048]{1,0:T(8,128)(2,1)}, u32[]{:S(2)}, u32[]{:S(2)}) collective-permute-start(bf16[256,2048]{1,0:T(8,128)(2,1)S(1)} %constant_dynamic-update-slice_fusion.refs_0_), channel_id=1, source_target_pairs={{0,4},{2,6},{4,0},{6,2},{1,5},{3,7},{5,1},{7,3},{8,12},{10,14},{12... | collective-permute-start | bytes 3145736 | tf_op jit(solution)/shard_map/ppermute | solution.py:24
  62.7 41.9 %collective-permute-start.5 = (bf16[4,800,128]{2,1,0:T(8,128)(2,1)S(1)}, bf16[4,800,128]{2,1,0:T(8,128)(2,1)S(1)}, u32[]{:S(2)}, u32[]{:S(2)}) collective-permute-start(bf16[4,800,128]{2,1,0:T(8,128)(2,1)S(1)} %all-to-all-done.refs_6_), channel_id=1, source_target_pairs={{0,16},{8,24},{16,0},{24,8},{1,17},{9,25},{17,1},{25,9},{2,18},{10... | collective-permute-start | bytes 2457608 | tf_op jit(solution)/shard_map/ppermute | solution.py:24
  64.1 0.9 copy-start.32
  65.0 1.5 copy-start.34
  104.6 34.1 %collective-permute-start.10 = (bf16[256,2048]{1,0:T(8,128)(2,1)S(1)}, bf16[256,2048]{1,0:T(8,128)(2,1)}, u32[]{:S(2)}, u32[]{:S(2)}) collective-permute-start(bf16[256,2048]{1,0:T(8,128)(2,1)S(1)} %collective-permute-done.6.refs_1_), channel_id=1, source_target_pairs={{0,1},{1,0},{2,3},{3,2},{4,5},{5,4},{6,7},{7,6},{8,9},{9,8},{10,11... | collective-permute-start | bytes 3145736 | tf_op jit(solution)/shard_map/ppermute | solution.py:24
  104.6 34.1 %collective-permute-start.11 = (bf16[256,2048]{1,0:T(8,128)(2,1)}, bf16[256,2048]{1,0:T(8,128)(2,1)}, u32[]{:S(2)}, u32[]{:S(2)}) collective-permute-start(bf16[256,2048]{1,0:T(8,128)(2,1)} %collective-permute-done.7.refs_2_), channel_id=1, source_target_pairs={{0,1},{1,0},{2,3},{3,2},{4,5},{5,4},{6,7},{7,6},{8,9},{9,8},{10,11... | collective-permute-start | bytes 3145736 | tf_op jit(solution)/shard_map/ppermute | solution.py:24
  105.2 33.6 %collective-permute-start.12 = (bf16[256,2048]{1,0:T(8,128)(2,1)}, bf16[256,2048]{1,0:T(8,128)(2,1)}, u32[]{:S(2)}, u32[]{:S(2)}) collective-permute-start(bf16[256,2048]{1,0:T(8,128)(2,1)} %collective-permute-done.8.refs_3_), channel_id=1, source_target_pairs={{0,1},{1,0},{2,3},{3,2},{4,5},{5,4},{6,7},{7,6},{8,9},{9,8},{10,11... | collective-permute-start | bytes 3145736 | tf_op jit(solution)/shard_map/ppermute | solution.py:24
  105.2 33.6 %collective-permute-start.9 = (bf16[256,2048]{1,0:T(8,128)(2,1)S(1)}, bf16[256,2048]{1,0:T(8,128)(2,1)}, u32[]{:S(2)}, u32[]{:S(2)}) collective-permute-start(bf16[256,2048]{1,0:T(8,128)(2,1)S(1)} %constant_dynamic-update-slice_fusion.refs_0_), channel_id=1, source_target_pairs={{0,1},{1,0},{2,3},{3,2},{4,5},{5,4},{6,7},{7,6},{8,9},{9,8},{10,11... | collective-permute-start | bytes 3145736 | tf_op jit(solution)/shard_map/ppermute | solution.py:24
  112.5 0.9 copy-start.6
  113.5 25.2 %copy-start.23 = (f32[2048]{0:T(1024)S(1)}, f32[2048]{0:T(1024)}, u32[]{:S(2)}) copy-start(f32[2048]{0:T(1024)} %param.32) | copy-start | bytes 24580
  113.5 25.2 %all-to-all-start.1 = ((bf16[32,112,128]{2,1,0:T(8,128)(2,1)}), bf16[32,112,128]{2,1,0:T(8,128)(2,1)S(1)}, u32[]{:S(2)}, u32[]{:S(2)}) async-start(bf16[32,112,128]{2,1,0:T(8,128)(2,1)} %copy-done.6), calls=%async_computation.1 | async-start | bytes 1835008 | tf_op jit(solution)/shard_map/all_to_all | solution.py:662
  138.7 1.0 copy-start.12
  144.5 24.4 %copy-start.2 = (bf16[96,2048]{1,0:T(8,128)(2,1)}, bf16[96,2048]{1,0:T(8,128)(2,1)S(1)}, u32[]{:S(2)}) copy-start(bf16[96,2048]{1,0:T(8,128)(2,1)S(1)} %shard_map.204.refs_1_.refs_0_) | copy-start | bytes 1179652
  144.5 13.3 %collective-permute-start.14 = (bf16[96,2048]{1,0:T(8,128)(2,1)S(1)}, bf16[96,2048]{1,0:T(8,128)(2,1)S(1)}, u32[]{:S(2)}, u32[]{:S(2)}) collective-permute-start(bf16[96,2048]{1,0:T(8,128)(2,1)S(1)} %shard_map.204.refs_1_.refs_0_), channel_id=1, source_target_pairs={{0,2},{2,4},{4,6},{6,0},{1,3},{3,5},{5,7},{7,1},{8,10},{10,12},{12... | collective-permute-start | bytes 1179656 | tf_op jit(solution)/shard_map/ppermute | solution.py:24
  146.2 11.6 %collective-permute-start.15 = (bf16[96,2048]{1,0:T(8,128)(2,1)S(1)}, bf16[96,2048]{1,0:T(8,128)(2,1)S(1)}, u32[]{:S(2)}, u32[]{:S(2)}) collective-permute-start(bf16[96,2048]{1,0:T(8,128)(2,1)S(1)} %shard_map.204.refs_1_.refs_0_), channel_id=1, source_target_pairs={{0,6},{2,0},{4,2},{6,4},{1,7},{3,1},{5,3},{7,5},{8,14},{10,8},{12,... | collective-permute-start | bytes 1179656 | tf_op jit(solution)/shard_map/ppermute | solution.py:24
  148.1 13.6 %collective-permute-start.13 = (bf16[96,2048]{1,0:T(8,128)(2,1)S(1)}, bf16[96,2048]{1,0:T(8,128)(2,1)S(1)}, u32[]{:S(2)}, u32[]{:S(2)}) collective-permute-start(bf16[96,2048]{1,0:T(8,128)(2,1)S(1)} %shard_map.204.refs_1_.refs_0_), channel_id=1, source_target_pairs={{0,1},{1,0},{2,3},{3,2},{4,5},{5,4},{6,7},{7,6},{8,9},{9,8},{10,11... | collective-permute-start | bytes 1179656 | tf_op jit(solution)/shard_map/ppermute | solution.py:24
  157.8 3.9 %collective-permute-start.16 = (bf16[96,2048]{1,0:T(8,128)(2,1)S(1)}, bf16[96,2048]{1,0:T(8,128)(2,1)S(1)}, u32[]{:S(2)}, u32[]{:S(2)}) collective-permute-start(bf16[96,2048]{1,0:T(8,128)(2,1)S(1)} %collective-permute-done.14.refs_3_), channel_id=1, source_target_pairs={{0,1},{1,0},{2,3},{3,2},{4,5},{5,4},{6,7},{7,6},{8,9},{9,8},{10,11... | collective-permute-start | bytes 1179656 | tf_op jit(solution)/shard_map/ppermute | solution.py:24
  157.8 3.9 %collective-permute-start.17 = (bf16[96,2048]{1,0:T(8,128)(2,1)S(1)}, bf16[96,2048]{1,0:T(8,128)(2,1)S(1)}, u32[]{:S(2)}, u32[]{:S(2)}) collective-permute-start(bf16[96,2048]{1,0:T(8,128)(2,1)S(1)} %collective-permute-done.15.refs_4_), channel_id=1, source_target_pairs={{0,1},{1,0},{2,3},{3,2},{4,5},{5,4},{6,7},{7,6},{8,9},{9,8},{10,11... | collective-permute-start | bytes 1179656 | tf_op jit(solution)/shard_map/ppermute | solution.py:24
  158.3 10.6 %collective-permute-start.18 = (bf16[48,2048]{1,0:T(8,128)(2,1)S(1)}, bf16[48,2048]{1,0:T(8,128)(2,1)S(1)}, u32[]{:S(2)}, u32[]{:S(2)}) collective-permute-start(bf16[48,2048]{1,0:T(8,128)(2,1)S(1)} %slice.8), channel_id=1, source_target_pairs={{0,2},{2,4},{4,6},{6,0},{1,3},{3,5},{5,7},{7,1},{8,10},{10,12},{12... | collective-permute-start | bytes 589832 | tf_op jit(solution)/shard_map/ppermute | solution.py:24
  159.0 9.9 %collective-permute-start.19 = (bf16[48,2048]{1,0:T(8,128)(2,1)S(1)}, bf16[48,2048]{1,0:T(8,128)(2,1)S(1)}, u32[]{:S(2)}, u32[]{:S(2)}) collective-permute-start(bf16[48,2048]{1,0:T(8,128)(2,1)S(1)} %slice.9), channel_id=1, source_target_pairs={{0,6},{2,0},{4,2},{6,4},{1,7},{3,1},{5,3},{7,5},{8,14},{10,8},{12,... | collective-permute-start | bytes 589832 | tf_op jit(solution)/shard_map/ppermute | solution.py:24
  161.8 2.8 %copy-start = (bf16[2048,1536]{1,0:T(8,128)(2,1)S(1)}, bf16[2048,1536]{1,0:T(8,128)(2,1)}, u32[]{:S(2)}) copy-start(bf16[2048,1536]{1,0:T(8,128)(2,1)} %all-gather.5.cloned.1.call-done.refs_7_.refs_8_.refs_5_.refs_6_) | copy-start | bytes 18874372
  164.6 6.2 %copy-start.1 = (bf16[2048,1536]{1,0:T(8,128)(2,1)S(1)}, bf16[2048,1536]{1,0:T(8,128)(2,1)}, u32[]{:S(2)}) copy-start(bf16[2048,1536]{1,0:T(8,128)(2,1)} %all-gather.5.cloned.1.call-done.refs_7_.refs_8_.refs_5_.refs_6_) | copy-start | bytes 18874372
  168.9 3.8 %copy-start.7 = (bf16[576,704]{1,0:T(8,128)(2,1)}, bf16[576,704]{1,0:T(8,128)(2,1)S(1)}, u32[]{:S(2)}) copy-start(bf16[576,704]{1,0:T(8,128)(2,1)S(1)} %get-tuple-element.109.refs_7_.refs_6_) | copy-start | bytes 2433028
  168.9 3.8 %copy-start.9 = (bf16[576,704]{1,0:T(8,128)(2,1)}, bf16[576,704]{1,0:T(8,128)(2,1)S(1)}, u32[]{:S(2)}) copy-start(bf16[576,704]{1,0:T(8,128)(2,1)S(1)} %get-tuple-element.110.refs_8_.refs_7_) | copy-start | bytes 2433028
  169.0 16.9 %copy-start.21 = (f32[3,704]{1,0:T(4,128)S(1)}, f32[3,704]{1,0:T(4,128)}, u32[]{:S(2)}) copy-start(f32[3,704]{1,0:T(4,128)} %refs_0_.3) | copy-start | bytes 25348
  169.0 16.9 %copy-start.22 = (f32[3,704]{1,0:T(4,128)S(1)}, f32[3,704]{1,0:T(4,128)}, u32[]{:S(2)}) copy-start(f32[3,704]{1,0:T(4,128)} %refs_1_.6) | copy-start | bytes 25348
  169.0 1.5 collective-permute-start.20
  169.1 1.7 collective-permute-start.21
  174.8 11.1 %collective-permute-start.22 = (bf16[32,704]{1,0:T(8,128)(2,1)S(1)}, bf16[32,704]{1,0:T(8,128)(2,1)S(1)}, u32[]{:S(2)}, u32[]{:S(2)}) collective-permute-start(bf16[32,704]{1,0:T(8,128)(2,1)S(1)} %get-tuple-element.102), channel_id=1, source_target_pairs={{0,8},{8,16},{16,24},{24,32},{32,40},{40,48},{48,56},{56,64},{64,7... | collective-permute-start | bytes 135176 | tf_op jit(solution)/shard_map/ppermute | solution.py:30
  185.9 1.9 copy-start.3
  187.8 1.0 copy-start.14
  188.8 0.9 copy-start.16
  189.7 0.9 copy-start.19
  190.6 8.3 %copy-start.4 = (bf16[2048,768]{1,0:T(8,128)(2,1)S(1)}, bf16[2048,768]{1,0:T(8,128)(2,1)}, u32[]{:S(2)}) copy-start(bf16[2048,768]{1,0:T(8,128)(2,1)} %all-gather.3.cloned.1.call-done.refs_2_) | copy-start | bytes 9437188
  194.4 1.7 collective-permute-start.23
  198.9 1.2 copy-start.8
  200.1 1.2 copy-start.10
  207.4 1.4 copy-start.5
  208.9 2.8 %collective-permute-start.24 = (bf16[3,96,2048]{2,1,0:T(8,128)(2,1)S(1)}, bf16[3,96,2048]{2,1,0:T(8,128)(2,1)S(1)}, u32[]{:S(2)}, u32[]{:S(2)}) collective-permute-start(bf16[3,96,2048]{2,1,0:T(8,128)(2,1)S(1)} %get-tuple-element.112), channel_id=1, source_target_pairs={{0,1},{1,0},{2,3},{3,2},{4,5},{5,4},{6,7},{7,6},{8,9},{9,8},{10,11... | collective-permute-start | bytes 3538952 | tf_op jit(solution)/shard_map/ppermute | solution.py:24
  209.0 13.7 %collective-permute-start.25 = (bf16[96,2048]{1,0:T(8,128)(2,1)}, bf16[96,2048]{1,0:T(8,128)(2,1)S(1)}, u32[]{:S(2)}, u32[]{:S(2)}) collective-permute-start(bf16[96,2048]{1,0:T(8,128)(2,1)} %shard_map.208), channel_id=1, source_target_pairs={{0,4},{2,6},{4,0},{6,2},{1,5},{3,7},{5,1},{7,3},{8,12},{10,14},{12... | collective-permute-start | bytes 1179656 | tf_op jit(solution)/shard_map/ppermute | solution.py:24
  211.7 1.1 copy-start.37
  216.0 13.1 %collective-permute-start.26 = (bf16[96,2048]{1,0:T(8,128)(2,1)}, bf16[96,2048]{1,0:T(8,128)(2,1)S(1)}, u32[]{:S(2)}, u32[]{:S(2)}) collective-permute-start(bf16[96,2048]{1,0:T(8,128)(2,1)} %get-tuple-element.115), channel_id=1, source_target_pairs={{0,6},{2,0},{4,2},{6,4},{1,7},{3,1},{5,3},{7,5},{8,14},{10,8},{12,... | collective-permute-start | bytes 1179656 | tf_op jit(solution)/shard_map/ppermute | solution.py:24
  217.2 13.3 %collective-permute-start.27 = (bf16[96,2048]{1,0:T(8,128)(2,1)}, bf16[96,2048]{1,0:T(8,128)(2,1)S(1)}, u32[]{:S(2)}, u32[]{:S(2)}) collective-permute-start(bf16[96,2048]{1,0:T(8,128)(2,1)} %get-tuple-element.116), channel_id=1, source_target_pairs={{0,2},{2,4},{4,6},{6,0},{1,3},{3,5},{5,7},{7,1},{8,10},{10,12},{12... | collective-permute-start | bytes 1179656 | tf_op jit(solution)/shard_map/ppermute | solution.py:24
  222.7 7.8 %copy-start.39 = (bf16[96,2048]{1,0:T(8,128)(2,1)}, bf16[96,2048]{1,0:T(8,128)(2,1)S(1)}, u32[]{:S(2)}) copy-start(bf16[96,2048]{1,0:T(8,128)(2,1)S(1)} %collective-permute-done.25.refs_2_) | copy-start | bytes 1179652
  229.1 1.4 copy-start.40
  (11 other events, 8.8 us)
Sparse Core Ops, SparseCore 0:
  26.4 79.8 all-gather.4
  108.5 53.9 all-gather.2

commit v4 on v3

--- a/solution.py
+++ b/solution.py
@@ -631,7 +631,11 @@
     after = shifted(pairs, "sp_x", -1)
     queries = [asked[0]] + [shifted(asked[k], "sp_z", k) for k in range(1, depth)]
     mixer = jnp.concatenate([mixer_small, mixer_large], axis=0)
-    mixers = [mixer] + [shifted(mixer, "tp_y", k) for k in (1, -1, 2)]
+    mixer, down_shard = lax.optimization_barrier((mixer, shards[1]))
+    down_weights = lax.all_gather(down_shard, SP, axis=0, tiled=True)
+    mixers = [mixer]
+    for k in (1, -1, 2):
+        mixers.append(shifted(mixer, "tp_y", k))
     calls = ((0,), (-1, 1), (2,))
     tables = work_tables(calls, depth, turns)
     place_here = jnp.stack([slot, column])
@@ -647,10 +651,7 @@
         12.0 * len(calls[k]),
     )
     state = call(0, [pairs], None)
-    pairs, before, after, state, down_shard = lax.optimization_barrier(
-        (pairs, before, after, state, shards[1])
-    )
-    down_weights = lax.all_gather(down_shard, SP, axis=0, tiled=True)
+    pairs, before, after, state = lax.optimization_barrier((pairs, before, after, state))
     far = shifted(pairs, "sp_x", 2)
     state = call(1, [before, after], state)
     far, state, mixers = lax.optimization_barrier((far, state, mixers))

time: 242 us -> 230 us (0.950)
  the two profiles are of different devices: /device:TPU:32 before, /device:TPU:4 now
where the time goes in v4:
time: 230 us; the launch traced here: 229 us
  waiting for transfers between devices  82.2 us (36%)
  Pallas kernels  65.4 us (28%)
  starting transfers between devices  44.7 us (19%)
  local copies, waits for them, and re-layouts  22.5 us (10%)
  between operations  13.8 us (6%)
    ppermute x27, waiting for transfers between devices, shifted(): lax.ppermute(value, axis, [(i, (i + steps) % count) for i in range(count)])  51.7 us
    pallas_call x3, Pallas kernels, attend(): pl.pallas_call(body, in_specs=[sm, sm] + [vm] * (len(args) - 2), out_spec...  34 us
    ppermute x27, starting transfers between devices, shifted(): lax.ppermute(value, axis, [(i, (i + steps) % count) for i in range(count)])  25.1 us
    unnamed x76, local copies, waits for them, and re-layouts  22.4 us
    all_to_all x1, waiting for transfers between devices, per_device(): lax.all_to_all(state, ('sp_z',) + TP, split_axis=0, concat_axis=0, tiled=...  15.8 us
    all_to_all x1, starting transfers between devices, per_device(): lax.all_to_all(state, ('sp_z',) + TP, split_axis=0, concat_axis=0, tiled=...  11.8 us
    all_to_all x1, waiting for transfers between devices, per_device(): lax.all_to_all(packed, 'sp_z', split_axis=0, concat_axis=0, tiled=True)  10.5 us
    pallas_call x2, Pallas kernels, downs(): pl.pallas_call(body, grid=(1,), in_specs=[pl.BlockSpec(memory_space=pltpu...  7.2 us
  transfers between devices with their start and end apart: 32, of which 15 were waited for; matrix products, arithmetic and copies ran while one was open for 0% of the time, Pallas kernels for 22%

profile of v4, /device:TPU:4, one launch (start us, length us, event | category | flops | bytes accessed | tf_op | source)
XLA Modules:
  0.0 228.8 jit_solution(3087552918031094703)
XLA Ops:
  6.5 3.0 %shard_map.199 = (bf16[4,800,128]{2,1,0:T(8,128)(2,1)}, bf16[768,128]{1,0:T(8,128)(2,1)}, bf16[768,128]{1,0:T(8,128)(2,1)}, bf16[768,128]{1,0:T(8,128)(2,1)}, bf16[768,128]{1,0:T(8,128)(2,1)}) custom-call(s32[1]{0:T(128)} %bitcast.2.slot_ref, bf16[768,128]{1,0:T(8,128)(2,1)} %ks.1, bf16[768,128]{1,0:T(8,128)(2,1)} %vs.1, bf16[768,128]{1,0:T(8,128)(2,1)} %kl.1, ...), custom_call_target="tpu_custom_call" | custom-call | flops 625000000 | tf_op jit(solution)/shard_map/pallas_call | solution.py:89
  9.5 5.4 %all-to-all-start = ((bf16[4,800,128]{2,1,0:T(8,128)(2,1)}), bf16[4,800,128]{2,1,0:T(8,128)(2,1)S(1)}, u32[]{:S(2)}, u32[]{:S(2)}) async-start(bf16[4,800,128]{2,1,0:T(8,128)(2,1)} %get-tuple-element.63), calls=%async_computation | async-start | bytes 1638400 | tf_op jit(solution)/shard_map/all_to_all | solution.py:626
  15.0 2.1 shard_map.200
  17.1 10.5 %all-to-all-done.refs_6_ = bf16[4,800,128]{2,1,0:T(8,128)(2,1)S(1)} async-done(((bf16[4,800,128]{2,1,0:T(8,128)(2,1)}), bf16[4,800,128]{2,1,0:T(8,128)(2,1)S(1)}, u32[]{:S(2)}, u32[]{:S(2)}) %all-to-all-start) | async-done | bytes 819232 | tf_op jit(solution)/shard_map/all_to_all | solution.py:626
  28.4 1.3 collective-permute-start.3
  29.6 0.8 collective-permute-start.4
  31.0 2.1 collective-permute-start.1
  33.8 7.1 %collective-permute-done.refs_3_ = bf16[768,128]{1,0:T(8,128)(2,1)S(1)} collective-permute-done((bf16[768,128]{1,0:T(8,128)(2,1)S(1)}, bf16[768,128]{1,0:T(8,128)(2,1)S(1)}, u32[]{:S(2)}, u32[]{:S(2)}) %collective-permute-start) | collective-permute-done | bytes 196640 | tf_op jit(solution)/shard_map/ppermute | solution.py:24
  40.8 1.6 collective-permute-start.6
  42.4 1.7 collective-permute-start.7
  44.1 3.1 %collective-permute-start.8 = (bf16[256,2048]{1,0:T(8,128)(2,1)S(1)}, bf16[256,2048]{1,0:T(8,128)(2,1)}, u32[]{:S(2)}, u32[]{:S(2)}) collective-permute-start(bf16[256,2048]{1,0:T(8,128)(2,1)S(1)} %pad_maximum_fusion.refs_0_), channel_id=1, source_target_pairs={{0,4},{2,6},{4,0},{6,2},{1,5},{3,7},{5,1},{7,3},{8,12},{10,14},{12... | collective-permute-start | bytes 3145736 | tf_op jit(solution)/shard_map/ppermute | solution.py:24
  47.2 0.9 copy-done.29
  48.1 9.4 %shard_map.201 = (f32[4,144,768]{2,1,0:T(8,128)S(1)}, f32[4,8,768]{2,1,0:T(8,128)S(1)}) custom-call(s32[2]{0:T(128)S(1)} %pad_add_fusion.1.refs_0_, s32[4,34]{1,0:T(4,128)S(1)} %copy-done.28, bf16[768,128]{1,0:T(8,128)(2,1)S(1)} %copy-done.29, bf16[768,128]{1,0:T(8,128)(2,1)S(1)} %collective-permute-done.refs_3_, ...), custom_call_target="tpu_custom_call" | custom-call | flops 3000000000 | tf_op jit(solution)/shard_map/pallas_call | solution.py:346
  57.6 1.8 collective-permute-start.5
  59.4 14.8 %shard_map.202 = (f32[4,144,768]{2,1,0:T(8,128)S(1)}, f32[4,8,768]{2,1,0:T(8,128)S(1)}) custom-call(s32[2]{0:T(128)S(1)} %pad_add_fusion.1.refs_0_, s32[4,64]{1,0:T(4,128)S(1)} %copy-done.27, bf16[768,128]{1,0:T(8,128)(2,1)S(1)} %copy-done.29, bf16[768,128]{1,0:T(8,128)(2,1)S(1)} %collective-permute-done.refs_3_, ...), custom_call_target="tpu_custom_call" | custom-call | flops 6000000000 | tf_op jit(solution)/shard_map/pallas_call | solution.py:346
  74.2 11.1 %collective-permute-done.7.refs_2_ = bf16[256,2048]{1,0:T(8,128)(2,1)} collective-permute-done((bf16[256,2048]{1,0:T(8,128)(2,1)S(1)}, bf16[256,2048]{1,0:T(8,128)(2,1)}, u32[]{:S(2)}, u32[]{:S(2)}) %collective-permute-start.7) | collective-permute-done | bytes 1048608 | tf_op jit(solution)/shard_map/ppermute | solution.py:24
  85.3 1.3 collective-permute-done.8.refs_3_
  86.7 5.6 %collective-permute-done.5.refs_6_ = bf16[4,800,128]{2,1,0:T(8,128)(2,1)S(1)} collective-permute-done((bf16[4,800,128]{2,1,0:T(8,128)(2,1)S(1)}, bf16[4,800,128]{2,1,0:T(8,128)(2,1)S(1)}, u32[]{:S(2)}, u32[]{:S(2)}) %collective-permute-start.5) | collective-permute-done | bytes 819232 | tf_op jit(solution)/shard_map/ppermute | solution.py:24
  93.3 0.9 copy-done.25
  94.3 9.8 %shard_map.203 = bf16[32,112,128]{2,1,0:T(8,128)(2,1)S(1)} custom-call(s32[2]{0:T(128)S(1)} %pad_add_fusion.1.refs_0_, s32[4,34]{1,0:T(4,128)S(1)} %copy-done.26, bf16[768,128]{1,0:T(8,128)(2,1)S(1)} %copy-done.29, bf16[768,128]{1,0:T(8,128)(2,1)S(1)} %collective-permute-done.refs_3_, bf16[768,128]{1,0:T(8,128)(2,1)S(1)} %collective-permute-done.1.refs_4_, ...), custom_call_target="tpu_custom_call" | custom-call | flops 3000000000 | tf_op jit(solution)/shard_map/pallas_call | solution.py:346
  104.1 0.9 copy-done.6
  105.0 11.8 %all-to-all-start.1 = ((bf16[32,112,128]{2,1,0:T(8,128)(2,1)}), bf16[32,112,128]{2,1,0:T(8,128)(2,1)S(1)}, u32[]{:S(2)}, u32[]{:S(2)}) async-start(bf16[32,112,128]{2,1,0:T(8,128)(2,1)} %copy-done.6), calls=%async_computation.1 | async-start | bytes 1835008 | tf_op jit(solution)/shard_map/all_to_all | solution.py:663
  116.8 15.8 %all-to-all-done.1.arrived_ref = bf16[32,112,128]{2,1,0:T(8,128)(2,1)S(1)} async-done(((bf16[32,112,128]{2,1,0:T(8,128)(2,1)}), bf16[32,112,128]{2,1,0:T(8,128)(2,1)S(1)}, u32[]{:S(2)}, u32[]{:S(2)}) %all-to-all-start.1) | async-done | bytes 917536 | tf_op jit(solution)/shard_map/all_to_all | solution.py:663
  132.7 1.0 copy-done.12
  133.7 4.7 %shard_map.204.refs_1_.refs_0_ = bf16[96,2048]{1,0:T(8,128)(2,1)S(1)} custom-call(s32[2]{0:T(128)S(1)} %pad_add_fusion.place_ref.refs_0_, bf16[32,112,128]{2,1,0:T(8,128)(2,1)S(1)} %all-to-all-done.1.arrived_ref, bf16[256,2048]{1,0:T(8,128)(2,1)S(1)} %pad_maximum_fusion.refs_0_, bf16[256,2048]{1,0:T(8,128)(2,1)S(1)} %collective-permute-done.6.refs_1_, ...), custom_call_target="tpu_custom_call" | custom-call | flops 1250000000 | tf_op jit(solution)/shard_map/pallas_call | solution.py:396
  138.4 1.4 collective-permute-start.14
  139.9 1.9 collective-permute-start.15
  141.7 9.0 %collective-permute-done.14.refs_3_ = bf16[96,2048]{1,0:T(8,128)(2,1)S(1)} collective-permute-done((bf16[96,2048]{1,0:T(8,128)(2,1)S(1)}, bf16[96,2048]{1,0:T(8,128)(2,1)S(1)}, u32[]{:S(2)}, u32[]{:S(2)}) %collective-permute-start.14) | collective-permute-done | bytes 393248 | tf_op jit(solution)/shard_map/ppermute | solution.py:24
  151.3 0.8 collective-permute-start.18
  152.1 2.6 %collective-permute-start.19 = (bf16[48,2048]{1,0:T(8,128)(2,1)S(1)}, bf16[48,2048]{1,0:T(8,128)(2,1)S(1)}, u32[]{:S(2)}, u32[]{:S(2)}) collective-permute-start(bf16[48,2048]{1,0:T(8,128)(2,1)S(1)} %slice.9), channel_id=1, source_target_pairs={{0,6},{2,0},{4,2},{6,4},{1,7},{3,1},{5,3},{7,5},{8,14},{10,8},{12,... | collective-permute-start | bytes 589832 | tf_op jit(solution)/shard_map/ppermute | solution.py:24
  154.8 2.9 %copy-done = bf16[2048,1536]{1,0:T(8,128)(2,1)S(1)} copy-done((bf16[2048,1536]{1,0:T(8,128)(2,1)S(1)}, bf16[2048,1536]{1,0:T(8,128)(2,1)}, u32[]{:S(2)}) %copy-start) | copy-done | bytes 6291480
  157.6 4.3 %shard_map.205 = (bf16[576,704]{1,0:T(8,128)(2,1)S(1)}, bf16[576,704]{1,0:T(8,128)(2,1)S(1)}) custom-call(s32[2]{0:T(128)S(1)} %pad_add_fusion.place_ref.refs_0_, bf16[96,2048]{1,0:T(8,128)(2,1)S(1)} %shard_map.204.refs_1_.refs_0_, bf16[96,2048]{1,0:T(8,128)(2,1)S(1)} %collective-permute-done.13.refs_2_, ...), custom_call_target="tpu_custom_call" | custom-call | flops 1250000000 | tf_op jit(solution)/shard_map/pallas_call | solution.py:470
  162.6 0.9 collective-permute-done.20.refs_3_
  163.9 1.9 shard_map.206
  165.8 0.7 copy-done.13
  166.5 0.7 copy-done.15
  167.9 2.3 %collective-permute-start.22 = (bf16[32,704]{1,0:T(8,128)(2,1)S(1)}, bf16[32,704]{1,0:T(8,128)(2,1)S(1)}, u32[]{:S(2)}, u32[]{:S(2)}) collective-permute-start(bf16[32,704]{1,0:T(8,128)(2,1)S(1)} %get-tuple-element.104), channel_id=1, source_target_pairs={{0,8},{8,16},{16,24},{24,32},{32,40},{40,48},{48,56},{56,64},{64,7... | collective-permute-start | bytes 135176 | tf_op jit(solution)/shard_map/ppermute | solution.py:30
  170.2 3.6 %collective-permute-done.22.refs_3_ = bf16[32,704]{1,0:T(8,128)(2,1)S(1)} collective-permute-done((bf16[32,704]{1,0:T(8,128)(2,1)S(1)}, bf16[32,704]{1,0:T(8,128)(2,1)S(1)}, u32[]{:S(2)}, u32[]{:S(2)}) %collective-permute-start.22) | collective-permute-done | bytes 45088 | tf_op jit(solution)/shard_map/ppermute | solution.py:30
  173.9 1.9 copy-done.3
  175.8 1.0 copy-done.14
  176.7 0.9 copy-done.16
  177.7 0.9 copy-done.19
  178.6 2.9 %shard_map.207 = (bf16[1,96,2048]{2,1,0:T(8,128)(2,1)S(1)}, f32[1,96,2048]{2,1,0:T(8,128)S(1)}) custom-call(s32[2]{0:T(128)S(1)} %pad_add_fusion.place_ref.refs_0_, f32[3,704]{1,0:T(4,128)S(1)} %copy-done.21, f32[3,704]{1,0:T(4,128)S(1)} %copy-done.22, bf16[2048,768]{1,0:T(8,128)(2,1)S(1)} %copy-done.3, bf16[32,704]{1,0:T(8,128)(2,1)S(1)} %collective-permute-done.22.refs_3_, ...), custom_call_target="tpu_custom_call" | custom-call | flops 1000000000 | tf_op jit(solution)/shard_map/pallas_call | solution.py:530
  181.5 0.9 copy-done.11
  182.4 1.7 collective-permute-done.23.their_ref
  184.1 0.7 copy-done.33
  184.8 2.1 shard_map.208
  186.9 1.2 copy-done.8
  188.1 1.2 copy-done.10
  189.2 0.9 copy-done.17
  190.1 0.9 copy-done.20
  191.1 4.3 %shard_map.209 = (bf16[3,96,2048]{2,1,0:T(8,128)(2,1)S(1)}, f32[3,96,2048]{2,1,0:T(8,128)S(1)}) custom-call(s32[2]{0:T(128)S(1)} %pad_add_fusion.place_ref.refs_0_, f32[3,704]{1,0:T(4,128)S(1)} %copy-done.21, f32[3,704]{1,0:T(4,128)S(1)} %copy-done.22, bf16[2048,768]{1,0:T(8,128)(2,1)S(1)} %copy-done.4, bf16[32,704]{1,0:T(8,128)(2,1)S(1)} %collective-permute-done.22.refs_3_, ...), custom_call_target="tpu_custom_call" | custom-call | flops 2000000000 | tf_op jit(solution)/shard_map/pallas_call | solution.py:530
  195.4 1.4 copy-done.5
  196.9 0.7 collective-permute-start.25
  197.7 2.0 collective-permute-done.24.their_ref
  199.6 1.0 copy-done.30
  200.7 3.2 %shard_map.210 = (f32[96,2048]{1,0:T(8,128)}, bf16[96,2048]{1,0:T(8,128)(2,1)}, bf16[96,2048]{1,0:T(8,128)(2,1)}) custom-call(f32[3,96,2048]{2,1,0:T(8,128)} %copy-done.5, bf16[3,96,2048]{2,1,0:T(8,128)(2,1)} %copy-done.30), custom_call_target="tpu_custom_call" | custom-call | flops 525000000 | tf_op jit(solution)/shard_map/pallas_call | solution.py:555
  203.9 1.3 collective-permute-start.26
  205.1 0.7 collective-permute-start.27
  205.9 4.8 %collective-permute-done.25.refs_2_ = bf16[96,2048]{1,0:T(8,128)(2,1)S(1)} collective-permute-done((bf16[96,2048]{1,0:T(8,128)(2,1)}, bf16[96,2048]{1,0:T(8,128)(2,1)S(1)}, u32[]{:S(2)}, u32[]{:S(2)}) %collective-permute-start.25) | collective-permute-done | bytes 393248 | tf_op jit(solution)/shard_map/ppermute | solution.py:24
  210.6 6.4 %collective-permute-done.26.refs_3_ = bf16[96,2048]{1,0:T(8,128)(2,1)S(1)} collective-permute-done((bf16[96,2048]{1,0:T(8,128)(2,1)}, bf16[96,2048]{1,0:T(8,128)(2,1)S(1)}, u32[]{:S(2)}, u32[]{:S(2)}) %collective-permute-start.26) | collective-permute-done | bytes 393248 | tf_op jit(solution)/shard_map/ppermute | solution.py:24
  217.1 1.4 collective-permute-done.27.refs_4_
  218.5 0.7 copy-done.36
  219.2 2.8 %shard_map.211 = bf16[96,2048]{1,0:T(8,128)(2,1)} custom-call(bf16[96,2048]{1,0:T(8,128)(2,1)} %copy-done.2, f32[96,2048]{1,0:T(8,128)} %get-tuple-element.115.refs_1_, bf16[96,2048]{1,0:T(8,128)(2,1)} %copy-done.34, bf16[96,2048]{1,0:T(8,128)(2,1)} %copy-done.35, bf16[96,2048]{1,0:T(8,128)(2,1)} %copy-done.36, f32[1,2048]{1,0:T(1,128)} %bitcast.11), custom_call_target="tpu_custom_call" | custom-call | flops 500000000 | tf_op jit(solution)/shard_map/pallas_call | solution.py:580
  (96 shorter events, 5.5 us)
Async XLA Ops:
  9.5 18.2 %copy-start.31 = (bf16[128,2048]{1,0:T(8,128)(2,1)S(1)}, bf16[128,2048]{1,0:T(8,128)(2,1)}, u32[]{:S(2)}) copy-start(bf16[128,2048]{1,0:T(8,128)(2,1)} %param.31) | copy-start | bytes 1572868
  9.5 18.2 %copy-start.32 = (bf16[128,2048]{1,0:T(8,128)(2,1)S(1)}, bf16[128,2048]{1,0:T(8,128)(2,1)}, u32[]{:S(2)}) copy-start(bf16[128,2048]{1,0:T(8,128)(2,1)} %param.30) | copy-start | bytes 1572868
  9.5 18.1 %all-to-all-start = ((bf16[4,800,128]{2,1,0:T(8,128)(2,1)}), bf16[4,800,128]{2,1,0:T(8,128)(2,1)S(1)}, u32[]{:S(2)}, u32[]{:S(2)}) async-start(bf16[4,800,128]{2,1,0:T(8,128)(2,1)} %get-tuple-element.63), calls=%async_computation | async-start | bytes 1638400 | tf_op jit(solution)/shard_map/all_to_all | solution.py:626
  15.0 15.5 %copy-start.37 = (bf16[768,128]{1,0:T(8,128)(2,1)S(1)}, bf16[768,128]{1,0:T(8,128)(2,1)}, u32[]{:S(2)}) copy-start(bf16[768,128]{1,0:T(8,128)(2,1)} %get-tuple-element.74) | copy-start | bytes 589828
  15.0 32.3 %copy-start.28 = (s32[4,34]{1,0:T(4,128)S(1)}, s32[4,34]{1,0:T(4,128)}, u32[]{:S(2)}) copy-start(s32[4,34]{1,0:T(4,128)} %constant.21.clone.refs_1_) | copy-start | bytes 1636
  15.0 139.8 %all-gather.5.cloned.1.call-start = ((), (), s32[]{:S(2)}) async-start(), calls=%async_computation.3 | async-start | bytes 6684672 | tf_op jit(solution)/shard_map/all_gather | solution.py:629
  27.6 142.6 %all-gather.3.cloned.1.call-start = ((), (), s32[]{:S(2)}) async-start(), calls=%async_computation.2 | async-start | bytes 3342336 | tf_op jit(solution)/shard_map/all_gather | solution.py:635
  28.4 29.2 %collective-permute-start.3 = (bf16[4,800,128]{2,1,0:T(8,128)(2,1)S(1)}, bf16[4,800,128]{2,1,0:T(8,128)(2,1)}, u32[]{:S(2)}, u32[]{:S(2)}) collective-permute-start(bf16[4,800,128]{2,1,0:T(8,128)(2,1)S(1)} %all-to-all-done.refs_6_), channel_id=1, source_target_pairs={{0,8},{8,16},{16,24},{24,0},{1,9},{9,17},{17,25},{25,1},{2,10},{10... | collective-permute-start | bytes 2457608 | tf_op jit(solution)/shard_map/ppermute | solution.py:24
  29.6 27.9 %collective-permute-start.4 = (bf16[4,800,128]{2,1,0:T(8,128)(2,1)S(1)}, bf16[4,800,128]{2,1,0:T(8,128)(2,1)}, u32[]{:S(2)}, u32[]{:S(2)}) collective-permute-start(bf16[4,800,128]{2,1,0:T(8,128)(2,1)S(1)} %all-to-all-done.refs_6_), channel_id=1, source_target_pairs={{0,24},{8,0},{16,8},{24,16},{1,25},{9,1},{17,9},{25,17},{2,26},{10... | collective-permute-start | bytes 2457608 | tf_op jit(solution)/shard_map/ppermute | solution.py:24
  30.5 10.4 %collective-permute-start = (bf16[768,128]{1,0:T(8,128)(2,1)S(1)}, bf16[768,128]{1,0:T(8,128)(2,1)S(1)}, u32[]{:S(2)}, u32[]{:S(2)}) collective-permute-start(bf16[768,128]{1,0:T(8,128)(2,1)S(1)} %copy-done.37), channel_id=1, source_target_pairs={{0,32},{32,64},{64,96},{96,0},{1,33},{33,65},{65,97},{97,1},{2,34}... | collective-permute-start | bytes 589832 | tf_op jit(solution)/shard_map/ppermute | solution.py:24
  31.0 11.4 %collective-permute-start.1 = (bf16[768,128]{1,0:T(8,128)(2,1)}, bf16[768,128]{1,0:T(8,128)(2,1)S(1)}, u32[]{:S(2)}, u32[]{:S(2)}) collective-permute-start(bf16[768,128]{1,0:T(8,128)(2,1)} %get-tuple-element.75), channel_id=1, source_target_pairs={{0,64},{32,96},{64,0},{96,32},{1,65},{33,97},{65,1},{97,33},{2,66}... | collective-permute-start | bytes 589832 | tf_op jit(solution)/shard_map/ppermute | solution.py:24
  33.1 11.0 %collective-permute-start.2 = (bf16[768,128]{1,0:T(8,128)(2,1)}, bf16[768,128]{1,0:T(8,128)(2,1)S(1)}, u32[]{:S(2)}, u32[]{:S(2)}) collective-permute-start(bf16[768,128]{1,0:T(8,128)(2,1)} %get-tuple-element.76), channel_id=1, source_target_pairs={{0,96},{32,0},{64,32},{96,64},{1,97},{33,1},{65,33},{97,65},{2,98}... | collective-permute-start | bytes 589832 | tf_op jit(solution)/shard_map/ppermute | solution.py:24
  33.8 25.6 %copy-start.27 = (s32[4,64]{1,0:T(4,128)S(1)}, s32[4,64]{1,0:T(4,128)}, u32[]{:S(2)}) copy-start(s32[4,64]{1,0:T(4,128)} %constant.22.clone.refs_1_) | copy-start | bytes 3076
  40.8 33.4 %collective-permute-start.6 = (bf16[256,2048]{1,0:T(8,128)(2,1)S(1)}, bf16[256,2048]{1,0:T(8,128)(2,1)S(1)}, u32[]{:S(2)}, u32[]{:S(2)}) collective-permute-start(bf16[256,2048]{1,0:T(8,128)(2,1)S(1)} %pad_maximum_fusion.refs_0_), channel_id=1, source_target_pairs={{0,2},{2,4},{4,6},{6,0},{1,3},{3,5},{5,7},{7,1},{8,10},{10,12},{12... | collective-permute-start | bytes 3145736 | tf_op jit(solution)/shard_map/ppermute | solution.py:24
  42.4 42.9 %collective-permute-start.7 = (bf16[256,2048]{1,0:T(8,128)(2,1)S(1)}, bf16[256,2048]{1,0:T(8,128)(2,1)}, u32[]{:S(2)}, u32[]{:S(2)}) collective-permute-start(bf16[256,2048]{1,0:T(8,128)(2,1)S(1)} %pad_maximum_fusion.refs_0_), channel_id=1, source_target_pairs={{0,6},{2,0},{4,2},{6,4},{1,7},{3,1},{5,3},{7,5},{8,14},{10,8},{12,... | collective-permute-start | bytes 3145736 | tf_op jit(solution)/shard_map/ppermute | solution.py:24
  44.1 15.3 %copy-start.24 = (bf16[768,128]{1,0:T(8,128)(2,1)}, bf16[768,128]{1,0:T(8,128)(2,1)S(1)}, u32[]{:S(2)}) copy-start(bf16[768,128]{1,0:T(8,128)(2,1)S(1)} %collective-permute-done.2.refs_5_) | copy-start | bytes 589828
  44.1 42.6 %collective-permute-start.8 = (bf16[256,2048]{1,0:T(8,128)(2,1)S(1)}, bf16[256,2048]{1,0:T(8,128)(2,1)}, u32[]{:S(2)}, u32[]{:S(2)}) collective-permute-start(bf16[256,2048]{1,0:T(8,128)(2,1)S(1)} %pad_maximum_fusion.refs_0_), channel_id=1, source_target_pairs={{0,4},{2,6},{4,0},{6,2},{1,5},{3,7},{5,1},{7,3},{8,12},{10,14},{12... | collective-permute-start | bytes 3145736 | tf_op jit(solution)/shard_map/ppermute | solution.py:24
  47.2 0.9 copy-start.29
  57.6 35.7 %copy-start.26 = (s32[4,34]{1,0:T(4,128)S(1)}, s32[4,34]{1,0:T(4,128)}, u32[]{:S(2)}) copy-start(s32[4,34]{1,0:T(4,128)} %constant.23.clone.refs_1_) | copy-start | bytes 1636
  57.6 34.7 %collective-permute-start.5 = (bf16[4,800,128]{2,1,0:T(8,128)(2,1)S(1)}, bf16[4,800,128]{2,1,0:T(8,128)(2,1)S(1)}, u32[]{:S(2)}, u32[]{:S(2)}) collective-permute-start(bf16[4,800,128]{2,1,0:T(8,128)(2,1)S(1)} %all-to-all-done.refs_6_), channel_id=1, source_target_pairs={{0,16},{8,24},{16,0},{24,8},{1,17},{9,25},{17,1},{25,9},{2,18},{10... | collective-permute-start | bytes 2457608 | tf_op jit(solution)/shard_map/ppermute | solution.py:24
  92.3 40.4 %copy-start.23 = (f32[2048]{0:T(1024)S(1)}, f32[2048]{0:T(1024)}, u32[]{:S(2)}) copy-start(f32[2048]{0:T(1024)} %param.32) | copy-start | bytes 24580
  92.3 40.3 %collective-permute-start.10 = (bf16[256,2048]{1,0:T(8,128)(2,1)S(1)}, bf16[256,2048]{1,0:T(8,128)(2,1)}, u32[]{:S(2)}, u32[]{:S(2)}) collective-permute-start(bf16[256,2048]{1,0:T(8,128)(2,1)S(1)} %collective-permute-done.6.refs_1_), channel_id=1, source_target_pairs={{0,1},{1,0},{2,3},{3,2},{4,5},{5,4},{6,7},{7,6},{8,9},{9,8},{10,11... | collective-permute-start | bytes 3145736 | tf_op jit(solution)/shard_map/ppermute | solution.py:24
  92.3 40.3 %collective-permute-start.11 = (bf16[256,2048]{1,0:T(8,128)(2,1)}, bf16[256,2048]{1,0:T(8,128)(2,1)}, u32[]{:S(2)}, u32[]{:S(2)}) collective-permute-start(bf16[256,2048]{1,0:T(8,128)(2,1)} %collective-permute-done.7.refs_2_), channel_id=1, source_target_pairs={{0,1},{1,0},{2,3},{3,2},{4,5},{5,4},{6,7},{7,6},{8,9},{9,8},{10,11... | collective-permute-start | bytes 3145736 | tf_op jit(solution)/shard_map/ppermute | solution.py:24
  92.8 39.8 %collective-permute-start.12 = (bf16[256,2048]{1,0:T(8,128)(2,1)}, bf16[256,2048]{1,0:T(8,128)(2,1)}, u32[]{:S(2)}, u32[]{:S(2)}) collective-permute-start(bf16[256,2048]{1,0:T(8,128)(2,1)} %collective-permute-done.8.refs_3_), channel_id=1, source_target_pairs={{0,1},{1,0},{2,3},{3,2},{4,5},{5,4},{6,7},{7,6},{8,9},{9,8},{10,11... | collective-permute-start | bytes 3145736 | tf_op jit(solution)/shard_map/ppermute | solution.py:24
  92.8 39.8 %collective-permute-start.9 = (bf16[256,2048]{1,0:T(8,128)(2,1)S(1)}, bf16[256,2048]{1,0:T(8,128)(2,1)}, u32[]{:S(2)}, u32[]{:S(2)}) collective-permute-start(bf16[256,2048]{1,0:T(8,128)(2,1)S(1)} %pad_maximum_fusion.refs_0_), channel_id=1, source_target_pairs={{0,1},{1,0},{2,3},{3,2},{4,5},{5,4},{6,7},{7,6},{8,9},{9,8},{10,11... | collective-permute-start | bytes 3145736 | tf_op jit(solution)/shard_map/ppermute | solution.py:24
  93.3 0.9 copy-start.25
  104.1 0.9 copy-start.6
  105.0 27.7 %all-to-all-start.1 = ((bf16[32,112,128]{2,1,0:T(8,128)(2,1)}), bf16[32,112,128]{2,1,0:T(8,128)(2,1)S(1)}, u32[]{:S(2)}, u32[]{:S(2)}) async-start(bf16[32,112,128]{2,1,0:T(8,128)(2,1)} %copy-done.6), calls=%async_computation.1 | async-start | bytes 1835008 | tf_op jit(solution)/shard_map/all_to_all | solution.py:663
  132.7 1.0 copy-start.12
  138.4 23.6 %copy-start.2 = (bf16[96,2048]{1,0:T(8,128)(2,1)}, bf16[96,2048]{1,0:T(8,128)(2,1)S(1)}, u32[]{:S(2)}) copy-start(bf16[96,2048]{1,0:T(8,128)(2,1)S(1)} %shard_map.204.refs_1_.refs_0_) | copy-start | bytes 1179652
  138.4 12.3 %collective-permute-start.14 = (bf16[96,2048]{1,0:T(8,128)(2,1)S(1)}, bf16[96,2048]{1,0:T(8,128)(2,1)S(1)}, u32[]{:S(2)}, u32[]{:S(2)}) collective-permute-start(bf16[96,2048]{1,0:T(8,128)(2,1)S(1)} %shard_map.204.refs_1_.refs_0_), channel_id=1, source_target_pairs={{0,2},{2,4},{4,6},{6,0},{1,3},{3,5},{5,7},{7,1},{8,10},{10,12},{12... | collective-permute-start | bytes 1179656 | tf_op jit(solution)/shard_map/ppermute | solution.py:24
  139.9 10.9 %collective-permute-start.15 = (bf16[96,2048]{1,0:T(8,128)(2,1)S(1)}, bf16[96,2048]{1,0:T(8,128)(2,1)S(1)}, u32[]{:S(2)}, u32[]{:S(2)}) collective-permute-start(bf16[96,2048]{1,0:T(8,128)(2,1)S(1)} %shard_map.204.refs_1_.refs_0_), channel_id=1, source_target_pairs={{0,6},{2,0},{4,2},{6,4},{1,7},{3,1},{5,3},{7,5},{8,14},{10,8},{12,... | collective-permute-start | bytes 1179656 | tf_op jit(solution)/shard_map/ppermute | solution.py:24
  141.7 13.0 %collective-permute-start.13 = (bf16[96,2048]{1,0:T(8,128)(2,1)S(1)}, bf16[96,2048]{1,0:T(8,128)(2,1)S(1)}, u32[]{:S(2)}, u32[]{:S(2)}) collective-permute-start(bf16[96,2048]{1,0:T(8,128)(2,1)S(1)} %shard_map.204.refs_1_.refs_0_), channel_id=1, source_target_pairs={{0,1},{1,0},{2,3},{3,2},{4,5},{5,4},{6,7},{7,6},{8,9},{9,8},{10,11... | collective-permute-start | bytes 1179656 | tf_op jit(solution)/shard_map/ppermute | solution.py:24
  150.8 3.9 %collective-permute-start.16 = (bf16[96,2048]{1,0:T(8,128)(2,1)S(1)}, bf16[96,2048]{1,0:T(8,128)(2,1)S(1)}, u32[]{:S(2)}, u32[]{:S(2)}) collective-permute-start(bf16[96,2048]{1,0:T(8,128)(2,1)S(1)} %collective-permute-done.14.refs_3_), channel_id=1, source_target_pairs={{0,1},{1,0},{2,3},{3,2},{4,5},{5,4},{6,7},{7,6},{8,9},{9,8},{10,11... | collective-permute-start | bytes 1179656 | tf_op jit(solution)/shard_map/ppermute | solution.py:24
  150.8 3.9 %collective-permute-start.17 = (bf16[96,2048]{1,0:T(8,128)(2,1)S(1)}, bf16[96,2048]{1,0:T(8,128)(2,1)S(1)}, u32[]{:S(2)}, u32[]{:S(2)}) collective-permute-start(bf16[96,2048]{1,0:T(8,128)(2,1)S(1)} %collective-permute-done.15.refs_4_), channel_id=1, source_target_pairs={{0,1},{1,0},{2,3},{3,2},{4,5},{5,4},{6,7},{7,6},{8,9},{9,8},{10,11... | collective-permute-start | bytes 1179656 | tf_op jit(solution)/shard_map/ppermute | solution.py:24
  151.3 10.7 %collective-permute-start.18 = (bf16[48,2048]{1,0:T(8,128)(2,1)S(1)}, bf16[48,2048]{1,0:T(8,128)(2,1)S(1)}, u32[]{:S(2)}, u32[]{:S(2)}) collective-permute-start(bf16[48,2048]{1,0:T(8,128)(2,1)S(1)} %slice.8), channel_id=1, source_target_pairs={{0,2},{2,4},{4,6},{6,0},{1,3},{3,5},{5,7},{7,1},{8,10},{10,12},{12... | collective-permute-start | bytes 589832 | tf_op jit(solution)/shard_map/ppermute | solution.py:24
  152.1 9.9 %collective-permute-start.19 = (bf16[48,2048]{1,0:T(8,128)(2,1)S(1)}, bf16[48,2048]{1,0:T(8,128)(2,1)S(1)}, u32[]{:S(2)}, u32[]{:S(2)}) collective-permute-start(bf16[48,2048]{1,0:T(8,128)(2,1)S(1)} %slice.9), channel_id=1, source_target_pairs={{0,6},{2,0},{4,2},{6,4},{1,7},{3,1},{5,3},{7,5},{8,14},{10,8},{12,... | collective-permute-start | bytes 589832 | tf_op jit(solution)/shard_map/ppermute | solution.py:24
  154.7 2.9 %copy-start = (bf16[2048,1536]{1,0:T(8,128)(2,1)S(1)}, bf16[2048,1536]{1,0:T(8,128)(2,1)}, u32[]{:S(2)}) copy-start(bf16[2048,1536]{1,0:T(8,128)(2,1)} %all-gather.5.cloned.1.call-done.refs_7_.refs_8_.refs_5_.refs_6_) | copy-start | bytes 18874372
  157.6 6.2 %copy-start.1 = (bf16[2048,1536]{1,0:T(8,128)(2,1)S(1)}, bf16[2048,1536]{1,0:T(8,128)(2,1)}, u32[]{:S(2)}) copy-start(bf16[2048,1536]{1,0:T(8,128)(2,1)} %all-gather.5.cloned.1.call-done.refs_7_.refs_8_.refs_5_.refs_6_) | copy-start | bytes 18874372
  162.0 3.8 %copy-start.7 = (bf16[576,704]{1,0:T(8,128)(2,1)}, bf16[576,704]{1,0:T(8,128)(2,1)S(1)}, u32[]{:S(2)}) copy-start(bf16[576,704]{1,0:T(8,128)(2,1)S(1)} %get-tuple-element.111.refs_7_.refs_6_) | copy-start | bytes 2433028
  162.0 3.8 %copy-start.9 = (bf16[576,704]{1,0:T(8,128)(2,1)}, bf16[576,704]{1,0:T(8,128)(2,1)S(1)}, u32[]{:S(2)}) copy-start(bf16[576,704]{1,0:T(8,128)(2,1)S(1)} %get-tuple-element.112.refs_8_.refs_7_) | copy-start | bytes 2433028
  162.0 11.8 %copy-start.21 = (f32[3,704]{1,0:T(4,128)S(1)}, f32[3,704]{1,0:T(4,128)}, u32[]{:S(2)}) copy-start(f32[3,704]{1,0:T(4,128)} %refs_0_.3) | copy-start | bytes 25348
  162.0 11.8 %copy-start.22 = (f32[3,704]{1,0:T(4,128)S(1)}, f32[3,704]{1,0:T(4,128)}, u32[]{:S(2)}) copy-start(f32[3,704]{1,0:T(4,128)} %refs_1_.6) | copy-start | bytes 25348
  162.1 1.5 collective-permute-start.20
  162.1 1.7 collective-permute-start.21
  167.9 6.0 %collective-permute-start.22 = (bf16[32,704]{1,0:T(8,128)(2,1)S(1)}, bf16[32,704]{1,0:T(8,128)(2,1)S(1)}, u32[]{:S(2)}, u32[]{:S(2)}) collective-permute-start(bf16[32,704]{1,0:T(8,128)(2,1)S(1)} %get-tuple-element.104), channel_id=1, source_target_pairs={{0,8},{8,16},{16,24},{24,32},{32,40},{40,48},{48,56},{56,64},{64,7... | collective-permute-start | bytes 135176 | tf_op jit(solution)/shard_map/ppermute | solution.py:30
  173.9 1.9 copy-start.3
  175.8 1.0 copy-start.14
  176.7 0.9 copy-start.16
  177.7 0.9 copy-start.19
  178.6 8.3 %copy-start.4 = (bf16[2048,768]{1,0:T(8,128)(2,1)S(1)}, bf16[2048,768]{1,0:T(8,128)(2,1)}, u32[]{:S(2)}) copy-start(bf16[2048,768]{1,0:T(8,128)(2,1)} %all-gather.3.cloned.1.call-done.refs_2_) | copy-start | bytes 9437188
  182.4 1.7 collective-permute-start.23
  186.9 1.2 copy-start.8
  188.0 1.2 copy-start.10
  189.2 0.9 copy-start.17
  190.1 0.9 copy-start.20
  195.4 1.4 copy-start.5
  196.8 2.8 %collective-permute-start.24 = (bf16[3,96,2048]{2,1,0:T(8,128)(2,1)S(1)}, bf16[3,96,2048]{2,1,0:T(8,128)(2,1)S(1)}, u32[]{:S(2)}, u32[]{:S(2)}) collective-permute-start(bf16[3,96,2048]{2,1,0:T(8,128)(2,1)S(1)} %get-tuple-element.114), channel_id=1, source_target_pairs={{0,1},{1,0},{2,3},{3,2},{4,5},{5,4},{6,7},{7,6},{8,9},{9,8},{10,11... | collective-permute-start | bytes 3538952 | tf_op jit(solution)/shard_map/ppermute | solution.py:24
  196.9 13.7 %collective-permute-start.25 = (bf16[96,2048]{1,0:T(8,128)(2,1)}, bf16[96,2048]{1,0:T(8,128)(2,1)S(1)}, u32[]{:S(2)}, u32[]{:S(2)}) collective-permute-start(bf16[96,2048]{1,0:T(8,128)(2,1)} %shard_map.208), channel_id=1, source_target_pairs={{0,4},{2,6},{4,0},{6,2},{1,5},{3,7},{5,1},{7,3},{8,12},{10,14},{12... | collective-permute-start | bytes 1179656 | tf_op jit(solution)/shard_map/ppermute | solution.py:24
  199.6 1.0 copy-start.30
  203.9 13.2 %collective-permute-start.26 = (bf16[96,2048]{1,0:T(8,128)(2,1)}, bf16[96,2048]{1,0:T(8,128)(2,1)S(1)}, u32[]{:S(2)}, u32[]{:S(2)}) collective-permute-start(bf16[96,2048]{1,0:T(8,128)(2,1)} %get-tuple-element.117), channel_id=1, source_target_pairs={{0,6},{2,0},{4,2},{6,4},{1,7},{3,1},{5,3},{7,5},{8,14},{10,8},{12,... | collective-permute-start | bytes 1179656 | tf_op jit(solution)/shard_map/ppermute | solution.py:24
  205.1 13.3 %collective-permute-start.27 = (bf16[96,2048]{1,0:T(8,128)(2,1)}, bf16[96,2048]{1,0:T(8,128)(2,1)S(1)}, u32[]{:S(2)}, u32[]{:S(2)}) collective-permute-start(bf16[96,2048]{1,0:T(8,128)(2,1)} %get-tuple-element.118), channel_id=1, source_target_pairs={{0,2},{2,4},{4,6},{6,0},{1,3},{3,5},{5,7},{7,1},{8,10},{10,12},{12... | collective-permute-start | bytes 1179656 | tf_op jit(solution)/shard_map/ppermute | solution.py:24
  210.6 7.8 %copy-start.34 = (bf16[96,2048]{1,0:T(8,128)(2,1)}, bf16[96,2048]{1,0:T(8,128)(2,1)S(1)}, u32[]{:S(2)}) copy-start(bf16[96,2048]{1,0:T(8,128)(2,1)S(1)} %collective-permute-done.25.refs_2_) | copy-start | bytes 1179652
  217.1 1.4 copy-start.35
  (6 other events, 4.5 us)
Sparse Core Ops, SparseCore 0:
  27.7 72.8 all-gather.4
  102.8 56.5 all-gather.2

commit v5 on v2

--- a/solution.py
+++ b/solution.py
@@ -631,7 +631,9 @@
     after = shifted(pairs, "sp_x", -1)
     queries = [asked[0]] + [shifted(asked[k], "sp_z", k) for k in range(1, depth)]
     mixer = jnp.concatenate([mixer_small, mixer_large], axis=0)
-    mixers = [mixer] + [shifted(mixer, "tp_y", k) for k in (1, -1, 2)]
+    mixers = [mixer]
+    for k in (1, -1, 2):
+        mixers.append(shifted(mixer, "tp_y", k))
     calls = ((0,), (-1, 1), (2,))
     tables = work_tables(calls, depth, turns)
     place_here = jnp.stack([slot, column])
@@ -650,15 +652,16 @@
     pairs, before, after, state = lax.optimization_barrier((pairs, before, after, state))
     far = shifted(pairs, "sp_x", 2)
     state = call(1, [before, after], state)
+    far_mixer = mixers.pop()
     far, state, mixers = lax.optimization_barrier((far, state, mixers))
-    shifts = (0, -1, 1, 2)
-    mixers = [(a, shift, 0) for a, shift in zip(mixers, shifts)] + [
-        (shifted(a, "tp_c", 1), shift, 1) for a, shift in zip(mixers, shifts)
-    ]
+    crossed = [shifted(a, "tp_c", 1) for a in mixers]
     state = call(2, [far], state)
     arrived = lax.all_to_all(state, ("sp_z",) + TP, split_axis=0, concat_axis=0, tiled=True)
+    crossed.append(shifted(far_mixer, "tp_c", 1))
+    shifts = (0, -1, 1, 2)
+    mixers = [(a, k, 0) for a, k in zip(mixers + [far_mixer], shifts)]
+    mixers += [(a, k, 1) for a, k in zip(crossed, shifts)]
     place = jnp.stack([lax.axis_index("tp_y"), lax.axis_index("tp_c")]).astype(jnp.int32)
-    arrived, weights = lax.optimization_barrier((arrived, weights))
     mixed = mix_rows(place, arrived, mixers, residual, mix_gain)
     turns_y, cores = lax.axis_size("tp_y"), lax.axis_size("tp_c")
     own_rows = mixed.shape[0]
@@ -667,7 +670,6 @@
     spots = [(0, 0), (0, 1), (-1, 0), (1, 0), (-1, 1), (1, 1), (2, 0), (2, 1)]
     last_one, next_one = shifted(mixed, "tp_y", 1), shifted(mixed, "tp_y", -1)
     near = ups([mixed, shifted(mixed, "tp_c", 1)], weights, width, 3.0, place=place)
-    near, last_one, next_one = lax.optimization_barrier((near, last_one, next_one))
     opposite = [shifted(last_one[:half], "tp_y", 1), shifted(next_one[half:], "tp_y", -1)]
     beside = [last_one, next_one] + [shifted(a, "tp_c", 1) for a in (last_one, next_one)]
     beside = ups(beside, weights, width, 4.0, place=place)

time: 221 us -> 232 us (1.050)
  the two profiles are of different devices: /device:TPU:0 before, /device:TPU:4 now
where the time goes in v5:
time: 232 us; the launch traced here: 231 us
  waiting for transfers between devices  91.5 us (39%)
  Pallas kernels  66.7 us (29%)
  starting transfers between devices  40.8 us (18%)
  local copies, waits for them, and re-layouts  18.3 us (8%)
  between operations  13.7 us (6%)
    ppermute x27, waiting for transfers between devices, shifted(): lax.ppermute(value, axis, [(i, (i + steps) % count) for i in range(count)])  62.2 us
    pallas_call x3, Pallas kernels, attend(): pl.pallas_call(body, in_specs=[sm, sm] + [vm] * (len(args) - 2), out_spec...  34.2 us
    ppermute x27, starting transfers between devices, shifted(): lax.ppermute(value, axis, [(i, (i + steps) % count) for i in range(count)])  22.5 us
    unnamed x49, local copies, waits for them, and re-layouts  16.8 us
    all_to_all x1, waiting for transfers between devices, per_device(): lax.all_to_all(state, ('sp_z',) + TP, split_axis=0, concat_axis=0, tiled=...  15.8 us
    all_to_all x1, waiting for transfers between devices, per_device(): lax.all_to_all(packed, 'sp_z', split_axis=0, concat_axis=0, tiled=True)  10.4 us
    all_to_all x1, starting transfers between devices, per_device(): lax.all_to_all(state, ('sp_z',) + TP, split_axis=0, concat_axis=0, tiled=...  10 us
    pallas_call x3, Pallas kernels, ups(): pl.pallas_call(body, grid=(1,), in_specs=[pl.BlockSpec(memory_space=pltpu...  7.42 us
  transfers between devices with their start and end apart: 31, of which 12 were waited for; matrix products, arithmetic and copies ran while one was open for 1% of the time, Pallas kernels for 21%

profile of v5, /device:TPU:4, one launch (start us, length us, event | category | flops | bytes accessed | tf_op | source)
XLA Modules:
  0.0 231.1 jit_solution(11691730460811851614)
XLA Ops:
  6.5 2.9 %shard_map.199 = (bf16[4,800,128]{2,1,0:T(8,128)(2,1)}, bf16[768,128]{1,0:T(8,128)(2,1)}, bf16[768,128]{1,0:T(8,128)(2,1)}, bf16[768,128]{1,0:T(8,128)(2,1)}, bf16[768,128]{1,0:T(8,128)(2,1)}) custom-call(s32[1]{0:T(128)} %bitcast.2.slot_ref, bf16[768,128]{1,0:T(8,128)(2,1)} %ks.1, bf16[768,128]{1,0:T(8,128)(2,1)} %vs.1, bf16[768,128]{1,0:T(8,128)(2,1)} %kl.1, ...), custom_call_target="tpu_custom_call" | custom-call | flops 625000000 | tf_op jit(solution)/shard_map/pallas_call | solution.py:89
  9.5 5.4 %all-to-all-start = ((bf16[4,800,128]{2,1,0:T(8,128)(2,1)}), bf16[4,800,128]{2,1,0:T(8,128)(2,1)S(1)}, u32[]{:S(2)}, u32[]{:S(2)}) async-start(bf16[4,800,128]{2,1,0:T(8,128)(2,1)} %get-tuple-element.61), calls=%async_computation | async-start | bytes 1638400 | tf_op jit(solution)/shard_map/all_to_all | solution.py:626
  15.0 2.2 shard_map.200
  17.2 10.4 %all-to-all-done.refs_6_ = bf16[4,800,128]{2,1,0:T(8,128)(2,1)S(1)} async-done(((bf16[4,800,128]{2,1,0:T(8,128)(2,1)}), bf16[4,800,128]{2,1,0:T(8,128)(2,1)S(1)}, u32[]{:S(2)}, u32[]{:S(2)}) %all-to-all-start) | async-done | bytes 819232 | tf_op jit(solution)/shard_map/all_to_all | solution.py:626
  27.6 1.3 collective-permute-start.3
  28.9 0.8 collective-permute-start.4
  29.8 3.3 %collective-permute-start.8 = (bf16[256,2048]{1,0:T(8,128)(2,1)S(1)}, bf16[256,2048]{1,0:T(8,128)(2,1)S(1)}, u32[]{:S(2)}, u32[]{:S(2)}) collective-permute-start(bf16[256,2048]{1,0:T(8,128)(2,1)S(1)} %constant_dynamic-update-slice_fusion.refs_0_), channel_id=1, source_target_pairs={{0,4},{2,6},{4,0},{6,2},{1,5},{3,7},{5,1},{7,3},{8,12},{10,14},{12... | collective-permute-start | bytes 3145736 | tf_op jit(solution)/shard_map/ppermute | solution.py:24
  33.1 0.6 collective-permute-start
  33.6 2.1 collective-permute-start.1
  35.7 8.8 %collective-permute-done.refs_3_ = bf16[768,128]{1,0:T(8,128)(2,1)S(1)} collective-permute-done((bf16[768,128]{1,0:T(8,128)(2,1)}, bf16[768,128]{1,0:T(8,128)(2,1)S(1)}, u32[]{:S(2)}, u32[]{:S(2)}) %collective-permute-start) | collective-permute-done | bytes 196640 | tf_op jit(solution)/shard_map/ppermute | solution.py:24
  44.5 0.1 pad_add_fusion.1.refs_0_
  44.6 0.7 collective-permute-start.6
  45.3 7.8 %collective-permute-done.2.refs_5_ = bf16[768,128]{1,0:T(8,128)(2,1)S(1)} collective-permute-done((bf16[768,128]{1,0:T(8,128)(2,1)}, bf16[768,128]{1,0:T(8,128)(2,1)S(1)}, u32[]{:S(2)}, u32[]{:S(2)}) %collective-permute-start.2) | collective-permute-done | bytes 196640 | tf_op jit(solution)/shard_map/ppermute | solution.py:24
  53.1 1.0 collective-permute-start.7
  54.1 0.9 copy-done.16
  55.0 9.4 %shard_map.201 = (f32[4,144,768]{2,1,0:T(8,128)S(1)}, f32[4,8,768]{2,1,0:T(8,128)S(1)}) custom-call(s32[2]{0:T(128)S(1)} %pad_add_fusion.1.refs_0_, s32[4,34]{1,0:T(4,128)S(1)} %copy-done.15, bf16[768,128]{1,0:T(8,128)(2,1)S(1)} %copy-done.16, bf16[768,128]{1,0:T(8,128)(2,1)S(1)} %collective-permute-done.refs_3_, ...), custom_call_target="tpu_custom_call" | custom-call | flops 3000000000 | tf_op jit(solution)/shard_map/pallas_call | solution.py:346
  64.4 1.3 collective-permute-start.5
  65.7 15.0 %shard_map.202 = (f32[4,144,768]{2,1,0:T(8,128)S(1)}, f32[4,8,768]{2,1,0:T(8,128)S(1)}) custom-call(s32[2]{0:T(128)S(1)} %pad_add_fusion.1.refs_0_, s32[4,64]{1,0:T(4,128)S(1)} %copy-done.14, bf16[768,128]{1,0:T(8,128)(2,1)S(1)} %copy-done.16, bf16[768,128]{1,0:T(8,128)(2,1)S(1)} %collective-permute-done.refs_3_, ...), custom_call_target="tpu_custom_call" | custom-call | flops 6000000000 | tf_op jit(solution)/shard_map/pallas_call | solution.py:346
  80.7 20.7 %collective-permute-done.5.refs_6_ = bf16[4,800,128]{2,1,0:T(8,128)(2,1)S(1)} collective-permute-done((bf16[4,800,128]{2,1,0:T(8,128)(2,1)S(1)}, bf16[4,800,128]{2,1,0:T(8,128)(2,1)S(1)}, u32[]{:S(2)}, u32[]{:S(2)}) %collective-permute-start.5) | collective-permute-done | bytes 819232 | tf_op jit(solution)/shard_map/ppermute | solution.py:24
  101.4 0.5 collective-permute-start.11
  101.9 9.8 %shard_map.203 = bf16[32,112,128]{2,1,0:T(8,128)(2,1)S(1)} custom-call(s32[2]{0:T(128)S(1)} %pad_add_fusion.1.refs_0_, s32[4,34]{1,0:T(4,128)S(1)} %copy-done.13, bf16[768,128]{1,0:T(8,128)(2,1)S(1)} %copy-done.16, bf16[768,128]{1,0:T(8,128)(2,1)S(1)} %collective-permute-done.refs_3_, bf16[768,128]{1,0:T(8,128)(2,1)S(1)} %collective-permute-done.1.refs_4_, ...), custom_call_target="tpu_custom_call" | custom-call | flops 3000000000 | tf_op jit(solution)/shard_map/pallas_call | solution.py:346
  111.7 0.9 copy-done.5
  112.6 10.0 %all-to-all-start.1 = ((bf16[32,112,128]{2,1,0:T(8,128)(2,1)}), bf16[32,112,128]{2,1,0:T(8,128)(2,1)S(1)}, u32[]{:S(2)}, u32[]{:S(2)}) async-start(bf16[32,112,128]{2,1,0:T(8,128)(2,1)} %copy-done.5), calls=%async_computation.1 | async-start | bytes 1835008 | tf_op jit(solution)/shard_map/all_to_all | solution.py:659
  122.7 0.1 pad_add_fusion.place_ref.refs_0_
  122.8 15.8 %all-to-all-done.1.arrived_ref = bf16[32,112,128]{2,1,0:T(8,128)(2,1)S(1)} async-done(((bf16[32,112,128]{2,1,0:T(8,128)(2,1)}), bf16[32,112,128]{2,1,0:T(8,128)(2,1)S(1)}, u32[]{:S(2)}, u32[]{:S(2)}) %all-to-all-start.1) | async-done | bytes 917536 | tf_op jit(solution)/shard_map/all_to_all | solution.py:659
  138.6 1.0 copy-done.7
  139.5 4.7 %shard_map.204.refs_1_.refs_0_ = bf16[96,2048]{1,0:T(8,128)(2,1)S(1)} custom-call(s32[2]{0:T(128)S(1)} %pad_add_fusion.place_ref.refs_0_, bf16[32,112,128]{2,1,0:T(8,128)(2,1)S(1)} %all-to-all-done.1.arrived_ref, bf16[256,2048]{1,0:T(8,128)(2,1)S(1)} %constant_dynamic-update-slice_fusion.refs_0_, bf16[256,2048]{1,0:T(8,128)(2,1)} %collective-permute-done.6.refs_1_, ...), custom_call_target="tpu_custom_call" | custom-call | flops 1250000000 | tf_op jit(solution)/shard_map/pallas_call | solution.py:396
  144.3 0.6 collective-permute-start.13
  144.9 2.7 %collective-permute-start.14 = (bf16[96,2048]{1,0:T(8,128)(2,1)S(1)}, bf16[96,2048]{1,0:T(8,128)(2,1)S(1)}, u32[]{:S(2)}, u32[]{:S(2)}) collective-permute-start(bf16[96,2048]{1,0:T(8,128)(2,1)S(1)} %shard_map.204.refs_1_.refs_0_), channel_id=1, source_target_pairs={{0,6},{2,0},{4,2},{6,4},{1,7},{3,1},{5,3},{7,5},{8,14},{10,8},{12,... | collective-permute-start | bytes 1179656 | tf_op jit(solution)/shard_map/ppermute | solution.py:24
  147.6 9.1 %collective-permute-done.13.refs_1_ = bf16[96,2048]{1,0:T(8,128)(2,1)S(1)} collective-permute-done((bf16[96,2048]{1,0:T(8,128)(2,1)S(1)}, bf16[96,2048]{1,0:T(8,128)(2,1)S(1)}, u32[]{:S(2)}, u32[]{:S(2)}) %collective-permute-start.13) | collective-permute-done | bytes 393248 | tf_op jit(solution)/shard_map/ppermute | solution.py:24
  156.7 0.5 collective-permute-start.16
  157.2 0.7 slice.8
  157.9 0.7 slice.9
  158.6 3.2 %collective-permute-start.18 = (bf16[48,2048]{1,0:T(8,128)(2,1)}, bf16[48,2048]{1,0:T(8,128)(2,1)}, u32[]{:S(2)}, u32[]{:S(2)}) collective-permute-start(bf16[48,2048]{1,0:T(8,128)(2,1)} %slice.9), channel_id=1, source_target_pairs={{0,6},{2,0},{4,2},{6,4},{1,7},{3,1},{5,3},{7,5},{8,14},{10,8},{12,... | collective-permute-start | bytes 589832 | tf_op jit(solution)/shard_map/ppermute | solution.py:24
  161.8 0.7 copy-done.8
  162.6 3.7 %copy-done = bf16[2048,2304]{1,0:T(8,128)(2,1)S(1)} copy-done((bf16[2048,2304]{1,0:T(8,128)(2,1)S(1)}, bf16[2048,2304]{1,0:T(8,128)(2,1)}, u32[]{:S(2)}) %copy-start) | copy-done | bytes 9437208
  166.3 1.0 copy-done.9
  167.3 3.1 %shard_map.205 = (bf16[384,704]{1,0:T(8,128)(2,1)S(1)}, bf16[384,704]{1,0:T(8,128)(2,1)S(1)}) custom-call(s32[2]{0:T(128)S(1)} %pad_add_fusion.place_ref.refs_0_, bf16[96,2048]{1,0:T(8,128)(2,1)S(1)} %collective-permute-done.13.refs_1_, bf16[96,2048]{1,0:T(8,128)(2,1)S(1)} %collective-permute-done.14.refs_2_, ...), custom_call_target="tpu_custom_call" | custom-call | flops 1000000000 | tf_op jit(solution)/shard_map/pallas_call | solution.py:470
  170.4 0.1 collective-permute-start.19
  170.5 0.5 collective-permute-start.20
  171.0 1.9 shard_map.206
  173.0 2.3 %shard_map.207 = (bf16[192,704]{1,0:T(8,128)(2,1)S(1)}, bf16[192,704]{1,0:T(8,128)(2,1)S(1)}, bf16[8,16,704]{2,1,0:T(8,128)(2,1)S(1)}, bf16[8,16,704]{2,1,0:T(8,128)(2,1)S(1)}, bf16[32,704]{1,0:T(8,128)(2,1)S(1)}) custom-call(s32[2]{0:T(128)S(1)} %pad_add_fusion.place_ref.refs_0_, bf16[48,2048]{1,0:T(8,128)(2,1)S(1)} %collective-permute-done.17.refs_1_, ...), custom_call_target="tpu_custom_call" | custom-call | flops 750000000 | tf_op jit(solution)/shard_map/pallas_call | solution.py:470
  175.4 2.8 %collective-permute-start.22 = (bf16[32,704]{1,0:T(8,128)(2,1)S(1)}, bf16[32,704]{1,0:T(8,128)(2,1)S(1)}, u32[]{:S(2)}, u32[]{:S(2)}) collective-permute-start(bf16[32,704]{1,0:T(8,128)(2,1)S(1)} %get-tuple-element.98), channel_id=1, source_target_pairs={{0,8},{8,16},{16,24},{24,32},{32,40},{40,48},{48,56},{56,64},{64,7... | collective-permute-start | bytes 135176 | tf_op jit(solution)/shard_map/ppermute | solution.py:30
  178.2 3.1 %collective-permute-done.22.refs_3_ = bf16[32,704]{1,0:T(8,128)(2,1)S(1)} collective-permute-done((bf16[32,704]{1,0:T(8,128)(2,1)S(1)}, bf16[32,704]{1,0:T(8,128)(2,1)S(1)}, u32[]{:S(2)}, u32[]{:S(2)}) %collective-permute-start.22) | collective-permute-done | bytes 45088 | tf_op jit(solution)/shard_map/ppermute | solution.py:30
  181.4 2.9 %shard_map.208 = (bf16[1,96,2048]{2,1,0:T(8,128)(2,1)S(1)}, f32[1,96,2048]{2,1,0:T(8,128)S(1)}) custom-call(s32[2]{0:T(128)S(1)} %pad_add_fusion.place_ref.refs_0_, f32[3,704]{1,0:T(4,128)S(1)} %copy-done.10, f32[3,704]{1,0:T(4,128)S(1)} %copy-done.11, bf16[2048,2304]{1,0:T(8,128)(2,1)S(1)} %copy-done.1, ...), custom_call_target="tpu_custom_call" | custom-call | flops 1000000000 | tf_op jit(solution)/shard_map/pallas_call | solution.py:530
  184.2 0.9 copy-done.6
  185.1 1.7 collective-permute-done.23.their_ref
  186.8 0.7 copy-done.20
  187.6 2.0 shard_map.209
  189.6 3.7 %copy-done.2 = bf16[2048,2304]{1,0:T(8,128)(2,1)S(1)} copy-done((bf16[2048,2304]{1,0:T(8,128)(2,1)S(1)}, bf16[2048,2304]{1,0:T(8,128)(2,1)}, u32[]{:S(2)}) %copy-start.2) | copy-done | bytes 9437208
  193.3 4.3 %shard_map.210 = (bf16[3,96,2048]{2,1,0:T(8,128)(2,1)S(1)}, f32[3,96,2048]{2,1,0:T(8,128)S(1)}) custom-call(s32[2]{0:T(128)S(1)} %pad_add_fusion.place_ref.refs_0_, f32[3,704]{1,0:T(4,128)S(1)} %copy-done.10, f32[3,704]{1,0:T(4,128)S(1)} %copy-done.11, bf16[2048,2304]{1,0:T(8,128)(2,1)S(1)} %copy-done.2, ...), custom_call_target="tpu_custom_call" | custom-call | flops 2000000000 | tf_op jit(solution)/shard_map/pallas_call | solution.py:530
  197.7 1.4 copy-done.4
  199.1 0.1 collective-permute-start.24
  199.2 1.2 collective-permute-start.25
  200.4 1.5 collective-permute-done.24.their_ref
  201.9 1.0 copy-done.17
  202.9 3.2 %shard_map.211 = (f32[96,2048]{1,0:T(8,128)}, bf16[96,2048]{1,0:T(8,128)(2,1)}, bf16[96,2048]{1,0:T(8,128)(2,1)}) custom-call(f32[3,96,2048]{2,1,0:T(8,128)} %copy-done.4, bf16[3,96,2048]{2,1,0:T(8,128)(2,1)} %copy-done.17), custom_call_target="tpu_custom_call" | custom-call | flops 525000000 | tf_op jit(solution)/shard_map/pallas_call | solution.py:555
  206.1 1.7 collective-permute-start.26
  207.9 0.3 collective-permute-start.27
  208.2 4.7 %collective-permute-done.25.refs_2_ = bf16[96,2048]{1,0:T(8,128)(2,1)S(1)} collective-permute-done((bf16[96,2048]{1,0:T(8,128)(2,1)}, bf16[96,2048]{1,0:T(8,128)(2,1)S(1)}, u32[]{:S(2)}, u32[]{:S(2)}) %collective-permute-start.25) | collective-permute-done | bytes 393248 | tf_op jit(solution)/shard_map/ppermute | solution.py:24
  212.9 6.9 %collective-permute-done.26.refs_3_ = bf16[96,2048]{1,0:T(8,128)(2,1)S(1)} collective-permute-done((bf16[96,2048]{1,0:T(8,128)(2,1)}, bf16[96,2048]{1,0:T(8,128)(2,1)S(1)}, u32[]{:S(2)}, u32[]{:S(2)}) %collective-permute-start.26) | collective-permute-done | bytes 393248 | tf_op jit(solution)/shard_map/ppermute | solution.py:24
  219.8 0.9 collective-permute-done.27.refs_4_
  220.8 0.7 copy-done.23
  221.5 2.8 %shard_map.212 = bf16[96,2048]{1,0:T(8,128)(2,1)} custom-call(bf16[96,2048]{1,0:T(8,128)(2,1)} %copy-done.3, f32[96,2048]{1,0:T(8,128)} %get-tuple-element.111.refs_1_, bf16[96,2048]{1,0:T(8,128)(2,1)} %copy-done.21, bf16[96,2048]{1,0:T(8,128)(2,1)} %copy-done.22, bf16[96,2048]{1,0:T(8,128)(2,1)} %copy-done.23, f32[1,2048]{1,0:T(1,128)} %bitcast.11), custom_call_target="tpu_custom_call" | custom-call | flops 500000000 | tf_op jit(solution)/shard_map/pallas_call | solution.py:580
  (67 shorter events, 0.3 us)
Async XLA Ops:
  9.5 18.1 %copy-start.18 = (bf16[128,2048]{1,0:T(8,128)(2,1)S(1)}, bf16[128,2048]{1,0:T(8,128)(2,1)}, u32[]{:S(2)}) copy-start(bf16[128,2048]{1,0:T(8,128)(2,1)} %param.30) | copy-start | bytes 1572868
  9.5 18.1 %all-to-all-start = ((bf16[4,800,128]{2,1,0:T(8,128)(2,1)}), bf16[4,800,128]{2,1,0:T(8,128)(2,1)S(1)}, u32[]{:S(2)}, u32[]{:S(2)}) async-start(bf16[4,800,128]{2,1,0:T(8,128)(2,1)} %get-tuple-element.61), calls=%async_computation | async-start | bytes 1638400 | tf_op jit(solution)/shard_map/all_to_all | solution.py:626
  14.9 14.8 %copy-start.19 = (bf16[128,2048]{1,0:T(8,128)(2,1)S(1)}, bf16[128,2048]{1,0:T(8,128)(2,1)}, u32[]{:S(2)}) copy-start(bf16[128,2048]{1,0:T(8,128)(2,1)} %param.31) | copy-start | bytes 1572868
  14.9 39.1 %copy-start.15 = (s32[4,34]{1,0:T(4,128)S(1)}, s32[4,34]{1,0:T(4,128)}, u32[]{:S(2)}) copy-start(s32[4,34]{1,0:T(4,128)} %constant.21.clone.refs_1_) | copy-start | bytes 1636
  14.9 147.7 %all-gather.2.cloned.1.call-start = ((), (), s32[]{:S(2)}) async-start(), calls=%async_computation.2 | async-start | bytes 10027008 | tf_op jit(solution)/shard_map/all_gather | solution.py:629
  27.6 36.8 %collective-permute-start.3 = (bf16[4,800,128]{2,1,0:T(8,128)(2,1)S(1)}, bf16[4,800,128]{2,1,0:T(8,128)(2,1)}, u32[]{:S(2)}, u32[]{:S(2)}) collective-permute-start(bf16[4,800,128]{2,1,0:T(8,128)(2,1)S(1)} %all-to-all-done.refs_6_), channel_id=1, source_target_pairs={{0,8},{8,16},{16,24},{24,0},{1,9},{9,17},{17,25},{25,1},{2,10},{10... | collective-permute-start | bytes 2457608 | tf_op jit(solution)/shard_map/ppermute | solution.py:24
  28.9 35.5 %collective-permute-start.4 = (bf16[4,800,128]{2,1,0:T(8,128)(2,1)S(1)}, bf16[4,800,128]{2,1,0:T(8,128)(2,1)}, u32[]{:S(2)}, u32[]{:S(2)}) collective-permute-start(bf16[4,800,128]{2,1,0:T(8,128)(2,1)S(1)} %all-to-all-done.refs_6_), channel_id=1, source_target_pairs={{0,24},{8,0},{16,8},{24,16},{1,25},{9,1},{17,9},{25,17},{2,26},{10... | collective-permute-start | bytes 2457608 | tf_op jit(solution)/shard_map/ppermute | solution.py:24
  29.8 35.9 %collective-permute-start.8 = (bf16[256,2048]{1,0:T(8,128)(2,1)S(1)}, bf16[256,2048]{1,0:T(8,128)(2,1)S(1)}, u32[]{:S(2)}, u32[]{:S(2)}) collective-permute-start(bf16[256,2048]{1,0:T(8,128)(2,1)S(1)} %constant_dynamic-update-slice_fusion.refs_0_), channel_id=1, source_target_pairs={{0,4},{2,6},{4,0},{6,2},{1,5},{3,7},{5,1},{7,3},{8,12},{10,14},{12... | collective-permute-start | bytes 3145736 | tf_op jit(solution)/shard_map/ppermute | solution.py:24
  33.1 11.4 %collective-permute-start = (bf16[768,128]{1,0:T(8,128)(2,1)}, bf16[768,128]{1,0:T(8,128)(2,1)S(1)}, u32[]{:S(2)}, u32[]{:S(2)}) collective-permute-start(bf16[768,128]{1,0:T(8,128)(2,1)} %get-tuple-element.70), channel_id=1, source_target_pairs={{0,32},{32,64},{64,96},{96,0},{1,33},{33,65},{65,97},{97,1},{2,34}... | collective-permute-start | bytes 589832 | tf_op jit(solution)/shard_map/ppermute | solution.py:24
  33.6 10.9 %collective-permute-start.1 = (bf16[768,128]{1,0:T(8,128)(2,1)}, bf16[768,128]{1,0:T(8,128)(2,1)S(1)}, u32[]{:S(2)}, u32[]{:S(2)}) collective-permute-start(bf16[768,128]{1,0:T(8,128)(2,1)} %get-tuple-element.71), channel_id=1, source_target_pairs={{0,64},{32,96},{64,0},{96,32},{1,65},{33,97},{65,1},{97,33},{2,66}... | collective-permute-start | bytes 589832 | tf_op jit(solution)/shard_map/ppermute | solution.py:24
  44.5 8.6 %collective-permute-start.2 = (bf16[768,128]{1,0:T(8,128)(2,1)}, bf16[768,128]{1,0:T(8,128)(2,1)S(1)}, u32[]{:S(2)}, u32[]{:S(2)}) collective-permute-start(bf16[768,128]{1,0:T(8,128)(2,1)} %get-tuple-element.72), channel_id=1, source_target_pairs={{0,96},{32,0},{64,32},{96,64},{1,97},{33,1},{65,33},{97,65},{2,98}... | collective-permute-start | bytes 589832 | tf_op jit(solution)/shard_map/ppermute | solution.py:24
  44.6 21.2 %copy-start.14 = (s32[4,64]{1,0:T(4,128)S(1)}, s32[4,64]{1,0:T(4,128)}, u32[]{:S(2)}) copy-start(s32[4,64]{1,0:T(4,128)} %constant.22.clone.refs_1_) | copy-start | bytes 3076
  44.6 36.1 %collective-permute-start.6 = (bf16[256,2048]{1,0:T(8,128)(2,1)S(1)}, bf16[256,2048]{1,0:T(8,128)(2,1)}, u32[]{:S(2)}, u32[]{:S(2)}) collective-permute-start(bf16[256,2048]{1,0:T(8,128)(2,1)S(1)} %constant_dynamic-update-slice_fusion.refs_0_), channel_id=1, source_target_pairs={{0,2},{2,4},{4,6},{6,0},{1,3},{3,5},{5,7},{7,1},{8,10},{10,12},{12... | collective-permute-start | bytes 3145736 | tf_op jit(solution)/shard_map/ppermute | solution.py:24
  53.1 27.6 %collective-permute-start.7 = (bf16[256,2048]{1,0:T(8,128)(2,1)S(1)}, bf16[256,2048]{1,0:T(8,128)(2,1)}, u32[]{:S(2)}, u32[]{:S(2)}) collective-permute-start(bf16[256,2048]{1,0:T(8,128)(2,1)S(1)} %constant_dynamic-update-slice_fusion.refs_0_), channel_id=1, source_target_pairs={{0,6},{2,0},{4,2},{6,4},{1,7},{3,1},{5,3},{7,5},{8,14},{10,8},{12,... | collective-permute-start | bytes 3145736 | tf_op jit(solution)/shard_map/ppermute | solution.py:24
  54.1 0.9 copy-start.16
  64.4 37.5 %copy-start.13 = (s32[4,34]{1,0:T(4,128)S(1)}, s32[4,34]{1,0:T(4,128)}, u32[]{:S(2)}) copy-start(s32[4,34]{1,0:T(4,128)} %constant.23.clone.refs_1_) | copy-start | bytes 1636
  64.4 36.9 %collective-permute-start.5 = (bf16[4,800,128]{2,1,0:T(8,128)(2,1)S(1)}, bf16[4,800,128]{2,1,0:T(8,128)(2,1)S(1)}, u32[]{:S(2)}, u32[]{:S(2)}) collective-permute-start(bf16[4,800,128]{2,1,0:T(8,128)(2,1)S(1)} %all-to-all-done.refs_6_), channel_id=1, source_target_pairs={{0,16},{8,24},{16,0},{24,8},{1,17},{9,25},{17,1},{25,9},{2,18},{10... | collective-permute-start | bytes 2457608 | tf_op jit(solution)/shard_map/ppermute | solution.py:24
  65.7 57.0 %collective-permute-start.12 = (bf16[256,2048]{1,0:T(8,128)(2,1)S(1)}, bf16[256,2048]{1,0:T(8,128)(2,1)}, u32[]{:S(2)}, u32[]{:S(2)}) collective-permute-start(bf16[256,2048]{1,0:T(8,128)(2,1)S(1)} %collective-permute-done.8.refs_3_), channel_id=1, source_target_pairs={{0,1},{1,0},{2,3},{3,2},{4,5},{5,4},{6,7},{7,6},{8,9},{9,8},{10,11... | collective-permute-start | bytes 3145736 | tf_op jit(solution)/shard_map/ppermute | solution.py:24
  101.4 37.1 %collective-permute-start.10 = (bf16[256,2048]{1,0:T(8,128)(2,1)}, bf16[256,2048]{1,0:T(8,128)(2,1)}, u32[]{:S(2)}, u32[]{:S(2)}) collective-permute-start(bf16[256,2048]{1,0:T(8,128)(2,1)} %collective-permute-done.6.refs_1_), channel_id=1, source_target_pairs={{0,1},{1,0},{2,3},{3,2},{4,5},{5,4},{6,7},{7,6},{8,9},{9,8},{10,11... | collective-permute-start | bytes 3145736 | tf_op jit(solution)/shard_map/ppermute | solution.py:24
  101.4 37.1 %collective-permute-start.11 = (bf16[256,2048]{1,0:T(8,128)(2,1)}, bf16[256,2048]{1,0:T(8,128)(2,1)}, u32[]{:S(2)}, u32[]{:S(2)}) collective-permute-start(bf16[256,2048]{1,0:T(8,128)(2,1)} %collective-permute-done.7.refs_2_), channel_id=1, source_target_pairs={{0,1},{1,0},{2,3},{3,2},{4,5},{5,4},{6,7},{7,6},{8,9},{9,8},{10,11... | collective-permute-start | bytes 3145736 | tf_op jit(solution)/shard_map/ppermute | solution.py:24
  101.9 36.6 %collective-permute-start.9 = (bf16[256,2048]{1,0:T(8,128)(2,1)S(1)}, bf16[256,2048]{1,0:T(8,128)(2,1)}, u32[]{:S(2)}, u32[]{:S(2)}) collective-permute-start(bf16[256,2048]{1,0:T(8,128)(2,1)S(1)} %constant_dynamic-update-slice_fusion.refs_0_), channel_id=1, source_target_pairs={{0,1},{1,0},{2,3},{3,2},{4,5},{5,4},{6,7},{7,6},{8,9},{9,8},{10,11... | collective-permute-start | bytes 3145736 | tf_op jit(solution)/shard_map/ppermute | solution.py:24
  111.7 0.9 copy-start.5
  112.6 25.9 %copy-start.12 = (f32[2048]{0:T(1024)S(1)}, f32[2048]{0:T(1024)}, u32[]{:S(2)}) copy-start(f32[2048]{0:T(1024)} %param.32) | copy-start | bytes 24580
  112.6 25.9 %all-to-all-start.1 = ((bf16[32,112,128]{2,1,0:T(8,128)(2,1)}), bf16[32,112,128]{2,1,0:T(8,128)(2,1)S(1)}, u32[]{:S(2)}, u32[]{:S(2)}) async-start(bf16[32,112,128]{2,1,0:T(8,128)(2,1)} %copy-done.5), calls=%async_computation.1 | async-start | bytes 1835008 | tf_op jit(solution)/shard_map/all_to_all | solution.py:659
  138.5 1.0 copy-start.7
  144.3 26.7 %copy-start.3 = (bf16[96,2048]{1,0:T(8,128)(2,1)}, bf16[96,2048]{1,0:T(8,128)(2,1)S(1)}, u32[]{:S(2)}) copy-start(bf16[96,2048]{1,0:T(8,128)(2,1)S(1)} %shard_map.204.refs_1_.refs_0_) | copy-start | bytes 1179652
  144.3 12.4 %collective-permute-start.13 = (bf16[96,2048]{1,0:T(8,128)(2,1)S(1)}, bf16[96,2048]{1,0:T(8,128)(2,1)S(1)}, u32[]{:S(2)}, u32[]{:S(2)}) collective-permute-start(bf16[96,2048]{1,0:T(8,128)(2,1)S(1)} %shard_map.204.refs_1_.refs_0_), channel_id=1, source_target_pairs={{0,2},{2,4},{4,6},{6,0},{1,3},{3,5},{5,7},{7,1},{8,10},{10,12},{12... | collective-permute-start | bytes 1179656 | tf_op jit(solution)/shard_map/ppermute | solution.py:24
  144.9 11.8 %collective-permute-start.14 = (bf16[96,2048]{1,0:T(8,128)(2,1)S(1)}, bf16[96,2048]{1,0:T(8,128)(2,1)S(1)}, u32[]{:S(2)}, u32[]{:S(2)}) collective-permute-start(bf16[96,2048]{1,0:T(8,128)(2,1)S(1)} %shard_map.204.refs_1_.refs_0_), channel_id=1, source_target_pairs={{0,6},{2,0},{4,2},{6,4},{1,7},{3,1},{5,3},{7,5},{8,14},{10,8},{12,... | collective-permute-start | bytes 1179656 | tf_op jit(solution)/shard_map/ppermute | solution.py:24
  156.7 5.2 %collective-permute-start.15 = (bf16[96,2048]{1,0:T(8,128)(2,1)S(1)}, bf16[96,2048]{1,0:T(8,128)(2,1)S(1)}, u32[]{:S(2)}, u32[]{:S(2)}) collective-permute-start(bf16[96,2048]{1,0:T(8,128)(2,1)S(1)} %collective-permute-done.13.refs_1_), channel_id=1, source_target_pairs={{0,1},{1,0},{2,3},{3,2},{4,5},{5,4},{6,7},{7,6},{8,9},{9,8},{10,11... | collective-permute-start | bytes 1179656 | tf_op jit(solution)/shard_map/ppermute | solution.py:24
  156.7 5.1 %collective-permute-start.16 = (bf16[96,2048]{1,0:T(8,128)(2,1)S(1)}, bf16[96,2048]{1,0:T(8,128)(2,1)S(1)}, u32[]{:S(2)}, u32[]{:S(2)}) collective-permute-start(bf16[96,2048]{1,0:T(8,128)(2,1)S(1)} %collective-permute-done.14.refs_2_), channel_id=1, source_target_pairs={{0,1},{1,0},{2,3},{3,2},{4,5},{5,4},{6,7},{7,6},{8,9},{9,8},{10,11... | collective-permute-start | bytes 1179656 | tf_op jit(solution)/shard_map/ppermute | solution.py:24
  157.2 13.8 %collective-permute-start.21 = (bf16[96,2048]{1,0:T(8,128)(2,1)S(1)}, bf16[96,2048]{1,0:T(8,128)(2,1)S(1)}, u32[]{:S(2)}, u32[]{:S(2)}) collective-permute-start(bf16[96,2048]{1,0:T(8,128)(2,1)S(1)} %shard_map.204.refs_1_.refs_0_), channel_id=1, source_target_pairs={{0,1},{1,0},{2,3},{3,2},{4,5},{5,4},{6,7},{7,6},{8,9},{9,8},{10,11... | collective-permute-start | bytes 1179656 | tf_op jit(solution)/shard_map/ppermute | solution.py:24
  157.9 12.5 %collective-permute-start.17 = (bf16[48,2048]{1,0:T(8,128)(2,1)}, bf16[48,2048]{1,0:T(8,128)(2,1)S(1)}, u32[]{:S(2)}, u32[]{:S(2)}) collective-permute-start(bf16[48,2048]{1,0:T(8,128)(2,1)} %slice.8), channel_id=1, source_target_pairs={{0,2},{2,4},{4,6},{6,0},{1,3},{3,5},{5,7},{7,1},{8,10},{10,12},{12... | collective-permute-start | bytes 589832 | tf_op jit(solution)/shard_map/ppermute | solution.py:24
  158.6 11.8 %collective-permute-start.18 = (bf16[48,2048]{1,0:T(8,128)(2,1)}, bf16[48,2048]{1,0:T(8,128)(2,1)}, u32[]{:S(2)}, u32[]{:S(2)}) collective-permute-start(bf16[48,2048]{1,0:T(8,128)(2,1)} %slice.9), channel_id=1, source_target_pairs={{0,6},{2,0},{4,2},{6,4},{1,7},{3,1},{5,3},{7,5},{8,14},{10,8},{12,... | collective-permute-start | bytes 589832 | tf_op jit(solution)/shard_map/ppermute | solution.py:24
  161.8 0.7 copy-start.8
  162.6 3.7 %copy-start = (bf16[2048,2304]{1,0:T(8,128)(2,1)S(1)}, bf16[2048,2304]{1,0:T(8,128)(2,1)}, u32[]{:S(2)}) copy-start(bf16[2048,2304]{1,0:T(8,128)(2,1)} %all-gather.2.cloned.1.call-done.refs_5_.refs_6_.refs_3_.refs_4_.refs_2_) | copy-start | bytes 28311556
  166.3 1.0 copy-start.9
  167.3 3.8 %copy-start.1 = (bf16[2048,2304]{1,0:T(8,128)(2,1)S(1)}, bf16[2048,2304]{1,0:T(8,128)(2,1)}, u32[]{:S(2)}) copy-start(bf16[2048,2304]{1,0:T(8,128)(2,1)} %all-gather.2.cloned.1.call-done.refs_5_.refs_6_.refs_3_.refs_4_.refs_2_) | copy-start | bytes 28311556
  170.4 2.5 %collective-permute-start.19 = (bf16[48,2048]{1,0:T(8,128)(2,1)S(1)}, bf16[48,2048]{1,0:T(8,128)(2,1)S(1)}, u32[]{:S(2)}, u32[]{:S(2)}) collective-permute-start(bf16[48,2048]{1,0:T(8,128)(2,1)S(1)} %collective-permute-done.17.refs_1_), channel_id=1, source_target_pairs={{0,1},{1,0},{2,3},{3,2},{4,5},{5,4},{6,7},{7,6},{8,9},{9,8},{10,11... | collective-permute-start | bytes 589832 | tf_op jit(solution)/shard_map/ppermute | solution.py:24
  170.5 2.5 %collective-permute-start.20 = (bf16[48,2048]{1,0:T(8,128)(2,1)}, bf16[48,2048]{1,0:T(8,128)(2,1)S(1)}, u32[]{:S(2)}, u32[]{:S(2)}) collective-permute-start(bf16[48,2048]{1,0:T(8,128)(2,1)} %collective-permute-done.18.refs_2_), channel_id=1, source_target_pairs={{0,1},{1,0},{2,3},{3,2},{4,5},{5,4},{6,7},{7,6},{8,9},{9,8},{10,11... | collective-permute-start | bytes 589832 | tf_op jit(solution)/shard_map/ppermute | solution.py:24
  173.0 8.4 %copy-start.10 = (f32[3,704]{1,0:T(4,128)S(1)}, f32[3,704]{1,0:T(4,128)}, u32[]{:S(2)}) copy-start(f32[3,704]{1,0:T(4,128)} %refs_0_.3) | copy-start | bytes 25348
  173.0 8.4 %copy-start.11 = (f32[3,704]{1,0:T(4,128)S(1)}, f32[3,704]{1,0:T(4,128)}, u32[]{:S(2)}) copy-start(f32[3,704]{1,0:T(4,128)} %refs_1_.6) | copy-start | bytes 25348
  175.4 6.0 %collective-permute-start.22 = (bf16[32,704]{1,0:T(8,128)(2,1)S(1)}, bf16[32,704]{1,0:T(8,128)(2,1)S(1)}, u32[]{:S(2)}, u32[]{:S(2)}) collective-permute-start(bf16[32,704]{1,0:T(8,128)(2,1)S(1)} %get-tuple-element.98), channel_id=1, source_target_pairs={{0,8},{8,16},{16,24},{24,32},{32,40},{40,48},{48,56},{56,64},{64,7... | collective-permute-start | bytes 135176 | tf_op jit(solution)/shard_map/ppermute | solution.py:30
  184.2 0.9 copy-start.6
  185.1 1.7 collective-permute-start.23
  186.8 0.7 copy-start.20
  189.6 3.7 %copy-start.2 = (bf16[2048,2304]{1,0:T(8,128)(2,1)S(1)}, bf16[2048,2304]{1,0:T(8,128)(2,1)}, u32[]{:S(2)}) copy-start(bf16[2048,2304]{1,0:T(8,128)(2,1)} %all-gather.2.cloned.1.call-done.refs_5_.refs_6_.refs_3_.refs_4_.refs_2_) | copy-start | bytes 28311556
  197.6 1.4 copy-start.4
  199.1 2.8 %collective-permute-start.24 = (bf16[3,96,2048]{2,1,0:T(8,128)(2,1)S(1)}, bf16[3,96,2048]{2,1,0:T(8,128)(2,1)S(1)}, u32[]{:S(2)}, u32[]{:S(2)}) collective-permute-start(bf16[3,96,2048]{2,1,0:T(8,128)(2,1)S(1)} %get-tuple-element.110), channel_id=1, source_target_pairs={{0,1},{1,0},{2,3},{3,2},{4,5},{5,4},{6,7},{7,6},{8,9},{9,8},{10,11... | collective-permute-start | bytes 3538952 | tf_op jit(solution)/shard_map/ppermute | solution.py:24
  199.2 13.7 %collective-permute-start.25 = (bf16[96,2048]{1,0:T(8,128)(2,1)}, bf16[96,2048]{1,0:T(8,128)(2,1)S(1)}, u32[]{:S(2)}, u32[]{:S(2)}) collective-permute-start(bf16[96,2048]{1,0:T(8,128)(2,1)} %shard_map.209), channel_id=1, source_target_pairs={{0,4},{2,6},{4,0},{6,2},{1,5},{3,7},{5,1},{7,3},{8,12},{10,14},{12... | collective-permute-start | bytes 1179656 | tf_op jit(solution)/shard_map/ppermute | solution.py:24
  201.9 1.0 copy-start.17
  206.1 13.7 %collective-permute-start.26 = (bf16[96,2048]{1,0:T(8,128)(2,1)}, bf16[96,2048]{1,0:T(8,128)(2,1)S(1)}, u32[]{:S(2)}, u32[]{:S(2)}) collective-permute-start(bf16[96,2048]{1,0:T(8,128)(2,1)} %get-tuple-element.113), channel_id=1, source_target_pairs={{0,6},{2,0},{4,2},{6,4},{1,7},{3,1},{5,3},{7,5},{8,14},{10,8},{12,... | collective-permute-start | bytes 1179656 | tf_op jit(solution)/shard_map/ppermute | solution.py:24
  207.9 12.9 %collective-permute-start.27 = (bf16[96,2048]{1,0:T(8,128)(2,1)}, bf16[96,2048]{1,0:T(8,128)(2,1)S(1)}, u32[]{:S(2)}, u32[]{:S(2)}) collective-permute-start(bf16[96,2048]{1,0:T(8,128)(2,1)} %get-tuple-element.114), channel_id=1, source_target_pairs={{0,2},{2,4},{4,6},{6,0},{1,3},{3,5},{5,7},{7,1},{8,10},{10,12},{12... | collective-permute-start | bytes 1179656 | tf_op jit(solution)/shard_map/ppermute | solution.py:24
  212.9 7.9 %copy-start.21 = (bf16[96,2048]{1,0:T(8,128)(2,1)}, bf16[96,2048]{1,0:T(8,128)(2,1)S(1)}, u32[]{:S(2)}) copy-start(bf16[96,2048]{1,0:T(8,128)(2,1)S(1)} %collective-permute-done.25.refs_2_) | copy-start | bytes 1179652
  219.8 1.0 copy-start.22
  220.7 0.8 copy-start.23
Sparse Core Ops, SparseCore 0:
  27.7 92.0 all-gather.1

commit v6 on v5

--- a/solution.py
+++ b/solution.py
@@ -694,13 +694,14 @@
         cores,
         cost,
     )
-    theirs, mine = down([opposite], [(0, 0, 1, 2)], 4.0)
-    (distant,) = paired(mine, shifted(theirs, "tp_c", 1), [bf16])
-    near, beside, distant = lax.optimization_barrier((near, beside, distant))
-    shares = [shifted(distant, "tp_y", 2)]
-    theirs, mine = down([near, beside], [(0, 0, 1, 0), (1, 0, 2, -1), (1, 1, 3, 1)], 8.0)
-    own, before, after = paired(mine, shifted(theirs, "tp_c", 1), [f32, bf16, bf16])
-    shares += [shifted(before, "tp_y", -1), shifted(after, "tp_y", 1)]
+    theirs, mine = down([beside, opposite], [(0, 0, 2, -1), (0, 1, 3, 1), (1, 0, 1, 2)], 8.0)
+    sums = paired(mine, shifted(theirs, "tp_c", 1), [bf16] * 3)
+    near, sums = lax.optimization_barrier((near, sums))
+    shares = []
+    for part, steps in zip(sums, (-1, 1, 2)):
+        shares.append(shifted(part, "tp_y", steps))
+    theirs, mine = down([near], [(0, 0, 1, 0)], 4.0)
+    (own,) = paired(mine, shifted(theirs, "tp_c", 1), [f32])
     return finish(mixed, own, shares, final_gain)
 
 

time: 232 us -> 236 us (1.017)
    unnamed x49 -> x65, local copies, waits for them, and re-layouts: 16.8 us -> 19.7 us
  transfers between devices with their start and end apart: 31 -> 31, of which waited for: 12 -> 10; matrix products, arithmetic and copies ran while one was open for 1% -> 0% of each run, Pallas kernels for 21% -> 21%
where the time goes in v6:
time: 236 us
  waiting for transfers between devices  93.8 us (40%)
  Pallas kernels  66.5 us (28%)
  starting transfers between devices  41.6 us (18%)
  local copies, waits for them, and re-layouts  19.8 us (8%)
  between operations  13.7 us (6%)
    ppermute x27, waiting for transfers between devices, shifted(): lax.ppermute(value, axis, [(i, (i + steps) % count) for i in range(count)])  64.5 us
    pallas_call x3, Pallas kernels, attend(): pl.pallas_call(body, in_specs=[sm, sm] + [vm] * (len(args) - 2), out_spec...  34.3 us
    ppermute x27, starting transfers between devices, shifted(): lax.ppermute(value, axis, [(i, (i + steps) % count) for i in range(count)])  22.5 us
    unnamed x65, local copies, waits for them, and re-layouts  19.7 us
    all_to_all x1, waiting for transfers between devices, per_device(): lax.all_to_all(state, ('sp_z',) + TP, split_axis=0, concat_axis=0, tiled=...  15.8 us
    all_to_all x1, starting transfers between devices, per_device(): lax.all_to_all(state, ('sp_z',) + TP, split_axis=0, concat_axis=0, tiled=...  10.8 us
    all_to_all x1, waiting for transfers between devices, per_device(): lax.all_to_all(packed, 'sp_z', split_axis=0, concat_axis=0, tiled=True)  10.4 us
    pallas_call x2, Pallas kernels, downs(): pl.pallas_call(body, grid=(1,), in_specs=[pl.BlockSpec(memory_space=pltpu...  7.2 us
  transfers between devices with their start and end apart: 31, of which 10 were waited for; matrix products, arithmetic and copies ran while one was open for 0% of the time, Pallas kernels for 21%

profile of v6, /device:TPU:4, one launch (start us, length us, event | category | flops | bytes accessed | tf_op | source)
XLA Modules:
  0.0 235.5 jit_solution(18201398730159909831)
XLA Ops:
  6.5 3.0 %shard_map.199 = (bf16[4,800,128]{2,1,0:T(8,128)(2,1)}, bf16[768,128]{1,0:T(8,128)(2,1)}, bf16[768,128]{1,0:T(8,128)(2,1)}, bf16[768,128]{1,0:T(8,128)(2,1)}, bf16[768,128]{1,0:T(8,128)(2,1)}) custom-call(s32[1]{0:T(128)} %bitcast.2.slot_ref, bf16[768,128]{1,0:T(8,128)(2,1)} %ks.1, bf16[768,128]{1,0:T(8,128)(2,1)} %vs.1, bf16[768,128]{1,0:T(8,128)(2,1)} %kl.1, ...), custom_call_target="tpu_custom_call" | custom-call | flops 625000000 | tf_op jit(solution)/shard_map/pallas_call | solution.py:89
  9.5 5.4 %all-to-all-start = ((bf16[4,800,128]{2,1,0:T(8,128)(2,1)}), bf16[4,800,128]{2,1,0:T(8,128)(2,1)S(1)}, u32[]{:S(2)}, u32[]{:S(2)}) async-start(bf16[4,800,128]{2,1,0:T(8,128)(2,1)} %get-tuple-element.61), calls=%async_computation | async-start | bytes 1638400 | tf_op jit(solution)/shard_map/all_to_all | solution.py:626
  15.0 2.2 shard_map.200
  17.2 10.4 %all-to-all-done.refs_6_ = bf16[4,800,128]{2,1,0:T(8,128)(2,1)S(1)} async-done(((bf16[4,800,128]{2,1,0:T(8,128)(2,1)}), bf16[4,800,128]{2,1,0:T(8,128)(2,1)S(1)}, u32[]{:S(2)}, u32[]{:S(2)}) %all-to-all-start) | async-done | bytes 819232 | tf_op jit(solution)/shard_map/all_to_all | solution.py:626
  27.7 1.3 collective-permute-start.3
  28.9 0.8 collective-permute-start.4
  29.8 3.3 %collective-permute-start.8 = (bf16[256,2048]{1,0:T(8,128)(2,1)S(1)}, bf16[256,2048]{1,0:T(8,128)(2,1)S(1)}, u32[]{:S(2)}, u32[]{:S(2)}) collective-permute-start(bf16[256,2048]{1,0:T(8,128)(2,1)S(1)} %constant_dynamic-update-slice_fusion.refs_0_), channel_id=1, source_target_pairs={{0,4},{2,6},{4,0},{6,2},{1,5},{3,7},{5,1},{7,3},{8,12},{10,14},{12... | collective-permute-start | bytes 3145736 | tf_op jit(solution)/shard_map/ppermute | solution.py:24
  33.1 0.6 collective-permute-start
  33.6 2.1 collective-permute-start.1
  35.7 8.6 %collective-permute-done.refs_3_ = bf16[768,128]{1,0:T(8,128)(2,1)S(1)} collective-permute-done((bf16[768,128]{1,0:T(8,128)(2,1)S(1)}, bf16[768,128]{1,0:T(8,128)(2,1)S(1)}, u32[]{:S(2)}, u32[]{:S(2)}) %collective-permute-start) | collective-permute-done | bytes 196640 | tf_op jit(solution)/shard_map/ppermute | solution.py:24
  44.3 0.1 pad_add_fusion.1.refs_0_
  44.4 0.6 collective-permute-start.6
  45.0 8.1 %collective-permute-done.2.refs_5_ = bf16[768,128]{1,0:T(8,128)(2,1)S(1)} collective-permute-done((bf16[768,128]{1,0:T(8,128)(2,1)}, bf16[768,128]{1,0:T(8,128)(2,1)S(1)}, u32[]{:S(2)}, u32[]{:S(2)}) %collective-permute-start.2) | collective-permute-done | bytes 196640 | tf_op jit(solution)/shard_map/ppermute | solution.py:24
  53.1 0.5 collective-permute-start.7
  53.6 0.9 copy-done.20
  54.5 9.5 %shard_map.201 = (f32[4,144,768]{2,1,0:T(8,128)S(1)}, f32[4,8,768]{2,1,0:T(8,128)S(1)}) custom-call(s32[2]{0:T(128)S(1)} %pad_add_fusion.1.refs_0_, s32[4,34]{1,0:T(4,128)S(1)} %copy-done.19, bf16[768,128]{1,0:T(8,128)(2,1)S(1)} %copy-done.20, bf16[768,128]{1,0:T(8,128)(2,1)S(1)} %collective-permute-done.refs_3_, ...), custom_call_target="tpu_custom_call" | custom-call | flops 3000000000 | tf_op jit(solution)/shard_map/pallas_call | solution.py:346
  64.0 1.6 collective-permute-start.5
  65.7 15.0 %shard_map.202 = (f32[4,144,768]{2,1,0:T(8,128)S(1)}, f32[4,8,768]{2,1,0:T(8,128)S(1)}) custom-call(s32[2]{0:T(128)S(1)} %pad_add_fusion.1.refs_0_, s32[4,64]{1,0:T(4,128)S(1)} %copy-done.18, bf16[768,128]{1,0:T(8,128)(2,1)S(1)} %copy-done.20, bf16[768,128]{1,0:T(8,128)(2,1)S(1)} %collective-permute-done.refs_3_, ...), custom_call_target="tpu_custom_call" | custom-call | flops 6000000000 | tf_op jit(solution)/shard_map/pallas_call | solution.py:346
  80.7 19.7 %collective-permute-done.5.refs_6_ = bf16[4,800,128]{2,1,0:T(8,128)(2,1)S(1)} collective-permute-done((bf16[4,800,128]{2,1,0:T(8,128)(2,1)S(1)}, bf16[4,800,128]{2,1,0:T(8,128)(2,1)S(1)}, u32[]{:S(2)}, u32[]{:S(2)}) %collective-permute-start.5) | collective-permute-done | bytes 819232 | tf_op jit(solution)/shard_map/ppermute | solution.py:24
  100.4 0.5 collective-permute-start.11
  100.9 9.8 %shard_map.203 = bf16[32,112,128]{2,1,0:T(8,128)(2,1)S(1)} custom-call(s32[2]{0:T(128)S(1)} %pad_add_fusion.1.refs_0_, s32[4,34]{1,0:T(4,128)S(1)} %copy-done.17, bf16[768,128]{1,0:T(8,128)(2,1)S(1)} %copy-done.20, bf16[768,128]{1,0:T(8,128)(2,1)S(1)} %collective-permute-done.refs_3_, bf16[768,128]{1,0:T(8,128)(2,1)S(1)} %collective-permute-done.1.refs_4_, ...), custom_call_target="tpu_custom_call" | custom-call | flops 3000000000 | tf_op jit(solution)/shard_map/pallas_call | solution.py:346
  110.7 0.9 copy-done.5
  111.6 10.8 %all-to-all-start.1 = ((bf16[32,112,128]{2,1,0:T(8,128)(2,1)}), bf16[32,112,128]{2,1,0:T(8,128)(2,1)S(1)}, u32[]{:S(2)}, u32[]{:S(2)}) async-start(bf16[32,112,128]{2,1,0:T(8,128)(2,1)} %copy-done.5), calls=%async_computation.1 | async-start | bytes 1835008 | tf_op jit(solution)/shard_map/all_to_all | solution.py:659
  122.4 0.1 pad_add_fusion.place_ref.refs_0_
  122.5 15.8 %all-to-all-done.1.arrived_ref = bf16[32,112,128]{2,1,0:T(8,128)(2,1)S(1)} async-done(((bf16[32,112,128]{2,1,0:T(8,128)(2,1)}), bf16[32,112,128]{2,1,0:T(8,128)(2,1)S(1)}, u32[]{:S(2)}, u32[]{:S(2)}) %all-to-all-start.1) | async-done | bytes 917536 | tf_op jit(solution)/shard_map/all_to_all | solution.py:659
  138.3 1.0 copy-done.7
  139.3 4.8 %shard_map.204.refs_1_.refs_0_ = bf16[96,2048]{1,0:T(8,128)(2,1)S(1)} custom-call(s32[2]{0:T(128)S(1)} %pad_add_fusion.place_ref.refs_0_, bf16[32,112,128]{2,1,0:T(8,128)(2,1)S(1)} %all-to-all-done.1.arrived_ref, bf16[256,2048]{1,0:T(8,128)(2,1)S(1)} %constant_dynamic-update-slice_fusion.refs_0_, bf16[256,2048]{1,0:T(8,128)(2,1)} %collective-permute-done.6.refs_1_, ...), custom_call_target="tpu_custom_call" | custom-call | flops 1250000000 | tf_op jit(solution)/shard_map/pallas_call | solution.py:396
  144.1 0.6 collective-permute-start.13
  144.7 2.7 %collective-permute-start.14 = (bf16[96,2048]{1,0:T(8,128)(2,1)S(1)}, bf16[96,2048]{1,0:T(8,128)(2,1)S(1)}, u32[]{:S(2)}, u32[]{:S(2)}) collective-permute-start(bf16[96,2048]{1,0:T(8,128)(2,1)S(1)} %shard_map.204.refs_1_.refs_0_), channel_id=1, source_target_pairs={{0,6},{2,0},{4,2},{6,4},{1,7},{3,1},{5,3},{7,5},{8,14},{10,8},{12,... | collective-permute-start | bytes 1179656 | tf_op jit(solution)/shard_map/ppermute | solution.py:24
  147.4 9.1 %collective-permute-done.13.refs_1_ = bf16[96,2048]{1,0:T(8,128)(2,1)S(1)} collective-permute-done((bf16[96,2048]{1,0:T(8,128)(2,1)S(1)}, bf16[96,2048]{1,0:T(8,128)(2,1)S(1)}, u32[]{:S(2)}, u32[]{:S(2)}) %collective-permute-start.13) | collective-permute-done | bytes 393248 | tf_op jit(solution)/shard_map/ppermute | solution.py:24
  156.5 0.5 collective-permute-start.16
  157.1 3.3 %collective-permute-start.18 = (bf16[48,2048]{1,0:T(8,128)(2,1)S(1)}, bf16[48,2048]{1,0:T(8,128)(2,1)S(1)}, u32[]{:S(2)}, u32[]{:S(2)}) collective-permute-start(bf16[48,2048]{1,0:T(8,128)(2,1)S(1)} %slice.9), channel_id=1, source_target_pairs={{0,6},{2,0},{4,2},{6,4},{1,7},{3,1},{5,3},{7,5},{8,14},{10,8},{12,... | collective-permute-start | bytes 589832 | tf_op jit(solution)/shard_map/ppermute | solution.py:24
  160.4 0.7 copy-done.8
  161.1 0.8 copy-done.10
  161.9 3.7 %copy-done = bf16[2048,2304]{1,0:T(8,128)(2,1)S(1)} copy-done((bf16[2048,2304]{1,0:T(8,128)(2,1)S(1)}, bf16[2048,2304]{1,0:T(8,128)(2,1)}, u32[]{:S(2)}) %copy-start) | copy-done | bytes 9437208
  165.6 1.0 copy-done.9
  166.6 1.0 copy-done.11
  167.6 3.1 %shard_map.205 = (bf16[384,704]{1,0:T(8,128)(2,1)S(1)}, bf16[384,704]{1,0:T(8,128)(2,1)S(1)}) custom-call(s32[2]{0:T(128)S(1)} %pad_add_fusion.place_ref.refs_0_, bf16[96,2048]{1,0:T(8,128)(2,1)S(1)} %collective-permute-done.13.refs_1_, bf16[96,2048]{1,0:T(8,128)(2,1)S(1)} %collective-permute-done.14.refs_2_, bf16[96,2048]{1,0:T(8,128)(2,1)S(1)} %copy-done.9, ...), custom_call_target="tpu_custom_call" | custom-call | flops 1000000000 | tf_op jit(solution)/shard_map/pallas_call | solution.py:470
  170.7 0.1 collective-permute-start.19
  170.8 0.5 collective-permute-start.20
  171.3 1.9 shard_map.206
  173.3 0.9 copy-done.13
  174.3 1.9 shard_map.207
  176.2 2.8 %collective-permute-start.22 = (bf16[32,704]{1,0:T(8,128)(2,1)S(1)}, bf16[32,704]{1,0:T(8,128)(2,1)S(1)}, u32[]{:S(2)}, u32[]{:S(2)}) collective-permute-start(bf16[32,704]{1,0:T(8,128)(2,1)S(1)} %get-tuple-element.98), channel_id=1, source_target_pairs={{0,8},{8,16},{16,24},{24,32},{32,40},{40,48},{48,56},{56,64},{64,7... | collective-permute-start | bytes 135176 | tf_op jit(solution)/shard_map/ppermute | solution.py:30
  179.1 3.1 %collective-permute-done.22.refs_3_ = bf16[32,704]{1,0:T(8,128)(2,1)S(1)} collective-permute-done((bf16[32,704]{1,0:T(8,128)(2,1)S(1)}, bf16[32,704]{1,0:T(8,128)(2,1)S(1)}, u32[]{:S(2)}, u32[]{:S(2)}) %collective-permute-start.22) | collective-permute-done | bytes 45088 | tf_op jit(solution)/shard_map/ppermute | solution.py:30
  182.2 4.3 %shard_map.208 = (bf16[3,96,2048]{2,1,0:T(8,128)(2,1)S(1)}, f32[3,96,2048]{2,1,0:T(8,128)S(1)}) custom-call(s32[2]{0:T(128)S(1)} %pad_add_fusion.place_ref.refs_0_, f32[3,704]{1,0:T(4,128)S(1)} %copy-done.14, f32[3,704]{1,0:T(4,128)S(1)} %copy-done.15, bf16[2048,2304]{1,0:T(8,128)(2,1)S(1)} %copy-done.1, ...), custom_call_target="tpu_custom_call" | custom-call | flops 2000000000 | tf_op jit(solution)/shard_map/pallas_call | solution.py:530
  186.6 1.4 copy-done.4
  188.0 2.8 %collective-permute-done.23.their_ref = bf16[3,96,2048]{2,1,0:T(8,128)(2,1)S(1)} collective-permute-done((bf16[3,96,2048]{2,1,0:T(8,128)(2,1)S(1)}, bf16[3,96,2048]{2,1,0:T(8,128)(2,1)S(1)}, u32[]{:S(2)}, u32[]{:S(2)}) %collective-permute-start.23) | collective-permute-done | bytes 1179680 | tf_op jit(solution)/shard_map/ppermute | solution.py:24
  190.8 1.1 copy-done.21
  191.9 3.1 %shard_map.209 = (bf16[96,2048]{1,0:T(8,128)(2,1)}, bf16[96,2048]{1,0:T(8,128)(2,1)}, bf16[96,2048]{1,0:T(8,128)(2,1)}) custom-call(f32[3,96,2048]{2,1,0:T(8,128)} %copy-done.4, bf16[3,96,2048]{2,1,0:T(8,128)(2,1)} %copy-done.21), custom_call_target="tpu_custom_call" | custom-call | flops 525000000 | tf_op jit(solution)/shard_map/pallas_call | solution.py:555
  194.9 3.7 %copy-done.2 = bf16[2048,2304]{1,0:T(8,128)(2,1)S(1)} copy-done((bf16[2048,2304]{1,0:T(8,128)(2,1)S(1)}, bf16[2048,2304]{1,0:T(8,128)(2,1)}, u32[]{:S(2)}) %copy-start.2) | copy-done | bytes 9437208
  198.6 2.9 %shard_map.210 = (bf16[1,96,2048]{2,1,0:T(8,128)(2,1)S(1)}, f32[1,96,2048]{2,1,0:T(8,128)S(1)}) custom-call(s32[2]{0:T(128)S(1)} %pad_add_fusion.place_ref.refs_0_, f32[3,704]{1,0:T(4,128)S(1)} %copy-done.14, f32[3,704]{1,0:T(4,128)S(1)} %copy-done.15, bf16[2048,2304]{1,0:T(8,128)(2,1)S(1)} %copy-done.2, ...), custom_call_target="tpu_custom_call" | custom-call | flops 1000000000 | tf_op jit(solution)/shard_map/pallas_call | solution.py:530
  201.5 0.9 copy-done.6
  202.4 0.1 collective-permute-start.24
  202.5 1.7 collective-permute-start.25
  204.3 0.3 collective-permute-start.26
  204.6 1.2 collective-permute-start.27
  205.8 0.7 copy-done.27
  206.6 2.2 shard_map.211.refs_1_
  208.8 5.7 %collective-permute-done.25.refs_2_ = bf16[96,2048]{1,0:T(8,128)(2,1)S(1)} collective-permute-done((bf16[96,2048]{1,0:T(8,128)(2,1)S(1)}, bf16[96,2048]{1,0:T(8,128)(2,1)S(1)}, u32[]{:S(2)}, u32[]{:S(2)}) %collective-permute-start.25) | collective-permute-done | bytes 393248 | tf_op jit(solution)/shard_map/ppermute | solution.py:24
  214.5 10.5 %collective-permute-done.26.refs_3_ = bf16[96,2048]{1,0:T(8,128)(2,1)S(1)} collective-permute-done((bf16[96,2048]{1,0:T(8,128)(2,1)S(1)}, bf16[96,2048]{1,0:T(8,128)(2,1)S(1)}, u32[]{:S(2)}, u32[]{:S(2)}) %collective-permute-start.26) | collective-permute-done | bytes 393248 | tf_op jit(solution)/shard_map/ppermute | solution.py:24
  225.0 0.7 copy-done.25
  225.8 0.1 copy-done.26
  225.9 2.8 %shard_map.212 = bf16[96,2048]{1,0:T(8,128)(2,1)} custom-call(bf16[96,2048]{1,0:T(8,128)(2,1)} %copy-done.3, f32[96,2048]{1,0:T(8,128)} %shard_map.211.refs_1_, bf16[96,2048]{1,0:T(8,128)(2,1)} %copy-done.24, bf16[96,2048]{1,0:T(8,128)(2,1)} %copy-done.25, bf16[96,2048]{1,0:T(8,128)(2,1)} %copy-done.26, f32[1,2048]{1,0:T(1,128)} %bitcast.11), custom_call_target="tpu_custom_call" | custom-call | flops 500000000 | tf_op jit(solution)/shard_map/pallas_call | solution.py:580
  (83 shorter events, 0.4 us)
Async XLA Ops:
  9.5 18.1 %copy-start.22 = (bf16[128,2048]{1,0:T(8,128)(2,1)S(1)}, bf16[128,2048]{1,0:T(8,128)(2,1)}, u32[]{:S(2)}) copy-start(bf16[128,2048]{1,0:T(8,128)(2,1)} %param.30) | copy-start | bytes 1572868
  9.5 18.1 %all-to-all-start = ((bf16[4,800,128]{2,1,0:T(8,128)(2,1)}), bf16[4,800,128]{2,1,0:T(8,128)(2,1)S(1)}, u32[]{:S(2)}, u32[]{:S(2)}) async-start(bf16[4,800,128]{2,1,0:T(8,128)(2,1)} %get-tuple-element.61), calls=%async_computation | async-start | bytes 1638400 | tf_op jit(solution)/shard_map/all_to_all | solution.py:626
  14.9 14.8 %copy-start.23 = (bf16[128,2048]{1,0:T(8,128)(2,1)S(1)}, bf16[128,2048]{1,0:T(8,128)(2,1)}, u32[]{:S(2)}) copy-start(bf16[128,2048]{1,0:T(8,128)(2,1)} %param.31) | copy-start | bytes 1572868
  14.9 18.1 %copy-start.31 = (bf16[768,128]{1,0:T(8,128)(2,1)S(1)}, bf16[768,128]{1,0:T(8,128)(2,1)}, u32[]{:S(2)}) copy-start(bf16[768,128]{1,0:T(8,128)(2,1)} %get-tuple-element.70) | copy-start | bytes 589828
  14.9 38.7 %copy-start.19 = (s32[4,34]{1,0:T(4,128)S(1)}, s32[4,34]{1,0:T(4,128)}, u32[]{:S(2)}) copy-start(s32[4,34]{1,0:T(4,128)} %constant.21.clone.refs_1_) | copy-start | bytes 1636
  14.9 147.0 %all-gather.2.cloned.1.call-start = ((), (), s32[]{:S(2)}) async-start(), calls=%async_computation.2 | async-start | bytes 10027008 | tf_op jit(solution)/shard_map/all_gather | solution.py:629
  27.7 36.4 %collective-permute-start.3 = (bf16[4,800,128]{2,1,0:T(8,128)(2,1)S(1)}, bf16[4,800,128]{2,1,0:T(8,128)(2,1)}, u32[]{:S(2)}, u32[]{:S(2)}) collective-permute-start(bf16[4,800,128]{2,1,0:T(8,128)(2,1)S(1)} %all-to-all-done.refs_6_), channel_id=1, source_target_pairs={{0,8},{8,16},{16,24},{24,0},{1,9},{9,17},{17,25},{25,1},{2,10},{10... | collective-permute-start | bytes 2457608 | tf_op jit(solution)/shard_map/ppermute | solution.py:24
  28.9 35.1 %collective-permute-start.4 = (bf16[4,800,128]{2,1,0:T(8,128)(2,1)S(1)}, bf16[4,800,128]{2,1,0:T(8,128)(2,1)}, u32[]{:S(2)}, u32[]{:S(2)}) collective-permute-start(bf16[4,800,128]{2,1,0:T(8,128)(2,1)S(1)} %all-to-all-done.refs_6_), channel_id=1, source_target_pairs={{0,24},{8,0},{16,8},{24,16},{1,25},{9,1},{17,9},{25,17},{2,26},{10... | collective-permute-start | bytes 2457608 | tf_op jit(solution)/shard_map/ppermute | solution.py:24
  29.8 35.9 %collective-permute-start.8 = (bf16[256,2048]{1,0:T(8,128)(2,1)S(1)}, bf16[256,2048]{1,0:T(8,128)(2,1)S(1)}, u32[]{:S(2)}, u32[]{:S(2)}) collective-permute-start(bf16[256,2048]{1,0:T(8,128)(2,1)S(1)} %constant_dynamic-update-slice_fusion.refs_0_), channel_id=1, source_target_pairs={{0,4},{2,6},{4,0},{6,2},{1,5},{3,7},{5,1},{7,3},{8,12},{10,14},{12... | collective-permute-start | bytes 3145736 | tf_op jit(solution)/shard_map/ppermute | solution.py:24
  33.1 11.2 %collective-permute-start = (bf16[768,128]{1,0:T(8,128)(2,1)S(1)}, bf16[768,128]{1,0:T(8,128)(2,1)S(1)}, u32[]{:S(2)}, u32[]{:S(2)}) collective-permute-start(bf16[768,128]{1,0:T(8,128)(2,1)S(1)} %copy-done.31), channel_id=1, source_target_pairs={{0,32},{32,64},{64,96},{96,0},{1,33},{33,65},{65,97},{97,1},{2,34}... | collective-permute-start | bytes 589832 | tf_op jit(solution)/shard_map/ppermute | solution.py:24
  33.6 10.7 %collective-permute-start.1 = (bf16[768,128]{1,0:T(8,128)(2,1)}, bf16[768,128]{1,0:T(8,128)(2,1)S(1)}, u32[]{:S(2)}, u32[]{:S(2)}) collective-permute-start(bf16[768,128]{1,0:T(8,128)(2,1)} %get-tuple-element.71), channel_id=1, source_target_pairs={{0,64},{32,96},{64,0},{96,32},{1,65},{33,97},{65,1},{97,33},{2,66}... | collective-permute-start | bytes 589832 | tf_op jit(solution)/shard_map/ppermute | solution.py:24
  44.3 8.8 %collective-permute-start.2 = (bf16[768,128]{1,0:T(8,128)(2,1)}, bf16[768,128]{1,0:T(8,128)(2,1)S(1)}, u32[]{:S(2)}, u32[]{:S(2)}) collective-permute-start(bf16[768,128]{1,0:T(8,128)(2,1)} %get-tuple-element.72), channel_id=1, source_target_pairs={{0,96},{32,0},{64,32},{96,64},{1,97},{33,1},{65,33},{97,65},{2,98}... | collective-permute-start | bytes 589832 | tf_op jit(solution)/shard_map/ppermute | solution.py:24
  44.4 21.3 %copy-start.18 = (s32[4,64]{1,0:T(4,128)S(1)}, s32[4,64]{1,0:T(4,128)}, u32[]{:S(2)}) copy-start(s32[4,64]{1,0:T(4,128)} %constant.22.clone.refs_1_) | copy-start | bytes 3076
  44.4 36.3 %collective-permute-start.6 = (bf16[256,2048]{1,0:T(8,128)(2,1)S(1)}, bf16[256,2048]{1,0:T(8,128)(2,1)}, u32[]{:S(2)}, u32[]{:S(2)}) collective-permute-start(bf16[256,2048]{1,0:T(8,128)(2,1)S(1)} %constant_dynamic-update-slice_fusion.refs_0_), channel_id=1, source_target_pairs={{0,2},{2,4},{4,6},{6,0},{1,3},{3,5},{5,7},{7,1},{8,10},{10,12},{12... | collective-permute-start | bytes 3145736 | tf_op jit(solution)/shard_map/ppermute | solution.py:24
  53.1 27.7 %collective-permute-start.7 = (bf16[256,2048]{1,0:T(8,128)(2,1)S(1)}, bf16[256,2048]{1,0:T(8,128)(2,1)}, u32[]{:S(2)}, u32[]{:S(2)}) collective-permute-start(bf16[256,2048]{1,0:T(8,128)(2,1)S(1)} %constant_dynamic-update-slice_fusion.refs_0_), channel_id=1, source_target_pairs={{0,6},{2,0},{4,2},{6,4},{1,7},{3,1},{5,3},{7,5},{8,14},{10,8},{12,... | collective-permute-start | bytes 3145736 | tf_op jit(solution)/shard_map/ppermute | solution.py:24
  53.6 0.9 copy-start.20
  64.0 36.9 %copy-start.17 = (s32[4,34]{1,0:T(4,128)S(1)}, s32[4,34]{1,0:T(4,128)}, u32[]{:S(2)}) copy-start(s32[4,34]{1,0:T(4,128)} %constant.23.clone.refs_1_) | copy-start | bytes 1636
  64.0 36.4 %collective-permute-start.5 = (bf16[4,800,128]{2,1,0:T(8,128)(2,1)S(1)}, bf16[4,800,128]{2,1,0:T(8,128)(2,1)S(1)}, u32[]{:S(2)}, u32[]{:S(2)}) collective-permute-start(bf16[4,800,128]{2,1,0:T(8,128)(2,1)S(1)} %all-to-all-done.refs_6_), channel_id=1, source_target_pairs={{0,16},{8,24},{16,0},{24,8},{1,17},{9,25},{17,1},{25,9},{2,18},{10... | collective-permute-start | bytes 2457608 | tf_op jit(solution)/shard_map/ppermute | solution.py:24
  65.7 56.9 %collective-permute-start.12 = (bf16[256,2048]{1,0:T(8,128)(2,1)S(1)}, bf16[256,2048]{1,0:T(8,128)(2,1)}, u32[]{:S(2)}, u32[]{:S(2)}) collective-permute-start(bf16[256,2048]{1,0:T(8,128)(2,1)S(1)} %collective-permute-done.8.refs_3_), channel_id=1, source_target_pairs={{0,1},{1,0},{2,3},{3,2},{4,5},{5,4},{6,7},{7,6},{8,9},{9,8},{10,11... | collective-permute-start | bytes 3145736 | tf_op jit(solution)/shard_map/ppermute | solution.py:24
  100.4 37.9 %collective-permute-start.10 = (bf16[256,2048]{1,0:T(8,128)(2,1)}, bf16[256,2048]{1,0:T(8,128)(2,1)}, u32[]{:S(2)}, u32[]{:S(2)}) collective-permute-start(bf16[256,2048]{1,0:T(8,128)(2,1)} %collective-permute-done.6.refs_1_), channel_id=1, source_target_pairs={{0,1},{1,0},{2,3},{3,2},{4,5},{5,4},{6,7},{7,6},{8,9},{9,8},{10,11... | collective-permute-start | bytes 3145736 | tf_op jit(solution)/shard_map/ppermute | solution.py:24
  100.4 37.9 %collective-permute-start.11 = (bf16[256,2048]{1,0:T(8,128)(2,1)}, bf16[256,2048]{1,0:T(8,128)(2,1)}, u32[]{:S(2)}, u32[]{:S(2)}) collective-permute-start(bf16[256,2048]{1,0:T(8,128)(2,1)} %collective-permute-done.7.refs_2_), channel_id=1, source_target_pairs={{0,1},{1,0},{2,3},{3,2},{4,5},{5,4},{6,7},{7,6},{8,9},{9,8},{10,11... | collective-permute-start | bytes 3145736 | tf_op jit(solution)/shard_map/ppermute | solution.py:24
  100.9 37.4 %collective-permute-start.9 = (bf16[256,2048]{1,0:T(8,128)(2,1)S(1)}, bf16[256,2048]{1,0:T(8,128)(2,1)}, u32[]{:S(2)}, u32[]{:S(2)}) collective-permute-start(bf16[256,2048]{1,0:T(8,128)(2,1)S(1)} %constant_dynamic-update-slice_fusion.refs_0_), channel_id=1, source_target_pairs={{0,1},{1,0},{2,3},{3,2},{4,5},{5,4},{6,7},{7,6},{8,9},{9,8},{10,11... | collective-permute-start | bytes 3145736 | tf_op jit(solution)/shard_map/ppermute | solution.py:24
  110.7 0.9 copy-start.5
  111.6 26.7 %copy-start.16 = (f32[2048]{0:T(1024)S(1)}, f32[2048]{0:T(1024)}, u32[]{:S(2)}) copy-start(f32[2048]{0:T(1024)} %param.32) | copy-start | bytes 24580
  111.6 26.6 %all-to-all-start.1 = ((bf16[32,112,128]{2,1,0:T(8,128)(2,1)}), bf16[32,112,128]{2,1,0:T(8,128)(2,1)S(1)}, u32[]{:S(2)}, u32[]{:S(2)}) async-start(bf16[32,112,128]{2,1,0:T(8,128)(2,1)} %copy-done.5), calls=%async_computation.1 | async-start | bytes 1835008 | tf_op jit(solution)/shard_map/all_to_all | solution.py:659
  138.3 1.0 copy-start.7
  144.1 27.3 %copy-start.3 = (bf16[96,2048]{1,0:T(8,128)(2,1)}, bf16[96,2048]{1,0:T(8,128)(2,1)S(1)}, u32[]{:S(2)}) copy-start(bf16[96,2048]{1,0:T(8,128)(2,1)S(1)} %shard_map.204.refs_1_.refs_0_) | copy-start | bytes 1179652
  144.1 12.4 %collective-permute-start.13 = (bf16[96,2048]{1,0:T(8,128)(2,1)S(1)}, bf16[96,2048]{1,0:T(8,128)(2,1)S(1)}, u32[]{:S(2)}, u32[]{:S(2)}) collective-permute-start(bf16[96,2048]{1,0:T(8,128)(2,1)S(1)} %shard_map.204.refs_1_.refs_0_), channel_id=1, source_target_pairs={{0,2},{2,4},{4,6},{6,0},{1,3},{3,5},{5,7},{7,1},{8,10},{10,12},{12... | collective-permute-start | bytes 1179656 | tf_op jit(solution)/shard_map/ppermute | solution.py:24
  144.7 11.8 %collective-permute-start.14 = (bf16[96,2048]{1,0:T(8,128)(2,1)S(1)}, bf16[96,2048]{1,0:T(8,128)(2,1)S(1)}, u32[]{:S(2)}, u32[]{:S(2)}) collective-permute-start(bf16[96,2048]{1,0:T(8,128)(2,1)S(1)} %shard_map.204.refs_1_.refs_0_), channel_id=1, source_target_pairs={{0,6},{2,0},{4,2},{6,4},{1,7},{3,1},{5,3},{7,5},{8,14},{10,8},{12,... | collective-permute-start | bytes 1179656 | tf_op jit(solution)/shard_map/ppermute | solution.py:24
  156.4 3.9 %collective-permute-start.15 = (bf16[96,2048]{1,0:T(8,128)(2,1)S(1)}, bf16[96,2048]{1,0:T(8,128)(2,1)S(1)}, u32[]{:S(2)}, u32[]{:S(2)}) collective-permute-start(bf16[96,2048]{1,0:T(8,128)(2,1)S(1)} %collective-permute-done.13.refs_1_), channel_id=1, source_target_pairs={{0,1},{1,0},{2,3},{3,2},{4,5},{5,4},{6,7},{7,6},{8,9},{9,8},{10,11... | collective-permute-start | bytes 1179656 | tf_op jit(solution)/shard_map/ppermute | solution.py:24
  156.5 4.7 %collective-permute-start.16 = (bf16[96,2048]{1,0:T(8,128)(2,1)S(1)}, bf16[96,2048]{1,0:T(8,128)(2,1)S(1)}, u32[]{:S(2)}, u32[]{:S(2)}) collective-permute-start(bf16[96,2048]{1,0:T(8,128)(2,1)S(1)} %collective-permute-done.14.refs_2_), channel_id=1, source_target_pairs={{0,1},{1,0},{2,3},{3,2},{4,5},{5,4},{6,7},{7,6},{8,9},{9,8},{10,11... | collective-permute-start | bytes 1179656 | tf_op jit(solution)/shard_map/ppermute | solution.py:24
  157.0 14.4 %collective-permute-start.21 = (bf16[96,2048]{1,0:T(8,128)(2,1)S(1)}, bf16[96,2048]{1,0:T(8,128)(2,1)S(1)}, u32[]{:S(2)}, u32[]{:S(2)}) collective-permute-start(bf16[96,2048]{1,0:T(8,128)(2,1)S(1)} %shard_map.204.refs_1_.refs_0_), channel_id=1, source_target_pairs={{0,1},{1,0},{2,3},{3,2},{4,5},{5,4},{6,7},{7,6},{8,9},{9,8},{10,11... | collective-permute-start | bytes 1179656 | tf_op jit(solution)/shard_map/ppermute | solution.py:24
  157.0 13.7 %collective-permute-start.17 = (bf16[48,2048]{1,0:T(8,128)(2,1)S(1)}, bf16[48,2048]{1,0:T(8,128)(2,1)S(1)}, u32[]{:S(2)}, u32[]{:S(2)}) collective-permute-start(bf16[48,2048]{1,0:T(8,128)(2,1)S(1)} %slice.8), channel_id=1, source_target_pairs={{0,2},{2,4},{4,6},{6,0},{1,3},{3,5},{5,7},{7,1},{8,10},{10,12},{12... | collective-permute-start | bytes 589832 | tf_op jit(solution)/shard_map/ppermute | solution.py:24
  157.1 13.6 %collective-permute-start.18 = (bf16[48,2048]{1,0:T(8,128)(2,1)S(1)}, bf16[48,2048]{1,0:T(8,128)(2,1)S(1)}, u32[]{:S(2)}, u32[]{:S(2)}) collective-permute-start(bf16[48,2048]{1,0:T(8,128)(2,1)S(1)} %slice.9), channel_id=1, source_target_pairs={{0,6},{2,0},{4,2},{6,4},{1,7},{3,1},{5,3},{7,5},{8,14},{10,8},{12,... | collective-permute-start | bytes 589832 | tf_op jit(solution)/shard_map/ppermute | solution.py:24
  160.4 0.7 copy-start.8
  161.1 0.8 copy-start.10
  161.9 3.7 %copy-start = (bf16[2048,2304]{1,0:T(8,128)(2,1)S(1)}, bf16[2048,2304]{1,0:T(8,128)(2,1)}, u32[]{:S(2)}) copy-start(bf16[2048,2304]{1,0:T(8,128)(2,1)} %all-gather.2.cloned.1.call-done.refs_5_.refs_6_.refs_3_.refs_4_.refs_2_) | copy-start | bytes 28311556
  165.6 1.0 copy-start.9
  166.6 1.0 copy-start.11
  167.6 3.8 %copy-start.1 = (bf16[2048,2304]{1,0:T(8,128)(2,1)S(1)}, bf16[2048,2304]{1,0:T(8,128)(2,1)}, u32[]{:S(2)}) copy-start(bf16[2048,2304]{1,0:T(8,128)(2,1)} %all-gather.2.cloned.1.call-done.refs_5_.refs_6_.refs_3_.refs_4_.refs_2_) | copy-start | bytes 28311556
  170.7 2.6 %copy-start.12 = (bf16[48,2048]{1,0:T(8,128)(2,1)}, bf16[48,2048]{1,0:T(8,128)(2,1)S(1)}, u32[]{:S(2)}) copy-start(bf16[48,2048]{1,0:T(8,128)(2,1)S(1)} %collective-permute-done.18.refs_2_) | copy-start | bytes 589828
  170.7 2.6 %collective-permute-start.19 = (bf16[48,2048]{1,0:T(8,128)(2,1)S(1)}, bf16[48,2048]{1,0:T(8,128)(2,1)S(1)}, u32[]{:S(2)}, u32[]{:S(2)}) collective-permute-start(bf16[48,2048]{1,0:T(8,128)(2,1)S(1)} %collective-permute-done.17.refs_1_), channel_id=1, source_target_pairs={{0,1},{1,0},{2,3},{3,2},{4,5},{5,4},{6,7},{7,6},{8,9},{9,8},{10,11... | collective-permute-start | bytes 589832 | tf_op jit(solution)/shard_map/ppermute | solution.py:24
  170.8 2.5 %collective-permute-start.20 = (bf16[48,2048]{1,0:T(8,128)(2,1)S(1)}, bf16[48,2048]{1,0:T(8,128)(2,1)S(1)}, u32[]{:S(2)}, u32[]{:S(2)}) collective-permute-start(bf16[48,2048]{1,0:T(8,128)(2,1)S(1)} %collective-permute-done.18.refs_2_), channel_id=1, source_target_pairs={{0,1},{1,0},{2,3},{3,2},{4,5},{5,4},{6,7},{7,6},{8,9},{9,8},{10,11... | collective-permute-start | bytes 589832 | tf_op jit(solution)/shard_map/ppermute | solution.py:24
  173.3 0.9 copy-start.13
  174.3 7.9 %copy-start.14 = (f32[3,704]{1,0:T(4,128)S(1)}, f32[3,704]{1,0:T(4,128)}, u32[]{:S(2)}) copy-start(f32[3,704]{1,0:T(4,128)} %refs_0_.3) | copy-start | bytes 25348
  174.3 7.9 %copy-start.15 = (f32[3,704]{1,0:T(4,128)S(1)}, f32[3,704]{1,0:T(4,128)}, u32[]{:S(2)}) copy-start(f32[3,704]{1,0:T(4,128)} %refs_1_.6) | copy-start | bytes 25348
  176.2 6.0 %collective-permute-start.22 = (bf16[32,704]{1,0:T(8,128)(2,1)S(1)}, bf16[32,704]{1,0:T(8,128)(2,1)S(1)}, u32[]{:S(2)}, u32[]{:S(2)}) collective-permute-start(bf16[32,704]{1,0:T(8,128)(2,1)S(1)} %get-tuple-element.98), channel_id=1, source_target_pairs={{0,8},{8,16},{16,24},{24,32},{32,40},{40,48},{48,56},{56,64},{64,7... | collective-permute-start | bytes 135176 | tf_op jit(solution)/shard_map/ppermute | solution.py:30
  186.6 1.4 copy-start.4
  188.0 2.8 %collective-permute-start.23 = (bf16[3,96,2048]{2,1,0:T(8,128)(2,1)S(1)}, bf16[3,96,2048]{2,1,0:T(8,128)(2,1)S(1)}, u32[]{:S(2)}, u32[]{:S(2)}) collective-permute-start(bf16[3,96,2048]{2,1,0:T(8,128)(2,1)S(1)} %get-tuple-element.104), channel_id=1, source_target_pairs={{0,1},{1,0},{2,3},{3,2},{4,5},{5,4},{6,7},{7,6},{8,9},{9,8},{10,11... | collective-permute-start | bytes 3538952 | tf_op jit(solution)/shard_map/ppermute | solution.py:24
  190.8 1.1 copy-start.21
  194.9 3.7 %copy-start.2 = (bf16[2048,2304]{1,0:T(8,128)(2,1)S(1)}, bf16[2048,2304]{1,0:T(8,128)(2,1)}, u32[]{:S(2)}) copy-start(bf16[2048,2304]{1,0:T(8,128)(2,1)} %all-gather.2.cloned.1.call-done.refs_5_.refs_6_.refs_3_.refs_4_.refs_2_) | copy-start | bytes 28311556
  198.6 3.9 %copy-start.30 = (bf16[96,2048]{1,0:T(8,128)(2,1)S(1)}, bf16[96,2048]{1,0:T(8,128)(2,1)}, u32[]{:S(2)}) copy-start(bf16[96,2048]{1,0:T(8,128)(2,1)} %get-tuple-element.112) | copy-start | bytes 1179652
  198.6 5.6 %copy-start.29 = (bf16[96,2048]{1,0:T(8,128)(2,1)S(1)}, bf16[96,2048]{1,0:T(8,128)(2,1)}, u32[]{:S(2)}) copy-start(bf16[96,2048]{1,0:T(8,128)(2,1)} %get-tuple-element.113) | copy-start | bytes 1179652
  198.6 5.9 %copy-start.28 = (bf16[96,2048]{1,0:T(8,128)(2,1)S(1)}, bf16[96,2048]{1,0:T(8,128)(2,1)}, u32[]{:S(2)}) copy-start(bf16[96,2048]{1,0:T(8,128)(2,1)} %get-tuple-element.114) | copy-start | bytes 1179652
  201.5 0.9 copy-start.6
  202.4 3.4 %collective-permute-start.24 = (bf16[1,96,2048]{2,1,0:T(8,128)(2,1)S(1)}, bf16[1,96,2048]{2,1,0:T(8,128)(2,1)S(1)}, u32[]{:S(2)}, u32[]{:S(2)}) collective-permute-start(bf16[1,96,2048]{2,1,0:T(8,128)(2,1)S(1)} %get-tuple-element.111), channel_id=1, source_target_pairs={{0,1},{1,0},{2,3},{3,2},{4,5},{5,4},{6,7},{7,6},{8,9},{9,8},{10,11... | collective-permute-start | bytes 1179656 | tf_op jit(solution)/shard_map/ppermute | solution.py:24
  202.5 12.0 %collective-permute-start.25 = (bf16[96,2048]{1,0:T(8,128)(2,1)S(1)}, bf16[96,2048]{1,0:T(8,128)(2,1)S(1)}, u32[]{:S(2)}, u32[]{:S(2)}) collective-permute-start(bf16[96,2048]{1,0:T(8,128)(2,1)S(1)} %copy-done.30), channel_id=1, source_target_pairs={{0,6},{2,0},{4,2},{6,4},{1,7},{3,1},{5,3},{7,5},{8,14},{10,8},{12,... | collective-permute-start | bytes 1179656 | tf_op jit(solution)/shard_map/ppermute | solution.py:24
  204.3 20.8 %collective-permute-start.26 = (bf16[96,2048]{1,0:T(8,128)(2,1)S(1)}, bf16[96,2048]{1,0:T(8,128)(2,1)S(1)}, u32[]{:S(2)}, u32[]{:S(2)}) collective-permute-start(bf16[96,2048]{1,0:T(8,128)(2,1)S(1)} %copy-done.29), channel_id=1, source_target_pairs={{0,2},{2,4},{4,6},{6,0},{1,3},{3,5},{5,7},{7,1},{8,10},{10,12},{12... | collective-permute-start | bytes 1179656 | tf_op jit(solution)/shard_map/ppermute | solution.py:24
  204.6 20.5 %collective-permute-start.27 = (bf16[96,2048]{1,0:T(8,128)(2,1)S(1)}, bf16[96,2048]{1,0:T(8,128)(2,1)S(1)}, u32[]{:S(2)}, u32[]{:S(2)}) collective-permute-start(bf16[96,2048]{1,0:T(8,128)(2,1)S(1)} %copy-done.28), channel_id=1, source_target_pairs={{0,4},{2,6},{4,0},{6,2},{1,5},{3,7},{5,1},{7,3},{8,12},{10,14},{12... | collective-permute-start | bytes 1179656 | tf_op jit(solution)/shard_map/ppermute | solution.py:24
  205.8 0.7 copy-start.27
  214.5 10.5 %copy-start.24 = (bf16[96,2048]{1,0:T(8,128)(2,1)}, bf16[96,2048]{1,0:T(8,128)(2,1)S(1)}, u32[]{:S(2)}) copy-start(bf16[96,2048]{1,0:T(8,128)(2,1)S(1)} %collective-permute-done.25.refs_2_) | copy-start | bytes 1179652
  225.0 0.7 copy-start.25
  225.0 0.9 copy-start.26
Sparse Core Ops, SparseCore 0:
  27.7 91.3 all-gather.1
